TPU v7x, 32 devices: a whole 2x2x4 slice. The times are simulated.
32 devices in a mesh: sp: 8 (over z, y), tp: 4 (over x, core).
Axes of the slice: x: 2, y: 2, z: 4, core: 2. Of those that a mesh axis runs over, the one named last changes fastest.
Arguments:
- out_grad: bfloat16 [1024, 2048], P('sp'), may hold values from -6 to 6
- residual: bfloat16 [1024, 2048], P('sp'), may hold values from -6 to 6
- routes: int32 [1024, 2], P('sp'), may hold values from 0 to 3, all different within a row; in each aligned block of 128 rows (0 to 127, 128 to 255, ...) at most 80 rows name the same one
- route_weights: float32 [1024, 2], P('sp'), may hold values from 0.15 to 0.85, as said below
- w_gate: bfloat16 [8, 2048, 2048], P('sp', None, 'tp'), may hold values from -0.125 to 0.125
- w_up: bfloat16 [8, 2048, 2048], P('sp', None, 'tp'), may hold values from -0.125 to 0.125
- w_down: bfloat16 [8, 2048, 2048], P('sp', 'tp'), may hold values from -0.09375 to 0.09375
- out_gate: bfloat16 [1024, 1024], P('sp', 'tp'), may hold values from -6 to 6
- in_gate: bfloat16 [1024, 1024], P('sp', 'tp'), may hold values from -6 to 6
- conv_input: bfloat16 [1024, 1024], P('sp', 'tp'), may hold values from -6 to 6
- conv_out: bfloat16 [1024, 1024], P('sp', 'tp'), may hold values from -6 to 6
- conv_taps: float32 [3, 1024], P(None, 'tp'), may hold values from -3.5 to 3.5
- w_out: bfloat16 [1024, 2048], P('tp'), may hold values from -0.1875 to 0.1875
Outputs:
- grad_resid: bfloat16 [1024, 2048], P('sp')
- grad_up: bfloat16 [8, 2048, 2048], P('sp', None, 'tp')
- grad_down: bfloat16 [8, 2048, 2048], P('sp', 'tp')
- grad_out_gate: bfloat16 [1024, 1024], P('sp', 'tp')
- grad_in_gate: bfloat16 [1024, 1024], P('sp', 'tp')
- grad_conv_input: bfloat16 [1024, 1024], P('sp', 'tp')
- grad_w_out: float32 [2048, 1024], P('sp', 'tp')
Inputs may be any that keep to these rules, and one draw needn't show every extreme that they name: `routes`: each row names 2 different experts. In the rows of one index of sp no expert is named more than 80 times, a bound that some block reaches. `route_weights`: the two weights of a row sum to one.
All inputs are finite; a program needn't handle non-finite values.
Results may differ from a plain program's by a relative error of at most 0.013.
Values may be sent and summed in bfloat16 or wider, within the bound.
No kernel may reach another device: no remote copies, remote signals or barrier semaphores. Data moves between devices by JAX's collectives and lax.ppermute only.
A program may use at most 128 MiB of HBM per device.

v0:
```python
import jax
import jax.numpy as jnp
from jax import lax
from jax.sharding import PartitionSpec as P

epsilon = 1e-06


def with_halo(cells, sides, width):
    for axis, dim in sides:
        count = lax.axis_size(axis)
        ends = count - 1
        head = lax.slice_in_dim(cells, 0, width, axis=dim)
        tail = lax.slice_in_dim(cells, cells.shape[dim] - width, cells.shape[dim], axis=dim)
        cells = jnp.concatenate(
            [
                lax.ppermute(tail, axis, [(i, (i + 1) % count) for i in range(ends)]),
                cells,
                lax.ppermute(head, axis, [((i + 1) % count, i) for i in range(ends)]),
            ],
            axis=dim,
        )
    return cells


def per_device(
    out_grad,
    residual,
    routes,
    route_weights,
    w_gate,
    w_up,
    w_down,
    out_gate,
    in_gate,
    conv_input,
    conv_out,
    conv_taps,
    w_out,
):
    tok_rows = out_grad.shape[0]
    features = out_grad.shape[1]
    top_count = routes.shape[1]
    slices = lax.axis_size("sp")
    experts = slices // 2
    capacity = 5 * tok_rows // slices
    n_assign = tok_rows * top_count
    resid_f32 = residual.astype(jnp.float32)
    inv_rms = lax.rsqrt(jnp.mean(resid_f32 * resid_f32, axis=-1, keepdims=True) + epsilon)
    unit_rows = resid_f32 * inv_rms
    normed = unit_rows.astype(jnp.bfloat16)
    weighted = (
        (route_weights[:, :, None] * out_grad.astype(jnp.float32)[:, None, :])
        .astype(jnp.bfloat16)
        .reshape(n_assign, features)
    )
    flat_routes = routes.reshape(-1)
    onehot = (flat_routes[:, None] == jnp.arange(experts, dtype=jnp.int32)[None, :]).astype(
        jnp.int32
    )
    slot_rank = jnp.sum((jnp.cumsum(onehot, axis=0) - onehot) * onehot, axis=1)
    slot_index = flat_routes * capacity + slot_rank
    slot_table = (
        jnp.full((experts * capacity,), n_assign, jnp.int32)
        .at[slot_index]
        .set(jnp.arange(n_assign, dtype=jnp.int32))
    )
    filled = slot_table < n_assign
    safe_index = jnp.where(filled, slot_table, 0)
    send_rows = jnp.where(
        filled[:, None], normed[safe_index // top_count], jnp.zeros((), jnp.bfloat16)
    )
    send_grads = jnp.where(filled[:, None], weighted[safe_index], jnp.zeros((), jnp.bfloat16))
    outgoing = jnp.stack([send_rows, send_grads])
    doubled = jnp.repeat(outgoing.reshape(2, experts, capacity, features), 2, axis=1)
    arrived = lax.all_to_all(doubled, "sp", split_axis=1, concat_axis=1, tiled=True)
    expert_rows = arrived[0].reshape(slices * capacity, features)
    expert_grads = arrived[1].reshape(slices * capacity, features)
    gate_local = w_gate[0]
    up_local = w_up[0]
    down_local = w_down[0]
    pre_gate = jnp.dot(expert_rows, gate_local, preferred_element_type=jnp.float32)
    pre_up = jnp.dot(expert_rows, up_local, preferred_element_type=jnp.float32)
    sigmoid_gate = jax.nn.sigmoid(pre_gate)
    activated = pre_gate * sigmoid_gate
    hidden = (activated * pre_up).astype(jnp.bfloat16)
    d_hidden = lax.dot_general(
        expert_grads, down_local, (((1,), (1,)), ((), ())), preferred_element_type=jnp.float32
    )
    grad_down = lax.dot_general(
        hidden, expert_grads, (((0,), (0,)), ((), ())), preferred_element_type=jnp.float32
    ).astype(jnp.bfloat16)
    d_gate = (d_hidden * pre_up * sigmoid_gate * (1.0 + pre_gate * (1.0 - sigmoid_gate))).astype(
        jnp.bfloat16
    )
    d_up = (d_hidden * activated).astype(jnp.bfloat16)
    grad_up = lax.dot_general(
        expert_rows, d_up, (((0,), (0,)), ((), ())), preferred_element_type=jnp.float32
    ).astype(jnp.bfloat16)
    partial_value = lax.dot_general(
        d_gate, gate_local, (((1,), (1,)), ((), ())), preferred_element_type=jnp.float32
    )
    partial_value = partial_value + lax.dot_general(
        d_up, up_local, (((1,), (1,)), ((), ())), preferred_element_type=jnp.float32
    )
    partial_value = partial_value.astype(jnp.bfloat16).reshape(slices, capacity, features)
    summed = lax.psum_scatter(partial_value, "tp", scatter_dimension=2, tiled=True).astype(
        jnp.float32
    )
    returned = lax.all_to_all(
        summed.astype(jnp.bfloat16), "sp", split_axis=0, concat_axis=0, tiled=True
    )
    columns = returned.shape[2]
    flat_back = returned.reshape(slices * capacity, columns)
    first_index = 2 * flat_routes * capacity + slot_rank
    contrib = flat_back[first_index].astype(jnp.float32) + flat_back[first_index + capacity].astype(
        jnp.float32
    )
    d_normed = jnp.sum(contrib.reshape(tok_rows, top_count, columns), axis=1)
    col_start = lax.axis_index("tp") * columns
    unit_part = lax.dynamic_slice_in_dim(unit_rows, col_start, columns, 1)
    grad_part = lax.dynamic_slice_in_dim(out_grad, col_start, columns, 1).astype(jnp.float32)
    row_dots = lax.psum(jnp.sum(unit_part * d_normed, axis=-1), "tp")
    row_mean = row_dots[:, None] / features
    resid_part = (grad_part + inv_rms * (d_normed - unit_part * row_mean)).astype(jnp.bfloat16)
    grad_resid = lax.all_gather(resid_part, "tp", axis=1, tiled=True)
    d_mix = lax.dot_general(
        grad_resid, w_out, (((1,), (1,)), ((), ())), preferred_element_type=jnp.float32
    )
    conv_f32 = conv_out.astype(jnp.float32)
    gate_f32 = out_gate.astype(jnp.float32)
    grad_out_gate = (d_mix * conv_f32).astype(jnp.bfloat16)
    d_conv = d_mix * gate_f32
    padded = with_halo(d_conv.astype(jnp.bfloat16), (("sp", 0),), 1).astype(d_conv.dtype)
    d_inner = conv_taps[0] * padded[2:] + conv_taps[1] * padded[1:-1] + conv_taps[2] * padded[:-2]
    grad_in_gate = (d_inner * conv_input.astype(jnp.float32)).astype(jnp.bfloat16)
    grad_conv_input = (d_inner * in_gate.astype(jnp.float32)).astype(jnp.bfloat16)
    mixed = (gate_f32 * conv_f32).astype(jnp.bfloat16)
    grad_w_out = lax.psum_scatter(
        lax.dot_general(
            grad_resid, mixed, (((0,), (0,)), ((), ())), preferred_element_type=jnp.float32
        ),
        "sp",
        scatter_dimension=0,
        tiled=True,
    )
    return (
        grad_resid,
        grad_up[None],
        grad_down[None],
        grad_out_gate,
        grad_in_gate,
        grad_conv_input,
        grad_w_out,
    )


def solution(mesh):
    in_specs = (
        P("sp", None),
        P("sp", None),
        P("sp", None),
        P("sp", None),
        P("sp", None, "tp"),
        P("sp", None, "tp"),
        P("sp", "tp", None),
        P("sp", "tp"),
        P("sp", "tp"),
        P("sp", "tp"),
        P("sp", "tp"),
        P(None, "tp"),
        P("tp", None),
    )
    out_specs = (
        P("sp", None),
        P("sp", None, "tp"),
        P("sp", "tp", None),
        P("sp", "tp"),
        P("sp", "tp"),
        P("sp", "tp"),
        P("sp", "tp"),
    )
    return jax.shard_map(
        per_device, mesh=mesh, in_specs=in_specs, out_specs=out_specs, check_vma=False
    )
```

profile of v0, /device:TPU:0, one launch (start us, length us, event | category | flops | bytes accessed | tf_op | source)
XLA Modules:
  0.0 325.2 jit_solution(2175908563554208962)
XLA Ops:
  15.1 2.2 convert_multiply_fusion
  17.2 2.4 mul.164
  19.6 3.6 %mul.165 = f32[256,2048]{1,0:T(8,128)} reshape(f32[128,2,2048]{2,1,0:T(2,128)} %mul.164) | data formatting | bytes 4194304 | tf_op jit(solution)/shard_map/mul | solution.py:53
  23.3 3.0 gather_fusion
  26.3 1.8 multiply_convert_fusion
  28.1 3.0 gather_fusion.1
  31.1 1.9 broadcast_select_fusion.1
  34.2 122.8 %all_to_all.10 = bf16[2,8,80,2048]{3,2,0,1:T(8,128)(2,1)S(1)} all-to-all(bf16[2,8,80,2048]{3,2,0,1:T(8,128)(2,1)S(1)} %bitcast.65), channel_id=1, replica_groups=mesh['sp'=8,'tp'=4] {'sp'}, dimensions={1} | all-to-all | bytes 10485760 | tf_op jit(solution)/shard_map/all_to_all | solution.py:76
  162.7 1.7 multiply_convert_fusion.2
  164.4 1.9 fusion.2
  166.3 3.0 add_convert_fusion
  169.4 33.5 %reduce-scatter.3.cloned.1.call-done = bf16[8,80,512]{2,1,0:T(8,128)(2,1)} async-done(((bf16[8,80,2048]{2,1,0:T(8,128)(2,1)}), bf16[8,80,512]{2,1,0:T(8,128)(2,1)}) %reduce-scatter.3.cloned.1.call-update) | async-done | bytes 655376 | tf_op jit(solution)/shard_map/reduce_scatter | solution.py:107
  202.9 5.5 %all-to-all-start.1 = ((bf16[8,80,512]{2,1,0:T(8,128)(2,1)}), bf16[8,80,512]{2,1,0:T(8,128)(2,1)S(1)}, u32[]{:S(2)}, u32[]{:S(2)}) async-start(bf16[8,80,512]{2,1,0:T(8,128)(2,1)} %reduce-scatter.3.cloned.1.call-done), calls=%async_computation.2 | async-start | bytes 1310720 | tf_op jit(solution)/shard_map/all_to_all | solution.py:110
  208.5 17.1 %all-to-all-done.1 = bf16[8,80,512]{2,1,0:T(8,128)(2,1)S(1)} async-done(((bf16[8,80,512]{2,1,0:T(8,128)(2,1)}), bf16[8,80,512]{2,1,0:T(8,128)(2,1)S(1)}, u32[]{:S(2)}, u32[]{:S(2)}) %all-to-all-start.1) | async-done | bytes 655392 | tf_op jit(solution)/shard_map/all_to_all | solution.py:110
  226.7 1.9 gather_fusion.2
  228.6 1.9 convert_add_fusion
  230.5 2.2 add.145
  234.5 5.9 %psum.7 = f32[128]{0:T(128)S(1)} all-reduce(f32[128]{0:T(128)S(1)} %multiply_reduce_fusion), channel_id=1, replica_groups=mesh['sp'=8,'tp'=4] {'tp'}, use_global_device_ids=true, to_apply=%region_8.9 | all-reduce | flops 128 | bytes 1024 | tf_op jit(solution)/shard_map/psum | solution.py:123
  241.4 6.8 %all_gather.3 = bf16[128,2048]{1,0:T(8,128)(2,1)S(1)} all-gather(bf16[128,512]{1,0:T(8,128)(2,1)S(1)} %add_convert_fusion.1), channel_id=1, replica_groups=mesh['sp'=8,'tp'=4] {'tp'}, dimensions={1}, use_global_device_ids=true | all-gather | bytes 655360 | tf_op jit(solution)/shard_map/all_gather | solution.py:126
  248.2 1.8 fusion.20
  250.1 5.9 %fusion.1 = bf16[1,512,2048]{2,1,0:T(8,128)(2,1)} fusion(bf16[640,2048]{1,0:T(8,128)(2,1)} %bitcast.73, f32[640,512]{1,0:T(8,128)} %copy-done.17, f32[640,512]{1,0:T(8,128)} %copy-done.16), kind=kOutput, calls=%fused_computation.9 | convolution fusion | flops 1345191936 | bytes 7340032 | tf_op jit(solution)/shard_map/dot_general | solution.py:90
  257.1 3.4 %collective-permute-start = (bf16[1,256]{1,0:T(2,128)(2,1)S(1)}, bf16[1,256]{1,0:T(2,128)(2,1)S(1)}, u32[]{:S(2)}, u32[]{:S(2)}) collective-permute-start(bf16[1,256]{1,0:T(2,128)(2,1)S(1)} %get-tuple-element.15), channel_id=1, source_target_pairs={{0,4},{4,8},{8,12},{12,16},{16,20},{20,24},{24,28},{1,5},{5,9},{9,... | collective-permute-start | bytes 1544 | tf_op jit(solution)/shard_map/ppermute | solution.py:17
  262.0 3.2 fusion
  267.5 50.1 %reduce-scatter.5.cloned.1.call-done = f32[256,256]{1,0:T(8,128)} async-done(((f32[2048,256]{1,0:T(8,128)}), f32[256,256]{1,0:T(8,128)}) %reduce-scatter.5.cloned.1.call-update) | async-done | bytes 262160 | tf_op jit(solution)/shard_map/reduce_scatter | solution.py:139
  (91 shorter events, 24.4 us)
Async XLA Ops:
  7.2 150.3 %copy-start = (bf16[1,2048,512]{2,1,0:T(8,128)(2,1)S(1)}, bf16[1,2048,512]{2,1,0:T(8,128)(2,1)}, u32[]{:S(2)}) copy-start(bf16[1,2048,512]{2,1,0:T(8,128)(2,1)} %param.17) | copy-start | bytes 6291460
  7.2 10.1 %copy-start.7 = (bf16[128,2048]{1,0:T(8,128)(2,1)S(1)}, bf16[128,2048]{1,0:T(8,128)(2,1)}, u32[]{:S(2)}) copy-start(bf16[128,2048]{1,0:T(8,128)(2,1)} %param.13) | copy-start | bytes 1572868
  7.2 195.7 %reduce-scatter.3.cloned.1.call-start = ((), (), s32[]{:S(2)}) async-start(), calls=%async_computation.4 | async-start | bytes 3276800 | tf_op jit(solution)/shard_map/reduce_scatter | solution.py:107
  157.4 1.6 copy-start.1
  157.4 4.7 %copy-start.3 = (bf16[1,8,80,2048]{3,2,0,1:T(8,128)(2,1)}, bf16[1,8,80,2048]{3,2,0,1:T(8,128)(2,1)S(1)}, u32[]{:S(2)}) copy-start(bf16[1,8,80,2048]{3,2,0,1:T(8,128)(2,1)S(1)} %get-tuple-element.9) | copy-start | bytes 7864324
  157.4 3.2 copy-start.5
  160.6 3.8 %copy-start.16 = (f32[640,512]{1,0:T(8,128)}, f32[640,512]{1,0:T(8,128)S(1)}, u32[]{:S(2)}) copy-start(f32[640,512]{1,0:T(8,128)S(1)} %fusion.4) | copy-start | bytes 3932164
  160.6 2.1 copy-start.15
  162.1 2.3 copy-start.17
  164.4 2.0 copy-start.8
  202.9 22.7 %all-to-all-start.1 = ((bf16[8,80,512]{2,1,0:T(8,128)(2,1)}), bf16[8,80,512]{2,1,0:T(8,128)(2,1)S(1)}, u32[]{:S(2)}, u32[]{:S(2)}) async-start(bf16[8,80,512]{2,1,0:T(8,128)(2,1)} %reduce-scatter.3.cloned.1.call-done), calls=%async_computation.2 | async-start | bytes 1310720 | tf_op jit(solution)/shard_map/all_to_all | solution.py:110
  208.5 109.1 %reduce-scatter.5.cloned.1.call-start = ((), (), s32[]{:S(2)}) async-start(), calls=%async_computation.5 | async-start | bytes 2359296 | tf_op jit(solution)/shard_map/reduce_scatter | solution.py:139
  228.6 5.8 %copy-start.4 = (f32[128,2048]{1,0:T(8,128)S(1)}, f32[128,2048]{1,0:T(8,128)}, u32[]{:S(2)}) copy-start(f32[128,2048]{1,0:T(8,128)} %get-tuple-element.11) | copy-start | bytes 3145732
  230.5 17.7 %copy-start.10 = (bf16[128,256]{1,0:T(8,128)(2,1)S(1)}, bf16[128,256]{1,0:T(8,128)(2,1)}, u32[]{:S(2)}) copy-start(bf16[128,256]{1,0:T(8,128)(2,1)} %param.20) | copy-start | bytes 196612
  230.5 17.7 %copy-start.11 = (bf16[128,256]{1,0:T(8,128)(2,1)S(1)}, bf16[128,256]{1,0:T(8,128)(2,1)}, u32[]{:S(2)}) copy-start(bf16[128,256]{1,0:T(8,128)(2,1)} %param.23) | copy-start | bytes 196612
  248.2 1.8 copy-start.14
  250.1 5.9 %copy-start.6 = (bf16[256,2048]{1,0:T(8,128)(2,1)S(1)}, bf16[256,2048]{1,0:T(8,128)(2,1)}, u32[]{:S(2)}) copy-start(bf16[256,2048]{1,0:T(8,128)(2,1)} %param.25) | copy-start | bytes 3145732
  250.1 11.9 %copy-start.2 = (bf16[1,8,80,2048]{3,2,0,1:T(8,128)(2,1)S(1)}, bf16[1,8,80,2048]{3,2,0,1:T(8,128)(2,1)}, u32[]{:S(2)}) copy-start(bf16[1,8,80,2048]{3,2,0,1:T(8,128)(2,1)} %copy-done.1) | copy-start | bytes 7864324
  250.1 11.9 %copy-start.9 = (bf16[640,512]{1,0:T(8,128)(2,1)S(1)}, bf16[640,512]{1,0:T(8,128)(2,1)}, u32[]{:S(2)}) copy-start(bf16[640,512]{1,0:T(8,128)(2,1)} %copy-done.8) | copy-start | bytes 1966084
  257.1 8.0 %collective-permute-start = (bf16[1,256]{1,0:T(2,128)(2,1)S(1)}, bf16[1,256]{1,0:T(2,128)(2,1)S(1)}, u32[]{:S(2)}, u32[]{:S(2)}) collective-permute-start(bf16[1,256]{1,0:T(2,128)(2,1)S(1)} %get-tuple-element.15), channel_id=1, source_target_pairs={{0,4},{4,8},{8,12},{12,16},{16,20},{20,24},{24,28},{1,5},{5,9},{9,... | collective-permute-start | bytes 1544 | tf_op jit(solution)/shard_map/ppermute | solution.py:17
  260.5 5.6 %copy-start.12 = (bf16[128,256]{1,0:T(8,128)(2,1)S(1)}, bf16[128,256]{1,0:T(8,128)(2,1)}, u32[]{:S(2)}) copy-start(bf16[128,256]{1,0:T(8,128)(2,1)} %param.21) | copy-start | bytes 196612
  260.5 6.3 %copy-start.13 = (bf16[128,256]{1,0:T(8,128)(2,1)S(1)}, bf16[128,256]{1,0:T(8,128)(2,1)}, u32[]{:S(2)}) copy-start(bf16[128,256]{1,0:T(8,128)(2,1)} %param.22) | copy-start | bytes 196612
  260.5 5.6 %collective-permute-start.1 = (bf16[1,256]{1,0:T(2,128)(2,1)S(1)}, bf16[1,256]{1,0:T(2,128)(2,1)S(1)}, u32[]{:S(2)}, u32[]{:S(2)}) collective-permute-start(bf16[1,256]{1,0:T(2,128)(2,1)S(1)} %get-tuple-element.16), channel_id=1, source_target_pairs={{4,0},{8,4},{12,8},{16,12},{20,16},{24,20},{28,24},{5,1},{9,5},{13... | collective-permute-start | bytes 1544 | tf_op jit(solution)/shard_map/ppermute | solution.py:19
Sparse Core Ops, SparseCore 0:
  169.5 33.3 reduce-scatter.2
  250.2 67.3 reduce-scatter.4
where the time goes:
time: 326 us; the launch traced here: 325 us
  blocking collectives  135 us (41%)
  waiting for transfers between devices  102 us (31%)
  local copies, waits for them, and re-layouts  25.9 us (8%)
  matrix products  21.7 us (7%)
  other arithmetic  15.7 us (5%)
  between operations  14.4 us (4%)
  starting transfers between devices  10.4 us (3%)
    all_to_all x1, blocking collectives, per_device(): lax.all_to_all(doubled, 'sp', split_axis=1, concat_axis=1, tiled=True)  123 us
    reduce_scatter x1, waiting for transfers between devices, per_device(): lax.psum_scatter(lax.dot_general(grad_resid, mixed, (((0,), (0,)), ((), (...  50.1 us
    reduce_scatter x1, waiting for transfers between devices, per_device(): lax.psum_scatter(partial_value, 'tp', scatter_dimension=2, tiled=True)  33.5 us
    all_to_all x1, waiting for transfers between devices, per_device(): lax.all_to_all(summed.astype(jnp.bfloat16), 'sp', split_axis=0, concat_ax...  17.1 us
    all_gather x1, blocking collectives, per_device(): grad_resid = lax.all_gather(resid_part, 'tp', axis=1, tiled=True)  6.76 us
  transfers between devices with their start and end apart: 5, of which 4 were waited for; matrix products, arithmetic and copies ran while one was open for 4% of the time, Pallas kernels for 0%

commit v1 on v0

v1 whole, which is shorter than its diff:
```python
import functools

import jax
import jax.numpy as jnp
from jax import lax
from jax.experimental import pallas as pl
from jax.experimental.pallas import tpu as pltpu
from jax.sharding import Mesh
from jax.sharding import PartitionSpec as P

epsilon = 1e-06
F32 = jnp.float32
BF16 = jnp.bfloat16


def swap(value, axis):
    return lax.ppermute(value, axis, [(0, 1), (1, 0)])


def swap_both(value):
    return lax.ppermute(value, ("j", "x"), [(i, 3 - i) for i in range(4)])


def shifted(value, step):
    count = lax.axis_size("e")
    return lax.ppermute(value, "e", [(i, (i + step) % count) for i in range(count)])


def dot(a, b, ca, cb):
    return lax.dot_general(a, b, (((ca,), (cb,)), ((), ())), preferred_element_type=F32)


def prepare(experts, cap, quarter, index_ref, routes_ref, weights_ref, resid_ref, grad_ref, *outs):
    sends, sel_ref = outs[:-1], outs[-1]
    tokens = resid_ref.shape[0]
    mine, column = index_ref[0], index_ref[1]
    resid = resid_ref[...].astype(F32)
    inv_rms = lax.rsqrt(jnp.mean(resid * resid, axis=-1, keepdims=True) + epsilon)
    cols = pl.ds(pl.multiple_of(column * quarter, quarter), quarter)
    normed = (resid_ref[:, cols].astype(F32) * inv_rms).astype(BF16)
    grad = grad_ref[:, cols]
    first, second = routes_ref[0:1, :], routes_ref[1:2, :]
    first = jnp.where(first >= mine, first - mine, first - mine + experts)
    second = jnp.where(second >= mine, second - mine, second - mine + experts)
    ids = lax.broadcasted_iota(jnp.int32, (experts, tokens), 0)
    in_first, in_second = ids == first, ids == second
    member = jnp.where(in_first | in_second, 1.0, 0.0)
    before = jnp.where(
        lax.broadcasted_iota(jnp.int32, (tokens, tokens), 0)
        < lax.broadcasted_iota(jnp.int32, (tokens, tokens), 1),
        1.0,
        0.0,
    )
    rank = dot(member.astype(BF16), before.astype(BF16), 1, 0)
    rank_first = jnp.sum(jnp.where(in_first, rank, 0.0), axis=0, keepdims=True).astype(jnp.int32)
    rank_second = jnp.sum(jnp.where(in_second, rank, 0.0), axis=0, keepdims=True).astype(jnp.int32)
    slot_first = first * cap + rank_first
    slot_second = second * cap + rank_second
    for step in range(experts):
        slots = lax.broadcasted_iota(jnp.int32, (cap, tokens), 0) + step * cap
        hit_first, hit_second = slots == slot_first, slots == slot_second
        pick = jnp.where(hit_first | hit_second, 1.0, 0.0).astype(BF16)
        share = jnp.where(hit_first, weights_ref[0:1, :], 0.0) + jnp.where(
            hit_second, weights_ref[1:2, :], 0.0
        )
        share = jnp.sum(share, axis=1, keepdims=True)
        sel_ref[step] = pick
        sends[step][0] = dot(pick, normed, 1, 0).astype(BF16)
        sends[step][1] = (share * dot(pick, grad, 1, 0)).astype(BF16)


def relative(value, axis, place):
    width = value.shape[axis] // 4
    parts = []
    for dc in range(2):
        for dx in range(2):
            parts.append(
                lax.dynamic_slice_in_dim(value, (place ^ (2 * dx + dc)) * width, width, axis)
            )
    return parts


def absolute(value, axis, place):
    width = value.shape[axis] // 4
    parts = []
    for q in range(4):
        r = place ^ q
        parts.append(
            lax.dynamic_slice_in_dim(value, ((r & 1) * 2 + (r >> 1)) * width, width, axis)
        )
    return jnp.concatenate(parts, axis=axis)


def per_device(
    out_grad,
    residual,
    routes,
    route_weights,
    w_gate,
    w_up,
    w_down,
    out_gate,
    in_gate,
    conv_input,
    conv_out,
    conv_taps,
    w_out,
):
    tokens, features = out_grad.shape
    experts = lax.axis_size("e")
    slices = 2 * experts
    cap = 5 * tokens // slices
    quarter = features // 4
    mine, half, core = lax.axis_index("e"), lax.axis_index("j"), lax.axis_index("c")
    place = 2 * lax.axis_index("x") + core

    outs = pl.pallas_call(
        functools.partial(prepare, experts, cap, quarter),
        out_shape=[jax.ShapeDtypeStruct((2, cap, quarter), BF16)] * experts
        + [jax.ShapeDtypeStruct((experts, cap, tokens), BF16)],
        in_specs=[pl.BlockSpec(memory_space=pltpu.SMEM)]
        + [pl.BlockSpec(memory_space=pltpu.VMEM)] * 4,
        out_specs=[pl.BlockSpec(memory_space=pltpu.VMEM)] * (experts + 1),
    )(
        jnp.stack([mine, place]).astype(jnp.int32),
        routes.T,
        route_weights.T,
        residual,
        out_grad,
    )
    sends, sel = outs[:-1], outs[-1]
    came = [sends[0]] + [shifted(sends[s], s) for s in range(1, experts)]
    rows_z = jnp.concatenate([b[0] for b in came], axis=0)
    grads_z = jnp.concatenate([b[1] for b in came], axis=0)
    count = rows_z.shape[0]

    rows_x, grads_y = swap(rows_z, "x"), swap(grads_z, "j")
    rows_pair = jnp.stack([rows_z, rows_x])
    grads_pair = jnp.stack([grads_z, grads_y])
    rows_four = jnp.stack([rows_pair, swap(rows_pair, "j")])
    grads_four = jnp.stack([grads_pair, swap(grads_pair, "x")])
    rows_sib, grads_sib = swap(rows_four, "c"), swap(grads_four, "c")
    rows = jnp.concatenate(
        [rows_four[:, 0], rows_four[:, 1], rows_sib[:, 0], rows_sib[:, 1]], axis=-1
    ).reshape(2 * count, features)
    grads = jnp.concatenate(
        [grads_four[0], grads_four[1], grads_sib[0], grads_sib[1]], axis=-1
    ).reshape(2 * count, features)

    gate_w = jnp.concatenate(relative(w_gate[0], 0, place), axis=0)
    up_w = jnp.concatenate(relative(w_up[0], 0, place), axis=0)
    down_w = jnp.concatenate(relative(w_down[0], 1, place), axis=1)
    pre_gate = dot(rows, gate_w, 1, 0)
    pre_up = dot(rows, up_w, 1, 0)
    sigmoid_gate = jax.nn.sigmoid(pre_gate)
    activated = pre_gate * sigmoid_gate
    hidden = (activated * pre_up).astype(BF16)
    d_hidden = dot(grads, down_w, 1, 1)
    d_gate = (d_hidden * pre_up * sigmoid_gate * (1.0 + pre_gate * (1.0 - sigmoid_gate))).astype(
        BF16
    )
    d_up = (d_hidden * activated).astype(BF16)

    split = features // 2
    away = dot(d_gate, gate_w[split:], 1, 1) + dot(d_up, up_w[split:], 1, 1)
    other = swap(away.astype(BF16), "c")
    kept = dot(d_gate, gate_w[:split], 1, 1) + dot(d_up, up_w[:split], 1, 1)
    total = (kept + other.astype(F32)).astype(BF16)
    block = lambda dj, dx: total[dj * count : (dj + 1) * count, dx * quarter : (dx + 1) * quarter]
    summed = (
        block(0, 0).astype(F32)
        + swap(block(0, 1), "x").astype(F32)
        + swap(block(1, 0), "j").astype(F32)
        + swap_both(block(1, 1)).astype(F32)
    ).astype(BF16)
    back = [summed[:cap]] + [
        shifted(summed[s * cap : (s + 1) * cap], -s) for s in range(1, experts)
    ]

    grad_up = absolute(dot(rows, d_up, 0, 0).astype(BF16), 0, place)
    grad_down = absolute(dot(hidden, grads, 0, 0).astype(BF16), 1, place)

    d_part = dot(
        sel.reshape(experts * cap, tokens), jnp.concatenate(back, axis=0), 0, 0
    ).astype(BF16)
    d_normed = lax.all_gather(d_part, ("x", "c"), axis=1, tiled=True).astype(F32)
    resid_f32 = residual.astype(F32)
    inv_rms = lax.rsqrt(jnp.mean(resid_f32 * resid_f32, axis=-1, keepdims=True) + epsilon)
    unit_rows = resid_f32 * inv_rms
    row_mean = jnp.mean(unit_rows * d_normed, axis=-1, keepdims=True)
    grad_resid = (out_grad.astype(F32) + inv_rms * (d_normed - unit_rows * row_mean)).astype(BF16)

    conv_f32 = conv_out.astype(F32)
    gate_f32 = out_gate.astype(F32)
    mixed = (gate_f32 * conv_f32).astype(BF16)
    mixed_pair = jnp.stack([mixed, swap(mixed, "j")])
    mixed_rel = jnp.stack([mixed_pair] + [shifted(mixed_pair, s) for s in range(1, experts)])
    channels = mixed.shape[1]
    mixed_rel = mixed_rel.reshape(slices, tokens, channels)
    mixed_all = jnp.concatenate(
        [
            lax.dynamic_slice_in_dim(
                mixed_rel, lax.rem(mine - e + experts, experts) * 2 + (half ^ j), 1, 0
            )
            for e in range(experts)
            for j in range(2)
        ],
        axis=0,
    )
    part = tokens // 2
    ordered = [
        lax.dynamic_slice_in_dim(mixed_all, (core ^ d) * part, part, 1).reshape(-1, channels)
        for d in range(2)
    ]
    width = features // slices
    mine_rows = lax.dynamic_slice_in_dim(grad_resid, core * part, part, 0)
    blocks = jnp.transpose(mine_rows.reshape(part, slices, width), (1, 0, 2))
    got = lax.all_to_all(blocks, ("e", "j"), 0, 0, tiled=True).reshape(slices * part, width)
    got_sib = swap(got, "c")
    grad_w_out = dot(got, ordered[0], 0, 0) + dot(got_sib, ordered[1], 0, 0)

    d_mix = dot(grad_resid, w_out, 1, 1)
    grad_out_gate = (d_mix * conv_f32).astype(BF16)
    d_conv = d_mix * gate_f32
    edge = d_conv.astype(BF16)
    ends = slices - 1
    above = lax.ppermute(edge[-1:], ("e", "j"), [(i, i + 1) for i in range(ends)]).astype(F32)
    below = lax.ppermute(edge[:1], ("e", "j"), [(i + 1, i) for i in range(ends)]).astype(F32)
    later = jnp.concatenate([d_conv[1:], below], axis=0)
    earlier = jnp.concatenate([above, d_conv[:-1]], axis=0)
    d_inner = conv_taps[0] * later + conv_taps[1] * d_conv + conv_taps[2] * earlier
    grad_in_gate = (d_inner * conv_input.astype(F32)).astype(BF16)
    grad_conv_input = (d_inner * in_gate.astype(F32)).astype(BF16)
    return (
        grad_resid,
        grad_up[None],
        grad_down[None],
        grad_out_gate,
        grad_in_gate,
        grad_conv_input,
        grad_w_out,
    )


def solution(mesh):
    slices, blocks = mesh.shape["sp"], mesh.shape["tp"]
    grid = mesh.devices.reshape(slices // 2, 2, blocks // 2, 2)
    inner = Mesh(grid, ("e", "j", "x", "c"))
    sp, tp = ("e", "j"), ("x", "c")
    in_specs = (
        P(sp, None),
        P(sp, None),
        P(sp, None),
        P(sp, None),
        P(sp, None, tp),
        P(sp, None, tp),
        P(sp, tp, None),
        P(sp, tp),
        P(sp, tp),
        P(sp, tp),
        P(sp, tp),
        P(None, tp),
        P(tp, None),
    )
    out_specs = (
        P(sp, None),
        P(sp, None, tp),
        P(sp, tp, None),
        P(sp, tp),
        P(sp, tp),
        P(sp, tp),
        P(sp, tp),
    )
    return jax.shard_map(
        per_device, mesh=inner, in_specs=in_specs, out_specs=out_specs, check_vma=False
    )
```

time: 326 us -> 156 us (0.48)
  blocking collectives: 135 us -> 7.3 us
  starting transfers between devices: 10.4 us -> 42.2 us
  waiting for transfers between devices: 102 us -> 70.7 us
  local copies, waits for them, and re-layouts: 25.9 us -> 6.2 us
  between operations: 14.4 us -> 1.29 us
  other arithmetic: 15.7 us -> 8.85 us
  matrix products: 21.7 us -> 16.9 us
    all_to_all x1 -> x0, blocking collectives: 123 us -> none  [per_device(): lax.all_to_all(doubled, 'sp', split_axis=1, concat_axis=1, tiled=True)]
    reduce_scatter x2 -> x0, waiting for transfers between devices: 83.6 us -> none  [the longest x1 50.1 us: per_device(): lax.psum_scatter(lax.dot_general(grad_resid, mixed, (((0,), (0,)), ((), (...]
    ppermute x2 -> x23, waiting for transfers between devices: 0.98 us -> 70.7 us  [the longest x11 48 us: swap(): return lax.ppermute(value, axis, [(0, 1), (1, 0)])]
    ppermute x2 -> x23, starting transfers between devices: 4.78 us -> 38.3 us  [the longest x9 20 us: shifted(): lax.ppermute(value, 'e', [(i, (i + step) % count) for i in range(count)])]
    all_to_all x1, waiting for transfers between devices: 17.1 us -> 0.01 us  [per_device(): lax.all_to_all(blocks, ('e', 'j'), 0, 0, tiled=True)]
    gather x4 -> x0, local copies, waits for them, and re-layouts: 9.04 us -> none  [the longest x1 3.02 us: per_device(): weighted[safe_index]]
    mul x7 -> x0, local copies, waits for them, and re-layouts: 6.66 us -> none  [the longest x3 6.16 us: per_device(): route_weights[:, :, None] * out_grad.astype(jnp.float32)[:, None, :]]
    psum x1 -> x0, blocking collectives: 5.92 us -> none  [per_device(): row_dots = lax.psum(jnp.sum(unit_part * d_normed, axis=-1), 'tp')]
  transfers between devices with their start and end apart: 5 -> 24, of which waited for: 4 -> 14; matrix products, arithmetic and copies ran while one was open for 4% -> 15% of each run, Pallas kernels for 0% -> 0%
where the time goes in v1:
time: 156 us
  waiting for transfers between devices  70.7 us (45%)
  starting transfers between devices  42.2 us (27%)
  matrix products  16.9 us (11%)
  other arithmetic  8.85 us (6%)
  blocking collectives  7.3 us (5%)
  local copies, waits for them, and re-layouts  6.2 us (4%)
  Pallas kernels  2.49 us (2%)
    ppermute x11, waiting for transfers between devices, swap(): return lax.ppermute(value, axis, [(0, 1), (1, 0)])  48 us
    ppermute x9, starting transfers between devices, shifted(): lax.ppermute(value, 'e', [(i, (i + step) % count) for i in range(count)])  20 us
    dot_general x13, matrix products, dot(): lax.dot_general(a, b, (((ca,), (cb,)), ((), ())), preferred_element_type=...  16.9 us
    ppermute x9, waiting for transfers between devices, shifted(): lax.ppermute(value, 'e', [(i, (i + step) % count) for i in range(count)])  15.5 us
    ppermute x11, starting transfers between devices, swap(): return lax.ppermute(value, axis, [(0, 1), (1, 0)])  11 us
    all_gather x1, blocking collectives, per_device(): lax.all_gather(d_part, ('x', 'c'), axis=1, tiled=True).astype(F32)  7.3 us
    ppermute x1, waiting for transfers between devices, swap_both(): return lax.ppermute(value, ('j', 'x'), [(i, 3 - i) for i in range(4)])  7.15 us
    ppermute x1, starting transfers between devices, per_device(): lax.ppermute(edge[-1:], ('e', 'j'), [(i, i + 1) for i in range(ends)])  4.55 us
  transfers between devices with their start and end apart: 24, of which 14 were waited for; matrix products, arithmetic and copies ran while one was open for 15% of the time, Pallas kernels for 0%

profile of v1, /device:TPU:0, one launch (start us, length us, event | category | flops | bytes accessed | tf_op | source)
XLA Modules:
  0.0 155.8 jit_solution(7727151132311310104)
XLA Ops:
  1.2 2.5 %shard_map.180 = (bf16[2,80,512]{2,1,0:T(8,128)(2,1)}, bf16[2,80,512]{2,1,0:T(8,128)(2,1)}, bf16[2,80,512]{2,1,0:T(8,128)(2,1)}, bf16[2,80,512]{2,1,0:T(8,128)(2,1)}, bf16[4,80,128]{2,1,0:T(8,128)(2,1)}) custom-call(s32[2]{0:T(128)} %pad_add_fusion.index_ref, s32[2,128]{1,0:T(2,128)} %bitcast.145, f32[2,128]{1,0:T(2,128)} %bitcast.146, ...), custom_call_target="tpu_custom_call" | custom-call | tf_op jit(solution)/shard_map/pallas_call | solution.py:117
  3.7 3.1 %collective-permute-start = (bf16[2,80,512]{2,1,0:T(8,128)(2,1)}, bf16[2,80,512]{2,1,0:T(8,128)(2,1)S(1)}, u32[]{:S(2)}, u32[]{:S(2)}) collective-permute-start(bf16[2,80,512]{2,1,0:T(8,128)(2,1)} %get-tuple-element.14), channel_id=1, source_target_pairs={{0,8},{8,16},{16,24},{24,0},{1,9},{9,17},{17,25},{25,1},{2,10},{10... | collective-permute-start | bytes 491528 | tf_op jit(solution)/shard_map/ppermute | solution.py:26
  6.8 2.6 %collective-permute-start.1 = (bf16[2,80,512]{2,1,0:T(8,128)(2,1)}, bf16[2,80,512]{2,1,0:T(8,128)(2,1)S(1)}, u32[]{:S(2)}, u32[]{:S(2)}) collective-permute-start(bf16[2,80,512]{2,1,0:T(8,128)(2,1)} %get-tuple-element.15), channel_id=1, source_target_pairs={{0,16},{8,24},{16,0},{24,8},{1,17},{9,25},{17,1},{25,9},{2,18},{10... | collective-permute-start | bytes 491528 | tf_op jit(solution)/shard_map/ppermute | solution.py:26
  11.7 2.5 %collective-permute-done = bf16[2,80,512]{2,1,0:T(8,128)(2,1)S(1)} collective-permute-done((bf16[2,80,512]{2,1,0:T(8,128)(2,1)}, bf16[2,80,512]{2,1,0:T(8,128)(2,1)S(1)}, u32[]{:S(2)}, u32[]{:S(2)}) %collective-permute-start) | collective-permute-done | bytes 163872 | tf_op jit(solution)/shard_map/ppermute | solution.py:26
  14.2 6.2 %collective-permute-done.1 = bf16[2,80,512]{2,1,0:T(8,128)(2,1)S(1)} collective-permute-done((bf16[2,80,512]{2,1,0:T(8,128)(2,1)}, bf16[2,80,512]{2,1,0:T(8,128)(2,1)S(1)}, u32[]{:S(2)}, u32[]{:S(2)}) %collective-permute-start.1) | collective-permute-done | bytes 163872 | tf_op jit(solution)/shard_map/ppermute | solution.py:26
  22.0 8.0 %collective-permute-done.6 = bf16[320,512]{1,0:T(8,128)(2,1)S(1)} collective-permute-done((bf16[320,512]{1,0:T(8,128)(2,1)S(1)}, bf16[320,512]{1,0:T(8,128)(2,1)S(1)}, u32[]{:S(2)}, u32[]{:S(2)}) %collective-permute-start.6) | collective-permute-done | bytes 327712 | tf_op jit(solution)/shard_map/ppermute | solution.py:17
  32.3 15.5 %collective-permute-done.7 = bf16[2,320,512]{2,1,0:T(8,128)(2,1)S(1)} collective-permute-done((bf16[2,320,512]{2,1,0:T(8,128)(2,1)S(1)}, bf16[2,320,512]{2,1,0:T(8,128)(2,1)S(1)}, u32[]{:S(2)}, u32[]{:S(2)}) %collective-permute-start.7) | collective-permute-done | bytes 655392 | tf_op jit(solution)/shard_map/ppermute | solution.py:17
  49.3 1.8 %dynamic-slice_bitcast_fusion.11 = (bf16[512,512]{1,0:T(8,128)(2,1)S(1)}, bf16[512,512]{1,0:T(8,128)(2,1)S(1)}, bf16[512,512]{1,0:T(8,128)(2,1)S(1)}, bf16[512,512]{1,0:T(8,128)(2,1)S(1)}) fusion(bf16[1,512,2048]{2,1,0:T(8,128)(2,1)} %param.19, s32[]{:T(128)S(6)} %select_n.67, s32[]{:T(128)S(6)} %select_n.68, s32[]{:T(128)S(6)} %select_n.70, s32[]{:T(128)S(6)} %select_n.69), kind=kLoop, calls=%fused_computation.87 | loop fusion | bytes 4194320 | tf_op jit(solution)/shard_map/dynamic_slice | solution.py:78
  51.1 1.9 %collective-permute-done.3 = bf16[320,512]{1,0:T(8,128)(2,1)} collective-permute-done((bf16[320,512]{1,0:T(8,128)(2,1)S(1)}, bf16[320,512]{1,0:T(8,128)(2,1)}, u32[]{:S(2)}, u32[]{:S(2)}) %collective-permute-start.3) | collective-permute-done | bytes 327712 | tf_op jit(solution)/shard_map/ppermute | solution.py:17
  56.2 13.3 %collective-permute-done.4 = bf16[2,320,512]{2,1,0:T(8,128)(2,1)S(1)} collective-permute-done((bf16[2,320,512]{2,1,0:T(8,128)(2,1)S(1)}, bf16[2,320,512]{2,1,0:T(8,128)(2,1)S(1)}, u32[]{:S(2)}, u32[]{:S(2)}) %collective-permute-start.4) | collective-permute-done | bytes 655392 | tf_op jit(solution)/shard_map/ppermute | solution.py:17
  74.3 1.9 %multiply_convert_fusion.1 = (bf16[640,512]{1,0:T(8,128)(2,1)S(1)}, bf16[640,512]{1,0:T(8,128)(2,1)S(1)}) fusion(f32[640,512]{1,0:T(8,128)S(1)} %fusion.16, f32[640,512]{1,0:T(8,128)S(1)} %fusion.8, bf16[512,512]{1,0:T(8,128)(2,1)S(1)} %get-tuple-element.37, bf16[512,512]{1,0:T(8,128)(2,1)S(1)} %get-tuple-element.38, ...), kind=kOutput, calls=%fused_computation.43 | convolution fusion | flops 1365311488 | bytes 8650752 | tf_op jit(solution)/shard_map/dot_general | solution.py:30
  78.6 2.5 %convolution_convert_fusion.1 = bf16[2048,512]{1,0:T(8,128)(2,1)S(1)} fusion(bf16[640,512]{1,0:T(8,128)(2,1)S(1)} %get-tuple-element.21, bf16[640,512]{1,0:T(8,128)(2,1)S(1)} %bitcast.132, bf16[640,512]{1,0:T(8,128)(2,1)S(1)} %bitcast.129, bf16[640,512]{1,0:T(8,128)(2,1)S(1)} %bitcast.122, bf16[640,512]{1,0:T(8,128)(2,1)S(1)} %bitcast.119), kind=kOutput, calls=%fused_computation.1 | convolution fusion | flops 1353711616 | bytes 5373952 | tf_op jit(solution)/shard_map/dot_general | solution.py:30
  82.1 3.3 %convolution_convert_fusion = bf16[512,2048]{1,0:T(8,128)(2,1)S(1)} fusion(f32[640,512]{1,0:T(8,128)S(1)} %fusion.8, bf16[640,512]{1,0:T(8,128)(2,1)S(1)} %bitcast.126, bf16[640,512]{1,0:T(8,128)(2,1)S(1)} %bitcast.124, bf16[640,512]{1,0:T(8,128)(2,1)S(1)} %bitcast.116, bf16[640,512]{1,0:T(8,128)(2,1)S(1)} %bitcast.134, f32[640,512]{1,0:T(8,128)S(1)} %fusion.16), kind=kOutput, calls=%fused_computation | convolution fusion | flops 1355677696 | bytes 7340032 | tf_op jit(solution)/shard_map/dot_general | solution.py:30
  91.8 5.2 %collective-permute-done.10 = bf16[320,512]{1,0:T(8,128)(2,1)S(1)} collective-permute-done((bf16[320,512]{1,0:T(8,128)(2,1)S(1)}, bf16[320,512]{1,0:T(8,128)(2,1)S(1)}, u32[]{:S(2)}, u32[]{:S(2)}) %collective-permute-start.10) | collective-permute-done | bytes 327712 | tf_op jit(solution)/shard_map/ppermute | solution.py:17
  97.1 7.2 %collective-permute-done.12 = bf16[320,512]{1,0:T(8,128)(2,1)S(1)} collective-permute-done((bf16[320,512]{1,0:T(8,128)(2,1)S(1)}, bf16[320,512]{1,0:T(8,128)(2,1)S(1)}, u32[]{:S(2)}, u32[]{:S(2)}) %collective-permute-start.12) | collective-permute-done | bytes 327712 | tf_op jit(solution)/shard_map/ppermute | solution.py:21
  105.8 4.3 %collective-permute-start.15 = (bf16[80,512]{1,0:T(8,128)(2,1)S(1)}, bf16[80,512]{1,0:T(8,128)(2,1)S(1)}, u32[]{:S(2)}, u32[]{:S(2)}) collective-permute-start(bf16[80,512]{1,0:T(8,128)(2,1)S(1)} %get-tuple-element.57), channel_id=1, source_target_pairs={{0,8},{8,16},{16,24},{24,0},{1,9},{9,17},{17,25},{25,1},{2,10},{10... | collective-permute-start | bytes 245768 | tf_op jit(solution)/shard_map/ppermute | solution.py:26
  114.0 2.1 %collective-permute-done.14 = bf16[80,512]{1,0:T(8,128)(2,1)S(1)} collective-permute-done((bf16[80,512]{1,0:T(8,128)(2,1)S(1)}, bf16[80,512]{1,0:T(8,128)(2,1)S(1)}, u32[]{:S(2)}, u32[]{:S(2)}) %collective-permute-start.14) | collective-permute-done | bytes 81952 | tf_op jit(solution)/shard_map/ppermute | solution.py:26
  116.4 7.3 %all_gather.3 = bf16[128,2048]{1,0:T(8,128)(2,1)S(1)} all-gather(bf16[128,512]{1,0:T(8,128)(2,1)S(1)} %convolution_convert_fusion.2), channel_id=1, replica_groups=mesh['e'=4,'j'=2,'x'=2,'c'=2] {'x','c'}, dimensions={1}, use_global_device_ids=true | all-gather | bytes 655360 | tf_op jit(solution)/shard_map/all_gather | solution.py:186
  125.3 3.9 %all-to-all-start = ((bf16[8,64,256]{2,1,0:T(8,128)(2,1)}), bf16[8,64,256]{2,1,0:T(8,128)(2,1)S(1)}, u32[]{:S(2)}, u32[]{:S(2)}) async-start(bf16[8,64,256]{2,1,0:T(8,128)(2,1)} %bitcast.101), calls=%async_computation | async-start | bytes 524288 | tf_op jit(solution)/shard_map/all_to_all | solution.py:218
  131.6 4.5 %collective-permute-start.17 = (bf16[1,256]{1,0:T(2,128)(2,1)S(1)}, bf16[1,256]{1,0:T(2,128)(2,1)S(1)}, u32[]{:S(2)}, u32[]{:S(2)}) collective-permute-start(bf16[1,256]{1,0:T(2,128)(2,1)S(1)} %get-tuple-element.79), channel_id=1, source_target_pairs={{0,4},{4,8},{8,12},{12,16},{16,20},{20,24},{24,28},{1,5},{5,9},{9,... | collective-permute-start | bytes 1544 | tf_op jit(solution)/shard_map/ppermute | solution.py:227
  136.2 3.0 %collective-permute-start.18 = (bf16[128,256]{1,0:T(8,128)(2,1)S(1)}, bf16[128,256]{1,0:T(8,128)(2,1)S(1)}, u32[]{:S(2)}, u32[]{:S(2)}) collective-permute-start(bf16[128,256]{1,0:T(8,128)(2,1)S(1)} %get-tuple-element.77), channel_id=1, source_target_pairs={{0,4},{4,0},{1,5},{5,1},{2,6},{6,2},{3,7},{7,3},{8,12},{12,8},{9,1... | collective-permute-start | bytes 196616 | tf_op jit(solution)/shard_map/ppermute | solution.py:17
  141.4 2.4 %collective-permute-start.20 = (bf16[2,128,256]{2,1,0:T(8,128)(2,1)S(1)}, bf16[2,128,256]{2,1,0:T(8,128)(2,1)S(1)}, u32[]{:S(2)}, u32[]{:S(2)}) collective-permute-start(bf16[2,128,256]{2,1,0:T(8,128)(2,1)S(1)} %get-tuple-element.73), channel_id=1, source_target_pairs={{0,16},{8,24},{16,0},{24,8},{1,17},{9,25},{17,1},{25,9},{2,18},{10... | collective-permute-start | bytes 393224 | tf_op jit(solution)/shard_map/ppermute | solution.py:26
  145.2 2.5 %collective-permute-start.21 = (bf16[2,128,256]{2,1,0:T(8,128)(2,1)S(1)}, bf16[2,128,256]{2,1,0:T(8,128)(2,1)S(1)}, u32[]{:S(2)}, u32[]{:S(2)}) collective-permute-start(bf16[2,128,256]{2,1,0:T(8,128)(2,1)S(1)} %get-tuple-element.73), channel_id=1, source_target_pairs={{0,24},{8,0},{16,8},{24,16},{1,25},{9,1},{17,9},{25,17},{2,26},{10... | collective-permute-start | bytes 393224 | tf_op jit(solution)/shard_map/ppermute | solution.py:26
  148.3 4.6 %collective-permute-done.20 = bf16[2,128,256]{2,1,0:T(8,128)(2,1)S(1)} collective-permute-done((bf16[2,128,256]{2,1,0:T(8,128)(2,1)S(1)}, bf16[2,128,256]{2,1,0:T(8,128)(2,1)S(1)}, u32[]{:S(2)}, u32[]{:S(2)}) %collective-permute-start.20) | collective-permute-done | bytes 131104 | tf_op jit(solution)/shard_map/ppermute | solution.py:26
  (111 shorter events, 42.5 us)
Async XLA Ops:
  3.7 10.4 %collective-permute-start = (bf16[2,80,512]{2,1,0:T(8,128)(2,1)}, bf16[2,80,512]{2,1,0:T(8,128)(2,1)S(1)}, u32[]{:S(2)}, u32[]{:S(2)}) collective-permute-start(bf16[2,80,512]{2,1,0:T(8,128)(2,1)} %get-tuple-element.14), channel_id=1, source_target_pairs={{0,8},{8,16},{16,24},{24,0},{1,9},{9,17},{17,25},{25,1},{2,10},{10... | collective-permute-start | bytes 491528 | tf_op jit(solution)/shard_map/ppermute | solution.py:26
  6.8 13.6 %collective-permute-start.1 = (bf16[2,80,512]{2,1,0:T(8,128)(2,1)}, bf16[2,80,512]{2,1,0:T(8,128)(2,1)S(1)}, u32[]{:S(2)}, u32[]{:S(2)}) collective-permute-start(bf16[2,80,512]{2,1,0:T(8,128)(2,1)} %get-tuple-element.15), channel_id=1, source_target_pairs={{0,16},{8,24},{16,0},{24,8},{1,17},{9,25},{17,1},{25,9},{2,18},{10... | collective-permute-start | bytes 491528 | tf_op jit(solution)/shard_map/ppermute | solution.py:26
  9.4 11.0 %collective-permute-start.2 = (bf16[2,80,512]{2,1,0:T(8,128)(2,1)}, bf16[2,80,512]{2,1,0:T(8,128)(2,1)S(1)}, u32[]{:S(2)}, u32[]{:S(2)}) collective-permute-start(bf16[2,80,512]{2,1,0:T(8,128)(2,1)} %get-tuple-element.16), channel_id=1, source_target_pairs={{0,24},{8,0},{16,8},{24,16},{1,25},{9,1},{17,9},{25,17},{2,26},{10... | collective-permute-start | bytes 491528 | tf_op jit(solution)/shard_map/ppermute | solution.py:26
  20.4 9.6 %collective-permute-start.6 = (bf16[320,512]{1,0:T(8,128)(2,1)S(1)}, bf16[320,512]{1,0:T(8,128)(2,1)S(1)}, u32[]{:S(2)}, u32[]{:S(2)}) collective-permute-start(bf16[320,512]{1,0:T(8,128)(2,1)S(1)} %get-tuple-element.63), channel_id=1, source_target_pairs={{0,2},{2,0},{1,3},{3,1},{4,6},{6,4},{5,7},{7,5},{8,10},{10,8},{9,1... | collective-permute-start | bytes 983048 | tf_op jit(solution)/shard_map/ppermute | solution.py:17
  30.1 17.7 %collective-permute-start.7 = (bf16[2,320,512]{2,1,0:T(8,128)(2,1)S(1)}, bf16[2,320,512]{2,1,0:T(8,128)(2,1)S(1)}, u32[]{:S(2)}, u32[]{:S(2)}) collective-permute-start(bf16[2,320,512]{2,1,0:T(8,128)(2,1)S(1)} %get-tuple-element.55), channel_id=1, source_target_pairs={{0,4},{4,0},{1,5},{5,1},{2,6},{6,2},{3,7},{7,3},{8,12},{12,8},{9,1... | collective-permute-start | bytes 1966088 | tf_op jit(solution)/shard_map/ppermute | solution.py:17
  31.8 21.3 %collective-permute-start.3 = (bf16[320,512]{1,0:T(8,128)(2,1)S(1)}, bf16[320,512]{1,0:T(8,128)(2,1)}, u32[]{:S(2)}, u32[]{:S(2)}) collective-permute-start(bf16[320,512]{1,0:T(8,128)(2,1)S(1)} %get-tuple-element.61), channel_id=1, source_target_pairs={{0,4},{4,0},{1,5},{5,1},{2,6},{6,2},{3,7},{7,3},{8,12},{12,8},{9,1... | collective-permute-start | bytes 983048 | tf_op jit(solution)/shard_map/ppermute | solution.py:17
  49.0 20.8 %collective-permute-start.8 = (bf16[2,2,320,512]{3,2,1,0:T(8,128)(2,1)}, bf16[2,2,320,512]{3,2,1,0:T(8,128)(2,1)}, u32[]{:S(2)}, u32[]{:S(2)}) collective-permute-start(bf16[2,2,320,512]{3,2,1,0:T(8,128)(2,1)} %pad_maximum_fusion.2), channel_id=1, source_target_pairs={{0,1},{1,0},{2,3},{3,2},{4,5},{5,4},{6,7},{7,6},{8,9},{9,8},{10,11... | collective-permute-start | bytes 3932168 | tf_op jit(solution)/shard_map/ppermute | solution.py:17
  54.1 15.4 %collective-permute-start.4 = (bf16[2,320,512]{2,1,0:T(8,128)(2,1)S(1)}, bf16[2,320,512]{2,1,0:T(8,128)(2,1)S(1)}, u32[]{:S(2)}, u32[]{:S(2)}) collective-permute-start(bf16[2,320,512]{2,1,0:T(8,128)(2,1)S(1)} %get-tuple-element.53), channel_id=1, source_target_pairs={{0,2},{2,0},{1,3},{3,1},{4,6},{6,4},{5,7},{7,5},{8,10},{10,8},{9,1... | collective-permute-start | bytes 1966088 | tf_op jit(solution)/shard_map/ppermute | solution.py:17
  69.6 4.6 %collective-permute-start.5 = (bf16[2,2,320,512]{3,2,1,0:T(8,128)(2,1)S(1)}, bf16[2,2,320,512]{3,2,1,0:T(8,128)(2,1)S(1)}, u32[]{:S(2)}, u32[]{:S(2)}) collective-permute-start(bf16[2,2,320,512]{3,2,1,0:T(8,128)(2,1)S(1)} %pad_maximum_fusion.3), channel_id=1, source_target_pairs={{0,1},{1,0},{2,3},{3,2},{4,5},{5,4},{6,7},{7,6},{8,9},{9,8},{10,11... | collective-permute-start | bytes 3932168 | tf_op jit(solution)/shard_map/ppermute | solution.py:17
  78.0 7.4 %collective-permute-start.9 = (bf16[640,1024]{1,0:T(8,128)(2,1)S(1)}, bf16[640,1024]{1,0:T(8,128)(2,1)S(1)}, u32[]{:S(2)}, u32[]{:S(2)}) collective-permute-start(bf16[640,1024]{1,0:T(8,128)(2,1)S(1)} %add_convert_fusion.1), channel_id=1, source_target_pairs={{0,1},{1,0},{2,3},{3,2},{4,5},{5,4},{6,7},{7,6},{8,9},{9,8},{10,11... | collective-permute-start | bytes 3932168 | tf_op jit(solution)/shard_map/ppermute | solution.py:17
  86.4 10.6 %collective-permute-start.10 = (bf16[320,512]{1,0:T(8,128)(2,1)S(1)}, bf16[320,512]{1,0:T(8,128)(2,1)S(1)}, u32[]{:S(2)}, u32[]{:S(2)}) collective-permute-start(bf16[320,512]{1,0:T(8,128)(2,1)S(1)} %get-tuple-element.43), channel_id=1, source_target_pairs={{0,2},{2,0},{1,3},{3,1},{4,6},{6,4},{5,7},{7,5},{8,10},{10,8},{9,1... | collective-permute-start | bytes 983048 | tf_op jit(solution)/shard_map/ppermute | solution.py:17
  88.0 16.2 %collective-permute-start.12 = (bf16[320,512]{1,0:T(8,128)(2,1)S(1)}, bf16[320,512]{1,0:T(8,128)(2,1)S(1)}, u32[]{:S(2)}, u32[]{:S(2)}) collective-permute-start(bf16[320,512]{1,0:T(8,128)(2,1)S(1)} %get-tuple-element.44), channel_id=1, source_target_pairs={{0,6},{2,4},{4,2},{6,0},{1,7},{3,5},{5,3},{7,1},{8,14},{10,12},{12... | collective-permute-start | bytes 983048 | tf_op jit(solution)/shard_map/ppermute | solution.py:21
  89.5 16.1 %collective-permute-start.11 = (bf16[320,512]{1,0:T(8,128)(2,1)S(1)}, bf16[320,512]{1,0:T(8,128)(2,1)S(1)}, u32[]{:S(2)}, u32[]{:S(2)}) collective-permute-start(bf16[320,512]{1,0:T(8,128)(2,1)S(1)} %get-tuple-element.45), channel_id=1, source_target_pairs={{0,4},{4,0},{1,5},{5,1},{2,6},{6,2},{3,7},{7,3},{8,12},{12,8},{9,1... | collective-permute-start | bytes 983048 | tf_op jit(solution)/shard_map/ppermute | solution.py:17
  105.8 8.2 %collective-permute-start.15 = (bf16[80,512]{1,0:T(8,128)(2,1)S(1)}, bf16[80,512]{1,0:T(8,128)(2,1)S(1)}, u32[]{:S(2)}, u32[]{:S(2)}) collective-permute-start(bf16[80,512]{1,0:T(8,128)(2,1)S(1)} %get-tuple-element.57), channel_id=1, source_target_pairs={{0,8},{8,16},{16,24},{24,0},{1,9},{9,17},{17,25},{25,1},{2,10},{10... | collective-permute-start | bytes 245768 | tf_op jit(solution)/shard_map/ppermute | solution.py:26
  110.1 6.0 %collective-permute-start.14 = (bf16[80,512]{1,0:T(8,128)(2,1)S(1)}, bf16[80,512]{1,0:T(8,128)(2,1)S(1)}, u32[]{:S(2)}, u32[]{:S(2)}) collective-permute-start(bf16[80,512]{1,0:T(8,128)(2,1)S(1)} %get-tuple-element.58), channel_id=1, source_target_pairs={{0,16},{8,24},{16,0},{24,8},{1,17},{9,25},{17,1},{25,9},{2,18},{10... | collective-permute-start | bytes 245768 | tf_op jit(solution)/shard_map/ppermute | solution.py:26
  110.7 5.4 %collective-permute-start.13 = (bf16[80,512]{1,0:T(8,128)(2,1)S(1)}, bf16[80,512]{1,0:T(8,128)(2,1)S(1)}, u32[]{:S(2)}, u32[]{:S(2)}) collective-permute-start(bf16[80,512]{1,0:T(8,128)(2,1)S(1)} %get-tuple-element.59), channel_id=1, source_target_pairs={{0,24},{8,0},{16,8},{24,16},{1,25},{9,1},{17,9},{25,17},{2,26},{10... | collective-permute-start | bytes 245768 | tf_op jit(solution)/shard_map/ppermute | solution.py:26
  125.3 28.0 %all-to-all-start = ((bf16[8,64,256]{2,1,0:T(8,128)(2,1)}), bf16[8,64,256]{2,1,0:T(8,128)(2,1)S(1)}, u32[]{:S(2)}, u32[]{:S(2)}) async-start(bf16[8,64,256]{2,1,0:T(8,128)(2,1)} %bitcast.101), calls=%async_computation | async-start | bytes 524288 | tf_op jit(solution)/shard_map/all_to_all | solution.py:218
  130.3 8.8 %collective-permute-start.16 = (bf16[1,256]{1,0:T(2,128)(2,1)S(1)}, bf16[1,256]{1,0:T(2,128)(2,1)S(1)}, u32[]{:S(2)}, u32[]{:S(2)}) collective-permute-start(bf16[1,256]{1,0:T(2,128)(2,1)S(1)} %get-tuple-element.78), channel_id=1, source_target_pairs={{4,0},{8,4},{12,8},{16,12},{20,16},{24,20},{28,24},{5,1},{9,5},{13... | collective-permute-start | bytes 1544 | tf_op jit(solution)/shard_map/ppermute | solution.py:228
  131.6 7.6 %collective-permute-start.17 = (bf16[1,256]{1,0:T(2,128)(2,1)S(1)}, bf16[1,256]{1,0:T(2,128)(2,1)S(1)}, u32[]{:S(2)}, u32[]{:S(2)}) collective-permute-start(bf16[1,256]{1,0:T(2,128)(2,1)S(1)} %get-tuple-element.79), channel_id=1, source_target_pairs={{0,4},{4,8},{8,12},{12,16},{16,20},{20,24},{24,28},{1,5},{5,9},{9,... | collective-permute-start | bytes 1544 | tf_op jit(solution)/shard_map/ppermute | solution.py:227
  136.2 5.2 %collective-permute-start.18 = (bf16[128,256]{1,0:T(8,128)(2,1)S(1)}, bf16[128,256]{1,0:T(8,128)(2,1)S(1)}, u32[]{:S(2)}, u32[]{:S(2)}) collective-permute-start(bf16[128,256]{1,0:T(8,128)(2,1)S(1)} %get-tuple-element.77), channel_id=1, source_target_pairs={{0,4},{4,0},{1,5},{5,1},{2,6},{6,2},{3,7},{7,3},{8,12},{12,8},{9,1... | collective-permute-start | bytes 196616 | tf_op jit(solution)/shard_map/ppermute | solution.py:17
  141.4 11.6 %collective-permute-start.20 = (bf16[2,128,256]{2,1,0:T(8,128)(2,1)S(1)}, bf16[2,128,256]{2,1,0:T(8,128)(2,1)S(1)}, u32[]{:S(2)}, u32[]{:S(2)}) collective-permute-start(bf16[2,128,256]{2,1,0:T(8,128)(2,1)S(1)} %get-tuple-element.73), channel_id=1, source_target_pairs={{0,16},{8,24},{16,0},{24,8},{1,17},{9,25},{17,1},{25,9},{2,18},{10... | collective-permute-start | bytes 393224 | tf_op jit(solution)/shard_map/ppermute | solution.py:26
  143.8 9.1 %collective-permute-start.19 = (bf16[2,128,256]{2,1,0:T(8,128)(2,1)S(1)}, bf16[2,128,256]{2,1,0:T(8,128)(2,1)S(1)}, u32[]{:S(2)}, u32[]{:S(2)}) collective-permute-start(bf16[2,128,256]{2,1,0:T(8,128)(2,1)S(1)} %get-tuple-element.73), channel_id=1, source_target_pairs={{0,8},{8,16},{16,24},{24,0},{1,9},{9,17},{17,25},{25,1},{2,10},{10... | collective-permute-start | bytes 393224 | tf_op jit(solution)/shard_map/ppermute | solution.py:26
  145.2 7.8 %collective-permute-start.21 = (bf16[2,128,256]{2,1,0:T(8,128)(2,1)S(1)}, bf16[2,128,256]{2,1,0:T(8,128)(2,1)S(1)}, u32[]{:S(2)}, u32[]{:S(2)}) collective-permute-start(bf16[2,128,256]{2,1,0:T(8,128)(2,1)S(1)} %get-tuple-element.73), channel_id=1, source_target_pairs={{0,24},{8,0},{16,8},{24,16},{1,25},{9,1},{17,9},{25,17},{2,26},{10... | collective-permute-start | bytes 393224 | tf_op jit(solution)/shard_map/ppermute | solution.py:26
  153.3 1.6 %collective-permute-start.22 = (bf16[512,256]{1,0:T(8,128)(2,1)S(1)}, bf16[512,256]{1,0:T(8,128)(2,1)S(1)}, u32[]{:S(2)}, u32[]{:S(2)}) collective-permute-start(bf16[512,256]{1,0:T(8,128)(2,1)S(1)} %bitcast.136), channel_id=1, source_target_pairs={{0,1},{1,0},{2,3},{3,2},{4,5},{5,4},{6,7},{7,6},{8,9},{9,8},{10,11... | collective-permute-start | bytes 786440 | tf_op jit(solution)/shard_map/ppermute | solution.py:17
  (12 other events, 272.0 us)

commit v2 on v1

--- a/solution.py
+++ b/solution.py
@@ -8,6 +8,7 @@
 from jax.sharding import Mesh
 from jax.sharding import PartitionSpec as P
 
+
 epsilon = 1e-06
 F32 = jnp.float32
 BF16 = jnp.bfloat16
@@ -21,9 +22,19 @@
     return lax.ppermute(value, ("j", "x"), [(i, 3 - i) for i in range(4)])
 
 
-def shifted(value, step):
+def exchange(blocks, sign):
     count = lax.axis_size("e")
-    return lax.ppermute(value, "e", [(i, (i + step) % count) for i in range(count)])
+    if count <= 8:
+        return [
+            lax.ppermute(b, "e", [(i, (i + sign * s) % count) for i in range(count)])
+            for s, b in enumerate(blocks)
+            if s
+        ]
+    mine, order = lax.axis_index("e"), jnp.arange(count)
+    to = jnp.take(jnp.stack(blocks), sign * (order - mine) % count, axis=0)
+    came = lax.all_to_all(to, "e", 0, 0, tiled=True)
+    came = jnp.take(came, (mine - sign * order) % count, axis=0)
+    return [came[s] for s in range(1, count)]
 
 
 def dot(a, b, ca, cb):
@@ -129,23 +140,40 @@
         out_grad,
     )
     sends, sel = outs[:-1], outs[-1]
-    came = [sends[0]] + [shifted(sends[s], s) for s in range(1, experts)]
+    conv_f32 = conv_out.astype(F32)
+    gate_f32 = out_gate.astype(F32)
+    mixed = (gate_f32 * conv_f32).astype(BF16)
+    mixed_pair = jnp.stack([mixed, swap(mixed, "j")])
+
+    came = exchange(sends, 1)
+    own_pair = jnp.stack([sends[0], swap(sends[0], "x")])
+    own_four = jnp.stack([own_pair, swap(own_pair, "j")])
+    came, own_four, mixed_pair = lax.optimization_barrier((came, own_four, mixed_pair))
     rows_z = jnp.concatenate([b[0] for b in came], axis=0)
     grads_z = jnp.concatenate([b[1] for b in came], axis=0)
-    count = rows_z.shape[0]
-
-    rows_x, grads_y = swap(rows_z, "x"), swap(grads_z, "j")
+    count = experts * cap
+
+    rows_x, grads_y = lax.optimization_barrier((swap(rows_z, "x"), swap(grads_z, "j")))
     rows_pair = jnp.stack([rows_z, rows_x])
     grads_pair = jnp.stack([grads_z, grads_y])
-    rows_four = jnp.stack([rows_pair, swap(rows_pair, "j")])
-    grads_four = jnp.stack([grads_pair, swap(grads_pair, "x")])
+    own_sib = swap(own_four, "c")
+    mixed_rel = [mixed_pair] + exchange([mixed_pair] * experts, 1)
+    rows_y, grads_x, own_sib, mixed_rel = lax.optimization_barrier(
+        (swap(rows_pair, "j"), swap(grads_pair, "x"), own_sib, mixed_rel)
+    )
+    rows_four = jnp.stack([rows_pair, rows_y])
+    grads_four = jnp.stack([grads_pair, grads_x], axis=1)
     rows_sib, grads_sib = swap(rows_four, "c"), swap(grads_four, "c")
-    rows = jnp.concatenate(
-        [rows_four[:, 0], rows_four[:, 1], rows_sib[:, 0], rows_sib[:, 1]], axis=-1
-    ).reshape(2 * count, features)
-    grads = jnp.concatenate(
-        [grads_four[0], grads_four[1], grads_sib[0], grads_sib[1]], axis=-1
-    ).reshape(2 * count, features)
+
+    def assemble(which, four, sib):
+        cells = []
+        for own, rest in ((own_four, four), (own_sib, sib)):
+            for dx in range(2):
+                cells.append(jnp.concatenate([own[:, dx, which], rest[:, dx]], axis=1))
+        return jnp.concatenate(cells, axis=-1).reshape(2 * count, features)
+
+    rows = assemble(0, rows_four, rows_sib)
+    grads = assemble(1, grads_four, grads_sib)
 
     gate_w = jnp.concatenate(relative(w_gate[0], 0, place), axis=0)
     up_w = jnp.concatenate(relative(w_up[0], 0, place), axis=0)
@@ -173,12 +201,12 @@
         + swap(block(1, 0), "j").astype(F32)
         + swap_both(block(1, 1)).astype(F32)
     ).astype(BF16)
-    back = [summed[:cap]] + [
-        shifted(summed[s * cap : (s + 1) * cap], -s) for s in range(1, experts)
-    ]
-
-    grad_up = absolute(dot(rows, d_up, 0, 0).astype(BF16), 0, place)
-    grad_down = absolute(dot(hidden, grads, 0, 0).astype(BF16), 1, place)
+    back = [summed[s * cap : (s + 1) * cap] for s in range(experts)]
+    back = back[:1] + exchange(back, -1)
+
+    grad_up = dot(rows, d_up, 0, 0).astype(BF16)
+    grad_down = dot(hidden, grads, 0, 0).astype(BF16)
+    grad_up, grad_down = absolute(grad_up, 0, place), absolute(grad_down, 1, place)
 
     d_part = dot(
         sel.reshape(experts * cap, tokens), jnp.concatenate(back, axis=0), 0, 0
@@ -190,11 +218,7 @@
     row_mean = jnp.mean(unit_rows * d_normed, axis=-1, keepdims=True)
     grad_resid = (out_grad.astype(F32) + inv_rms * (d_normed - unit_rows * row_mean)).astype(BF16)
 
-    conv_f32 = conv_out.astype(F32)
-    gate_f32 = out_gate.astype(F32)
-    mixed = (gate_f32 * conv_f32).astype(BF16)
-    mixed_pair = jnp.stack([mixed, swap(mixed, "j")])
-    mixed_rel = jnp.stack([mixed_pair] + [shifted(mixed_pair, s) for s in range(1, experts)])
+    mixed_rel = jnp.stack(mixed_rel)
     channels = mixed.shape[1]
     mixed_rel = mixed_rel.reshape(slices, tokens, channels)
     mixed_all = jnp.concatenate(
@@ -271,6 +295,7 @@
         P(sp, tp),
         P(sp, tp),
     )
+
     return jax.shard_map(
         per_device, mesh=inner, in_specs=in_specs, out_specs=out_specs, check_vma=False
     )

time: 156 us -> 142 us (0.910); the launches traced: 156 us -> 140 us
  waiting for transfers between devices: 70.7 us -> 41 us
  other arithmetic: 8.85 us -> 17.2 us
  local copies, waits for them, and re-layouts: 6.2 us -> 10.4 us
  starting transfers between devices: 42.2 us -> 46.1 us
  matrix products: 16.9 us -> 15 us
    ppermute x11 -> x14, waiting for transfers between devices: 48 us -> 19 us  [swap(): return lax.ppermute(value, axis, [(0, 1), (1, 0)])]
    another operation x7 -> x8, other arithmetic: 2.64 us -> 6.84 us  [the longest x2 2.9 us: per_device(): rows_four = jnp.stack([rows_pair, rows_y])]
    ppermute x9, waiting for transfers between devices: 15.5 us -> 12.7 us  [exchange(): lax.ppermute(b, 'e', [(i, (i + sign * s) % count) for i in range(count)])]
    dynamic_slice x2, local copies, waits for them, and re-layouts: 2.28 us -> 5.05 us  [relative(): lax.dynamic_slice_in_dim(value, (place ^ 2 * dx + dc) * width, width, axis)]
    concatenate x0 -> x2, other arithmetic: none -> 2.14 us  [assemble(): return jnp.concatenate(cells, axis=-1).reshape(2 * count, features)]
    dot_general x13, matrix products: 16.9 us -> 15 us  [dot(): lax.dot_general(a, b, (((ca,), (cb,)), ((), ())), preferred_element_type=...]
    unnamed x31 -> x57, local copies, waits for them, and re-layouts: 0.17 us -> 1.96 us
    ppermute x9, starting transfers between devices: 20 us -> 21.6 us  [exchange(): lax.ppermute(b, 'e', [(i, (i + sign * s) % count) for i in range(count)])]
  transfers between devices with their start and end apart: 24 -> 27, of which waited for: 14 -> 17; matrix products, arithmetic and copies ran while one was open for 15% -> 20% of each run, Pallas kernels for 0% -> 0%
where the time goes in v2:
time: 142 us; the launch traced here: 140 us
  starting transfers between devices  46.1 us (32%)
  waiting for transfers between devices  41 us (29%)
  other arithmetic  17.2 us (12%)
  matrix products  15 us (11%)
  local copies, waits for them, and re-layouts  10.4 us (7%)
  blocking collectives  6.63 us (5%)
  Pallas kernels  2.48 us (2%)
    ppermute x9, starting transfers between devices, exchange(): lax.ppermute(b, 'e', [(i, (i + sign * s) % count) for i in range(count)])  21.6 us
    ppermute x14, waiting for transfers between devices, swap(): return lax.ppermute(value, axis, [(0, 1), (1, 0)])  19 us
    dot_general x13, matrix products, dot(): lax.dot_general(a, b, (((ca,), (cb,)), ((), ())), preferred_element_type=...  15 us
    ppermute x9, waiting for transfers between devices, exchange(): lax.ppermute(b, 'e', [(i, (i + sign * s) % count) for i in range(count)])  12.7 us
    ppermute x14, starting transfers between devices, swap(): return lax.ppermute(value, axis, [(0, 1), (1, 0)])  12.2 us
    ppermute x1, waiting for transfers between devices, swap_both(): return lax.ppermute(value, ('j', 'x'), [(i, 3 - i) for i in range(4)])  7.54 us
    all_gather x1, blocking collectives, per_device(): lax.all_gather(d_part, ('x', 'c'), axis=1, tiled=True).astype(F32)  6.63 us
    dynamic_slice x2, local copies, waits for them, and re-layouts, relative(): lax.dynamic_slice_in_dim(value, (place ^ 2 * dx + dc) * width, width, axis)  5.05 us
  transfers between devices with their start and end apart: 27, of which 17 were waited for; matrix products, arithmetic and copies ran while one was open for 20% of the time, Pallas kernels for 0%

profile of v2, /device:TPU:0, one launch (start us, length us, event | category | flops | bytes accessed | tf_op | source)
XLA Modules:
  0.0 140.1 jit_solution(7020054979478896180)
XLA Ops:
  1.3 2.5 %shard_map.180 = (bf16[2,80,512]{2,1,0:T(8,128)(2,1)}, bf16[2,80,512]{2,1,0:T(8,128)(2,1)}, bf16[2,80,512]{2,1,0:T(8,128)(2,1)}, bf16[2,80,512]{2,1,0:T(8,128)(2,1)}, bf16[4,80,128]{2,1,0:T(8,128)(2,1)}) custom-call(s32[2]{0:T(128)} %pad_add_fusion.index_ref, s32[2,128]{1,0:T(2,128)} %bitcast.167, f32[2,128]{1,0:T(2,128)} %bitcast.168, ...), custom_call_target="tpu_custom_call" | custom-call | tf_op jit(solution)/shard_map/pallas_call | solution.py:128
  3.7 3.0 %collective-permute-start.3 = (bf16[2,80,512]{2,1,0:T(8,128)(2,1)}, bf16[2,80,512]{2,1,0:T(8,128)(2,1)S(1)}, u32[]{:S(2)}, u32[]{:S(2)}) collective-permute-start(bf16[2,80,512]{2,1,0:T(8,128)(2,1)} %get-tuple-element.30), channel_id=1, source_target_pairs={{0,2},{2,0},{1,3},{3,1},{4,6},{6,4},{5,7},{7,5},{8,10},{10,8},{9,1... | collective-permute-start | bytes 491528 | tf_op jit(solution)/shard_map/ppermute | solution.py:18
  6.7 4.4 %collective-permute-done.3 = bf16[2,80,512]{2,1,0:T(8,128)(2,1)S(1)} collective-permute-done((bf16[2,80,512]{2,1,0:T(8,128)(2,1)}, bf16[2,80,512]{2,1,0:T(8,128)(2,1)S(1)}, u32[]{:S(2)}, u32[]{:S(2)}) %collective-permute-start.3) | collective-permute-done | bytes 163872 | tf_op jit(solution)/shard_map/ppermute | solution.py:18
  12.1 1.8 %collective-permute-start.4 = (bf16[2,2,80,512]{3,2,1,0:T(8,128)(2,1)S(1)}, bf16[2,2,80,512]{3,2,1,0:T(8,128)(2,1)S(1)}, u32[]{:S(2)}, u32[]{:S(2)}) collective-permute-start(bf16[2,2,80,512]{3,2,1,0:T(8,128)(2,1)S(1)} %get-tuple-element.97), channel_id=1, source_target_pairs={{0,4},{4,0},{1,5},{5,1},{2,6},{6,2},{3,7},{7,3},{8,12},{12,8},{9,1... | collective-permute-start | bytes 983048 | tf_op jit(solution)/shard_map/ppermute | solution.py:18
  17.0 2.6 %collective-permute-start.1 = (bf16[2,80,512]{2,1,0:T(8,128)(2,1)}, bf16[2,80,512]{2,1,0:T(8,128)(2,1)S(1)}, u32[]{:S(2)}, u32[]{:S(2)}) collective-permute-start(bf16[2,80,512]{2,1,0:T(8,128)(2,1)} %get-tuple-element.28), channel_id=1, source_target_pairs={{0,16},{8,24},{16,0},{24,8},{1,17},{9,25},{17,1},{25,9},{2,18},{10... | collective-permute-start | bytes 491528 | tf_op jit(solution)/shard_map/ppermute | solution.py:29
  24.4 4.7 %collective-permute-done.1 = bf16[2,80,512]{2,1,0:T(8,128)(2,1)S(1)} collective-permute-done((bf16[2,80,512]{2,1,0:T(8,128)(2,1)}, bf16[2,80,512]{2,1,0:T(8,128)(2,1)S(1)}, u32[]{:S(2)}, u32[]{:S(2)}) %collective-permute-start.1) | collective-permute-done | bytes 163872 | tf_op jit(solution)/shard_map/ppermute | solution.py:29
  32.5 4.6 %collective-permute-done.7 = bf16[240,512]{1,0:T(8,128)(2,1)S(1)} collective-permute-done((bf16[240,512]{1,0:T(8,128)(2,1)S(1)}, bf16[240,512]{1,0:T(8,128)(2,1)S(1)}, u32[]{:S(2)}, u32[]{:S(2)}) %collective-permute-start.7) | collective-permute-done | bytes 245792 | tf_op jit(solution)/shard_map/ppermute | solution.py:18
  43.3 3.4 %dynamic-slice_bitcast_fusion.3 = (bf16[512,512]{1,0:T(8,128)(2,1)S(1)}, bf16[512,512]{1,0:T(8,128)(2,1)}, bf16[512,512]{1,0:T(8,128)(2,1)}, bf16[512,512]{1,0:T...) fusion(bf16[1,2048,512]{2,1,0:T(8,128)(2,1)S(1)} %copy-done.3, ...), kind=kLoop, calls=%fused_computation.76 | loop fusion | bytes 8388624 | tf_op jit(solution)/shard_map/dynamic_slice | solution.py:89
  46.7 3.7 %collective-permute-start.13 = (bf16[2,128,256]{2,1,0:T(8,128)(2,1)}, bf16[2,128,256]{2,1,0:T(8,128)(2,1)S(1)}, u32[]{:S(2)}, u32[]{:S(2)}) collective-permute-start(bf16[2,128,256]{2,1,0:T(8,128)(2,1)} %pad_maximum_fusion.9), channel_id=1, source_target_pairs={{0,24},{8,0},{16,8},{24,16},{1,25},{9,1},{17,9},{25,17},{2,26},{10... | collective-permute-start | bytes 393224 | tf_op jit(solution)/shard_map/ppermute | solution.py:29
  52.2 1.9 %collective-permute-start.12 = (bf16[2,128,256]{2,1,0:T(8,128)(2,1)S(1)}, bf16[2,128,256]{2,1,0:T(8,128)(2,1)S(1)}, u32[]{:S(2)}, u32[]{:S(2)}) collective-permute-start(bf16[2,128,256]{2,1,0:T(8,128)(2,1)S(1)} %copy-done.16), channel_id=1, source_target_pairs={{0,16},{8,24},{16,0},{24,8},{1,17},{9,25},{17,1},{25,9},{2,18},{10... | collective-permute-start | bytes 393224 | tf_op jit(solution)/shard_map/ppermute | solution.py:29
  55.3 5.3 %collective-permute-start.11 = (bf16[2,128,256]{2,1,0:T(8,128)(2,1)S(1)}, bf16[2,128,256]{2,1,0:T(8,128)(2,1)S(1)}, u32[]{:S(2)}, u32[]{:S(2)}) collective-permute-start(bf16[2,128,256]{2,1,0:T(8,128)(2,1)S(1)} %copy-done.16), channel_id=1, source_target_pairs={{0,8},{8,16},{16,24},{24,0},{1,9},{9,17},{17,25},{25,1},{2,10},{10... | collective-permute-start | bytes 393224 | tf_op jit(solution)/shard_map/ppermute | solution.py:29
  60.6 2.2 %collective-permute-done.12 = bf16[2,128,256]{2,1,0:T(8,128)(2,1)S(1)} collective-permute-done((bf16[2,128,256]{2,1,0:T(8,128)(2,1)S(1)}, bf16[2,128,256]{2,1,0:T(8,128)(2,1)S(1)}, u32[]{:S(2)}, u32[]{:S(2)}) %collective-permute-start.12) | collective-permute-done | bytes 131104 | tf_op jit(solution)/shard_map/ppermute | solution.py:29
  76.5 2.1 %multiply_convert_fusion.1 = (bf16[640,512]{1,0:T(8,128)(2,1)S(1)}, bf16[640,512]{1,0:T(8,128)(2,1)S(1)}) fusion(f32[640,512]{1,0:T(8,128)S(1)} %fusion.16, f32[640,512]{1,0:T(8,128)S(1)} %fusion.8, bf16[640,2048]{1,0:T(8,128)(2,1)S(1)} %bitcast.140, bf16[512,512]{1,0:T(8,128)(2,1)S(1)} %get-tuple-element.65, bf16[512,512]{1,0:T(8,128)(2,1)S(1)} %get-tuple-element.66, ...), kind=kOutput, calls=%fused_computation.37 | convolution fusion | flops 1354825728 | bytes 8650752 | tf_op jit(solution)/shard_map/dot_general | solution.py:41
  80.5 1.8 %convolution_convert_fusion.1 = bf16[2048,512]{1,0:T(8,128)(2,1)S(1)} fusion(bf16[640,2048]{1,0:T(8,128)(2,1)S(1)} %bitcast.139, bf16[640,512]{1,0:T(8,128)(2,1)S(1)} %get-tuple-element.49), kind=kOutput, calls=%fused_computation.1 | convolution fusion | flops 1343225856 | bytes 5373952 | tf_op jit(solution)/shard_map/dot_general | solution.py:41
  83.3 1.9 %convolution_convert_fusion = bf16[512,2048]{1,0:T(8,128)(2,1)S(1)} fusion(bf16[640,2048]{1,0:T(8,128)(2,1)S(1)} %bitcast.141, f32[640,512]{1,0:T(8,128)S(1)} %fusion.8, f32[640,512]{1,0:T(8,128)S(1)} %fusion.16), kind=kOutput, calls=%fused_computation | convolution fusion | flops 1345191936 | bytes 7340032 | tf_op jit(solution)/shard_map/dot_general | solution.py:41
  86.9 2.4 %collective-permute-start.19 = (bf16[320,512]{1,0:T(8,128)(2,1)S(1)}, bf16[320,512]{1,0:T(8,128)(2,1)S(1)}, u32[]{:S(2)}, u32[]{:S(2)}) collective-permute-start(bf16[320,512]{1,0:T(8,128)(2,1)S(1)} %get-tuple-element.72), channel_id=1, source_target_pairs={{0,6},{2,4},{4,2},{6,0},{1,7},{3,5},{5,3},{7,1},{8,14},{10,12},{12... | collective-permute-start | bytes 983048 | tf_op jit(solution)/shard_map/ppermute | solution.py:22
  91.7 5.2 %collective-permute-done.17 = bf16[320,512]{1,0:T(8,128)(2,1)S(1)} collective-permute-done((bf16[320,512]{1,0:T(8,128)(2,1)S(1)}, bf16[320,512]{1,0:T(8,128)(2,1)S(1)}, u32[]{:S(2)}, u32[]{:S(2)}) %collective-permute-start.17) | collective-permute-done | bytes 327712 | tf_op jit(solution)/shard_map/ppermute | solution.py:18
  96.9 7.5 %collective-permute-done.19 = bf16[320,512]{1,0:T(8,128)(2,1)S(1)} collective-permute-done((bf16[320,512]{1,0:T(8,128)(2,1)S(1)}, bf16[320,512]{1,0:T(8,128)(2,1)S(1)}, u32[]{:S(2)}, u32[]{:S(2)}) %collective-permute-start.19) | collective-permute-done | bytes 327712 | tf_op jit(solution)/shard_map/ppermute | solution.py:22
  106.1 2.5 %collective-permute-start.22 = (bf16[80,512]{1,0:T(8,128)(2,1)S(1)}, bf16[80,512]{1,0:T(8,128)(2,1)S(1)}, u32[]{:S(2)}, u32[]{:S(2)}) collective-permute-start(bf16[80,512]{1,0:T(8,128)(2,1)S(1)} %get-tuple-element.93), channel_id=1, source_target_pairs={{0,8},{8,16},{16,24},{24,0},{1,9},{9,17},{17,25},{25,1},{2,10},{10... | collective-permute-start | bytes 245768 | tf_op jit(solution)/shard_map/ppermute | solution.py:29
  108.6 2.4 %collective-permute-start.20 = (bf16[80,512]{1,0:T(8,128)(2,1)S(1)}, bf16[80,512]{1,0:T(8,128)(2,1)S(1)}, u32[]{:S(2)}, u32[]{:S(2)}) collective-permute-start(bf16[80,512]{1,0:T(8,128)(2,1)S(1)} %get-tuple-element.95), channel_id=1, source_target_pairs={{0,24},{8,0},{16,8},{24,16},{1,25},{9,1},{17,9},{25,17},{2,26},{10... | collective-permute-start | bytes 245768 | tf_op jit(solution)/shard_map/ppermute | solution.py:29
  112.8 2.8 %collective-permute-done.21 = bf16[80,512]{1,0:T(8,128)(2,1)S(1)} collective-permute-done((bf16[80,512]{1,0:T(8,128)(2,1)S(1)}, bf16[80,512]{1,0:T(8,128)(2,1)S(1)}, u32[]{:S(2)}, u32[]{:S(2)}) %collective-permute-start.21) | collective-permute-done | bytes 81952 | tf_op jit(solution)/shard_map/ppermute | solution.py:29
  115.8 6.6 %all_gather.3 = bf16[128,2048]{1,0:T(8,128)(2,1)S(1)} all-gather(bf16[128,512]{1,0:T(8,128)(2,1)S(1)} %convolution_convert_fusion.2), channel_id=1, replica_groups=mesh['e'=4,'j'=2,'x'=2,'c'=2] {'x','c'}, dimensions={1}, use_global_device_ids=true | all-gather | bytes 655360 | tf_op jit(solution)/shard_map/all_gather | solution.py:214
  124.0 4.1 %all-to-all-start = ((bf16[8,64,256]{2,1,0:T(8,128)(2,1)}), bf16[8,64,256]{2,1,0:T(8,128)(2,1)S(1)}, u32[]{:S(2)}, u32[]{:S(2)}) async-start(bf16[8,64,256]{2,1,0:T(8,128)(2,1)} %bitcast.136), calls=%async_computation | async-start | bytes 524288 | tf_op jit(solution)/shard_map/all_to_all | solution.py:242
  130.6 4.5 %collective-permute-start.24 = (bf16[1,256]{1,0:T(2,128)(2,1)S(1)}, bf16[1,256]{1,0:T(2,128)(2,1)S(1)}, u32[]{:S(2)}, u32[]{:S(2)}) collective-permute-start(bf16[1,256]{1,0:T(2,128)(2,1)S(1)} %get-tuple-element.112), channel_id=1, source_target_pairs={{0,4},{4,8},{8,12},{12,16},{16,20},{20,24},{24,28},{1,5},{5,9},{9,... | collective-permute-start | bytes 1544 | tf_op jit(solution)/shard_map/ppermute | solution.py:251
  (148 shorter events, 54.8 us)
Async XLA Ops:
  3.7 7.4 %collective-permute-start.3 = (bf16[2,80,512]{2,1,0:T(8,128)(2,1)}, bf16[2,80,512]{2,1,0:T(8,128)(2,1)S(1)}, u32[]{:S(2)}, u32[]{:S(2)}) collective-permute-start(bf16[2,80,512]{2,1,0:T(8,128)(2,1)} %get-tuple-element.30), channel_id=1, source_target_pairs={{0,2},{2,0},{1,3},{3,1},{4,6},{6,4},{5,7},{7,5},{8,10},{10,8},{9,1... | collective-permute-start | bytes 491528 | tf_op jit(solution)/shard_map/ppermute | solution.py:18
  12.1 11.0 %collective-permute-start.4 = (bf16[2,2,80,512]{3,2,1,0:T(8,128)(2,1)S(1)}, bf16[2,2,80,512]{3,2,1,0:T(8,128)(2,1)S(1)}, u32[]{:S(2)}, u32[]{:S(2)}) collective-permute-start(bf16[2,2,80,512]{3,2,1,0:T(8,128)(2,1)S(1)} %get-tuple-element.97), channel_id=1, source_target_pairs={{0,4},{4,0},{1,5},{5,1},{2,6},{6,2},{3,7},{7,3},{8,12},{12,8},{9,1... | collective-permute-start | bytes 983048 | tf_op jit(solution)/shard_map/ppermute | solution.py:18
  14.8 7.6 %collective-permute-start.5 = (bf16[128,256]{1,0:T(8,128)(2,1)S(1)}, bf16[128,256]{1,0:T(8,128)(2,1)S(1)}, u32[]{:S(2)}, u32[]{:S(2)}) collective-permute-start(bf16[128,256]{1,0:T(8,128)(2,1)S(1)} %fusion.58), channel_id=1, source_target_pairs={{0,4},{4,0},{1,5},{5,1},{2,6},{6,2},{3,7},{7,3},{8,12},{12,8},{9,1... | collective-permute-start | bytes 196616 | tf_op jit(solution)/shard_map/ppermute | solution.py:18
  15.1 9.2 %collective-permute-start = (bf16[2,80,512]{2,1,0:T(8,128)(2,1)}, bf16[2,80,512]{2,1,0:T(8,128)(2,1)S(1)}, u32[]{:S(2)}, u32[]{:S(2)}) collective-permute-start(bf16[2,80,512]{2,1,0:T(8,128)(2,1)} %get-tuple-element.27), channel_id=1, source_target_pairs={{0,8},{8,16},{16,24},{24,0},{1,9},{9,17},{17,25},{25,1},{2,10},{10... | collective-permute-start | bytes 491528 | tf_op jit(solution)/shard_map/ppermute | solution.py:29
  17.0 12.1 %collective-permute-start.1 = (bf16[2,80,512]{2,1,0:T(8,128)(2,1)}, bf16[2,80,512]{2,1,0:T(8,128)(2,1)S(1)}, u32[]{:S(2)}, u32[]{:S(2)}) collective-permute-start(bf16[2,80,512]{2,1,0:T(8,128)(2,1)} %get-tuple-element.28), channel_id=1, source_target_pairs={{0,16},{8,24},{16,0},{24,8},{1,17},{9,25},{17,1},{25,9},{2,18},{10... | collective-permute-start | bytes 491528 | tf_op jit(solution)/shard_map/ppermute | solution.py:29
  19.6 9.5 %collective-permute-start.2 = (bf16[2,80,512]{2,1,0:T(8,128)(2,1)}, bf16[2,80,512]{2,1,0:T(8,128)(2,1)S(1)}, u32[]{:S(2)}, u32[]{:S(2)}) collective-permute-start(bf16[2,80,512]{2,1,0:T(8,128)(2,1)} %get-tuple-element.29), channel_id=1, source_target_pairs={{0,24},{8,0},{16,8},{24,16},{1,25},{9,1},{17,9},{25,17},{2,26},{10... | collective-permute-start | bytes 491528 | tf_op jit(solution)/shard_map/ppermute | solution.py:29
  29.2 7.8 %collective-permute-start.7 = (bf16[240,512]{1,0:T(8,128)(2,1)S(1)}, bf16[240,512]{1,0:T(8,128)(2,1)S(1)}, u32[]{:S(2)}, u32[]{:S(2)}) collective-permute-start(bf16[240,512]{1,0:T(8,128)(2,1)S(1)} %get-tuple-element.99), channel_id=1, source_target_pairs={{0,4},{4,0},{1,5},{5,1},{2,6},{6,2},{3,7},{7,3},{8,12},{12,8},{9,1... | collective-permute-start | bytes 737288 | tf_op jit(solution)/shard_map/ppermute | solution.py:18
  30.8 7.7 %collective-permute-start.6 = (bf16[240,512]{1,0:T(8,128)(2,1)S(1)}, bf16[240,512]{1,0:T(8,128)(2,1)}, u32[]{:S(2)}, u32[]{:S(2)}) collective-permute-start(bf16[240,512]{1,0:T(8,128)(2,1)S(1)} %get-tuple-element.101), channel_id=1, source_target_pairs={{0,2},{2,0},{1,3},{3,1},{4,6},{6,4},{5,7},{7,5},{8,10},{10,8},{9,1... | collective-permute-start | bytes 737288 | tf_op jit(solution)/shard_map/ppermute | solution.py:18
  32.4 30.7 %collective-permute-start.10 = (bf16[2,2,2,80,512]{4,3,0,2,1:T(8,128)(2,1)S(1)}, bf16[2,2,2,80,512]{4,3,0,2,1:T(8,128)(2,1)}, u32[]{:S(2)}, u32[]{:S(2)}) collective-permute-start(bf16[2,2,2,80,512]{4,3,0,2,1:T(8,128)(2,1)S(1)} %pad_maximum_fusion.2), channel_id=1, source_target_pairs={{0,1},{1,0},{2,3},{3,2},{4,5},{5,4},{6,7},{7,6},{8,9},{9,8},{10,11... | collective-permute-start | bytes 1966088 | tf_op jit(solution)/shard_map/ppermute | solution.py:18
  40.3 22.8 %collective-permute-start.8 = (bf16[2,240,512]{2,1,0:T(8,128)(2,1)}, bf16[2,240,512]{2,1,0:T(8,128)(2,1)}, u32[]{:S(2)}, u32[]{:S(2)}) collective-permute-start(bf16[2,240,512]{2,1,0:T(8,128)(2,1)} %get-tuple-element.91), channel_id=1, source_target_pairs={{0,4},{4,0},{1,5},{5,1},{2,6},{6,2},{3,7},{7,3},{8,12},{12,8},{9,1... | collective-permute-start | bytes 1474568 | tf_op jit(solution)/shard_map/ppermute | solution.py:18
  41.8 21.3 %collective-permute-start.9 = (bf16[2,240,512]{2,1,0:T(8,128)(2,1)}, bf16[2,240,512]{2,1,0:T(8,128)(2,1)}, u32[]{:S(2)}, u32[]{:S(2)}) collective-permute-start(bf16[2,240,512]{2,1,0:T(8,128)(2,1)} %get-tuple-element.89), channel_id=1, source_target_pairs={{0,2},{2,0},{1,3},{3,1},{4,6},{6,4},{5,7},{7,5},{8,10},{10,8},{9,1... | collective-permute-start | bytes 1474568 | tf_op jit(solution)/shard_map/ppermute | solution.py:18
  46.7 8.6 %collective-permute-start.13 = (bf16[2,128,256]{2,1,0:T(8,128)(2,1)}, bf16[2,128,256]{2,1,0:T(8,128)(2,1)S(1)}, u32[]{:S(2)}, u32[]{:S(2)}) collective-permute-start(bf16[2,128,256]{2,1,0:T(8,128)(2,1)} %pad_maximum_fusion.9), channel_id=1, source_target_pairs={{0,24},{8,0},{16,8},{24,16},{1,25},{9,1},{17,9},{25,17},{2,26},{10... | collective-permute-start | bytes 393224 | tf_op jit(solution)/shard_map/ppermute | solution.py:29
  52.2 10.7 %collective-permute-start.12 = (bf16[2,128,256]{2,1,0:T(8,128)(2,1)S(1)}, bf16[2,128,256]{2,1,0:T(8,128)(2,1)S(1)}, u32[]{:S(2)}, u32[]{:S(2)}) collective-permute-start(bf16[2,128,256]{2,1,0:T(8,128)(2,1)S(1)} %copy-done.16), channel_id=1, source_target_pairs={{0,16},{8,24},{16,0},{24,8},{1,17},{9,25},{17,1},{25,9},{2,18},{10... | collective-permute-start | bytes 393224 | tf_op jit(solution)/shard_map/ppermute | solution.py:29
  55.3 7.8 %collective-permute-start.11 = (bf16[2,128,256]{2,1,0:T(8,128)(2,1)S(1)}, bf16[2,128,256]{2,1,0:T(8,128)(2,1)S(1)}, u32[]{:S(2)}, u32[]{:S(2)}) collective-permute-start(bf16[2,128,256]{2,1,0:T(8,128)(2,1)S(1)} %copy-done.16), channel_id=1, source_target_pairs={{0,8},{8,16},{16,24},{24,0},{1,9},{9,17},{17,25},{25,1},{2,10},{10... | collective-permute-start | bytes 393224 | tf_op jit(solution)/shard_map/ppermute | solution.py:29
  64.2 5.9 %collective-permute-start.15 = (bf16[2,2,240,512]{3,2,1,0:T(8,128)(2,1)S(1)}, bf16[2,2,240,512]{3,2,1,0:T(8,128)(2,1)S(1)}, u32[]{:S(2)}, u32[]{:S(2)}) collective-permute-start(bf16[2,2,240,512]{3,2,1,0:T(8,128)(2,1)S(1)} %pad_maximum_fusion), channel_id=1, source_target_pairs={{0,1},{1,0},{2,3},{3,2},{4,5},{5,4},{6,7},{7,6},{8,9},{9,8},{10,11... | collective-permute-start | bytes 2949128 | tf_op jit(solution)/shard_map/ppermute | solution.py:18
  65.4 9.2 %collective-permute-start.14 = (bf16[2,2,240,512]{3,2,0,1:T(8,128)(2,1)S(1)}, bf16[2,2,240,512]{3,2,0,1:T(8,128)(2,1)S(1)}, u32[]{:S(2)}, u32[]{:S(2)}) collective-permute-start(bf16[2,2,240,512]{3,2,0,1:T(8,128)(2,1)S(1)} %pad_maximum_fusion.1), channel_id=1, source_target_pairs={{0,1},{1,0},{2,3},{3,2},{4,5},{5,4},{6,7},{7,6},{8,9},{9,8},{10,11... | collective-permute-start | bytes 2949128 | tf_op jit(solution)/shard_map/ppermute | solution.py:18
  86.3 10.7 %collective-permute-start.17 = (bf16[320,512]{1,0:T(8,128)(2,1)S(1)}, bf16[320,512]{1,0:T(8,128)(2,1)S(1)}, u32[]{:S(2)}, u32[]{:S(2)}) collective-permute-start(bf16[320,512]{1,0:T(8,128)(2,1)S(1)} %get-tuple-element.71), channel_id=1, source_target_pairs={{0,2},{2,0},{1,3},{3,1},{4,6},{6,4},{5,7},{7,5},{8,10},{10,8},{9,1... | collective-permute-start | bytes 983048 | tf_op jit(solution)/shard_map/ppermute | solution.py:18
  86.9 17.6 %collective-permute-start.19 = (bf16[320,512]{1,0:T(8,128)(2,1)S(1)}, bf16[320,512]{1,0:T(8,128)(2,1)S(1)}, u32[]{:S(2)}, u32[]{:S(2)}) collective-permute-start(bf16[320,512]{1,0:T(8,128)(2,1)S(1)} %get-tuple-element.72), channel_id=1, source_target_pairs={{0,6},{2,4},{4,2},{6,0},{1,7},{3,5},{5,3},{7,1},{8,14},{10,12},{12... | collective-permute-start | bytes 983048 | tf_op jit(solution)/shard_map/ppermute | solution.py:22
  89.3 16.6 %collective-permute-start.18 = (bf16[320,512]{1,0:T(8,128)(2,1)S(1)}, bf16[320,512]{1,0:T(8,128)(2,1)S(1)}, u32[]{:S(2)}, u32[]{:S(2)}) collective-permute-start(bf16[320,512]{1,0:T(8,128)(2,1)S(1)} %get-tuple-element.73), channel_id=1, source_target_pairs={{0,4},{4,0},{1,5},{5,1},{2,6},{6,2},{3,7},{7,3},{8,12},{12,8},{9,1... | collective-permute-start | bytes 983048 | tf_op jit(solution)/shard_map/ppermute | solution.py:18
  106.1 6.7 %collective-permute-start.22 = (bf16[80,512]{1,0:T(8,128)(2,1)S(1)}, bf16[80,512]{1,0:T(8,128)(2,1)S(1)}, u32[]{:S(2)}, u32[]{:S(2)}) collective-permute-start(bf16[80,512]{1,0:T(8,128)(2,1)S(1)} %get-tuple-element.93), channel_id=1, source_target_pairs={{0,8},{8,16},{16,24},{24,0},{1,9},{9,17},{17,25},{25,1},{2,10},{10... | collective-permute-start | bytes 245768 | tf_op jit(solution)/shard_map/ppermute | solution.py:29
  108.6 7.0 %collective-permute-start.21 = (bf16[80,512]{1,0:T(8,128)(2,1)S(1)}, bf16[80,512]{1,0:T(8,128)(2,1)S(1)}, u32[]{:S(2)}, u32[]{:S(2)}) collective-permute-start(bf16[80,512]{1,0:T(8,128)(2,1)S(1)} %get-tuple-element.94), channel_id=1, source_target_pairs={{0,16},{8,24},{16,0},{24,8},{1,17},{9,25},{17,1},{25,9},{2,18},{10... | collective-permute-start | bytes 245768 | tf_op jit(solution)/shard_map/ppermute | solution.py:29
  108.6 7.0 %collective-permute-start.20 = (bf16[80,512]{1,0:T(8,128)(2,1)S(1)}, bf16[80,512]{1,0:T(8,128)(2,1)S(1)}, u32[]{:S(2)}, u32[]{:S(2)}) collective-permute-start(bf16[80,512]{1,0:T(8,128)(2,1)S(1)} %get-tuple-element.95), channel_id=1, source_target_pairs={{0,24},{8,0},{16,8},{24,16},{1,25},{9,1},{17,9},{25,17},{2,26},{10... | collective-permute-start | bytes 245768 | tf_op jit(solution)/shard_map/ppermute | solution.py:29
  124.0 13.6 %all-to-all-start = ((bf16[8,64,256]{2,1,0:T(8,128)(2,1)}), bf16[8,64,256]{2,1,0:T(8,128)(2,1)S(1)}, u32[]{:S(2)}, u32[]{:S(2)}) async-start(bf16[8,64,256]{2,1,0:T(8,128)(2,1)} %bitcast.136), calls=%async_computation | async-start | bytes 524288 | tf_op jit(solution)/shard_map/all_to_all | solution.py:242
  129.3 5.9 %collective-permute-start.23 = (bf16[1,256]{1,0:T(2,128)(2,1)S(1)}, bf16[1,256]{1,0:T(2,128)(2,1)S(1)}, u32[]{:S(2)}, u32[]{:S(2)}) collective-permute-start(bf16[1,256]{1,0:T(2,128)(2,1)S(1)} %get-tuple-element.111), channel_id=1, source_target_pairs={{4,0},{8,4},{12,8},{16,12},{20,16},{24,20},{28,24},{5,1},{9,5},{13... | collective-permute-start | bytes 1544 | tf_op jit(solution)/shard_map/ppermute | solution.py:252
  (28 other events, 345.9 us)

commit v3 on v2

--- a/solution.py
+++ b/solution.py
@@ -12,6 +12,7 @@
 epsilon = 1e-06
 F32 = jnp.float32
 BF16 = jnp.bfloat16
+LIMIT = 8 * 2**20
 
 
 def swap(value, axis):
@@ -80,26 +81,139 @@
         sends[step][1] = (share * dot(pick, grad, 1, 0)).astype(BF16)
 
 
-def relative(value, axis, place):
-    width = value.shape[axis] // 4
-    parts = []
-    for dc in range(2):
+def columns(place, step, width):
+    return pl.ds(pl.multiple_of((place ^ step) * width, width), width)
+
+
+def first_half(
+    cap,
+    place_ref,
+    own_ref,
+    own_sib_ref,
+    own_y_ref,
+    own_y_sib_ref,
+    pair_ref,
+    pair_sib_ref,
+    near_own_ref,
+    near_own_sib_ref,
+    near_ref,
+    near_sib_ref,
+    gate_ref,
+    up_ref,
+    down_ref,
+    rows_ref,
+    pre_gate_ref,
+    pre_up_ref,
+    near_out_ref,
+    half_ref,
+):
+    place = place_ref[0]
+    quarter = pair_ref.shape[-1]
+    count = cap + pair_ref.shape[1]
+    sides = (
+        (own_ref, own_y_ref, pair_ref, near_own_ref, near_ref),
+        (own_sib_ref, own_y_sib_ref, pair_sib_ref, near_own_sib_ref, near_sib_ref),
+    )
+    for dc, (own, own_y, pair, near_own, near) in enumerate(sides):
         for dx in range(2):
-            parts.append(
-                lax.dynamic_slice_in_dim(value, (place ^ (2 * dx + dc)) * width, width, axis)
-            )
-    return parts
+            cols = columns(place, 2 * dx + dc, quarter)
+            rows_ref[:cap, cols] = own[dx * cap : (dx + 1) * cap]
+            rows_ref[cap:count, cols] = pair[dx]
+            rows_ref[count:, cols] = own_y[dx * cap : (dx + 1) * cap]
+        cols = slice(dc * quarter, (dc + 1) * quarter)
+        for dj in range(2):
+            near_out_ref[dj * count : dj * count + cap, cols] = near_own[dj]
+            near_out_ref[dj * count + cap : (dj + 1) * count, cols] = near[dj]
+    rows = rows_ref[...]
+    pre_gate_ref[...] = dot(rows, gate_ref[...], 1, 0)
+    pre_up_ref[...] = dot(rows, up_ref[...], 1, 0)
+    half_ref[...] = dot(
+        near_out_ref[:, :quarter], down_ref[:, columns(place, 0, quarter)], 1, 1
+    ) + dot(near_out_ref[:, quarter:], down_ref[:, columns(place, 1, quarter)], 1, 1)
+
+
+def second_half(
+    cap,
+    place_ref,
+    rows_y_ref,
+    rows_y_sib_ref,
+    far_own_ref,
+    far_own_sib_ref,
+    far_ref,
+    far_sib_ref,
+    pre_gate_ref,
+    pre_up_ref,
+    half_ref,
+    gate_ref,
+    up_ref,
+    down_ref,
+    rows_ref,
+    far_out_ref,
+    hidden_ref,
+    d_gate_ref,
+    d_up_ref,
+    away_ref,
+    late_gate_ref,
+    late_up_ref,
+):
+    place = place_ref[0]
+    quarter = far_ref.shape[-1]
+    count = cap + far_ref.shape[1]
+    early = pre_gate_ref.shape[0]
+    sides = ((rows_y_ref, far_own_ref, far_ref), (rows_y_sib_ref, far_own_sib_ref, far_sib_ref))
+    for dc, (rows_y, far_own, far) in enumerate(sides):
+        for dx in range(2):
+            rows_ref[:, columns(place, 2 * dx + dc, quarter)] = rows_y[dx]
+        cols = slice(dc * quarter, (dc + 1) * quarter)
+        for dj in range(2):
+            far_out_ref[dj * count : dj * count + cap, cols] = far_own[dj]
+            far_out_ref[dj * count + cap : (dj + 1) * count, cols] = far[dj]
+    rows = rows_ref[...]
+    late_gate_ref[...] = dot(rows, gate_ref[...], 1, 0)
+    late_up_ref[...] = dot(rows, up_ref[...], 1, 0)
+    for low, high, gate_at, up_at in (
+        (0, early, pre_gate_ref, pre_up_ref),
+        (early, 2 * count, late_gate_ref, late_up_ref),
+    ):
+        part = slice(low, high)
+        d_hidden = half_ref[part] + (
+            dot(far_out_ref[part, :quarter], down_ref[:, columns(place, 2, quarter)], 1, 1)
+            + dot(far_out_ref[part, quarter:], down_ref[:, columns(place, 3, quarter)], 1, 1)
+        )
+        pre_gate, pre_up = gate_at[...], up_at[...]
+        sigmoid_gate = jax.nn.sigmoid(pre_gate)
+        activated = pre_gate * sigmoid_gate
+        hidden_ref[part] = (activated * pre_up).astype(BF16)
+        d_gate_ref[part] = (
+            d_hidden * pre_up * sigmoid_gate * (1.0 + pre_gate * (1.0 - sigmoid_gate))
+        ).astype(BF16)
+        d_up_ref[part] = (d_hidden * activated).astype(BF16)
+    for dx in range(2):
+        block = columns(place, 2 * dx + 1, quarter)
+        away_ref[:, dx * quarter : (dx + 1) * quarter] = (
+            dot(d_gate_ref[...], gate_ref[block], 1, 1) + dot(d_up_ref[...], up_ref[block], 1, 1)
+        ).astype(BF16)
+
+
+def in_vmem(kernel, outs, scratch, flops, scalars, *values):
+    vmem = pl.BlockSpec(memory_space=pltpu.VMEM)
+    return pl.pallas_call(
+        kernel,
+        out_shape=[jax.ShapeDtypeStruct(shape, kind) for shape, kind in outs],
+        in_specs=[pl.BlockSpec(memory_space=pltpu.SMEM)] + [vmem] * len(values),
+        out_specs=[vmem] * len(outs),
+        scratch_shapes=scratch,
+        cost_estimate=pl.CostEstimate(flops=flops, bytes_accessed=0, transcendentals=0),
+        compiler_params=pltpu.CompilerParams(vmem_limit_bytes=LIMIT),
+    )(scalars, *[pltpu.with_memory_space_constraint(v, pltpu.VMEM) for v in values])
 
 
 def absolute(value, axis, place):
     width = value.shape[axis] // 4
-    parts = []
-    for q in range(4):
-        r = place ^ q
-        parts.append(
-            lax.dynamic_slice_in_dim(value, ((r & 1) * 2 + (r >> 1)) * width, width, axis)
-        )
-    return jnp.concatenate(parts, axis=axis)
+    return jnp.concatenate(
+        [lax.dynamic_slice_in_dim(value, (place ^ q) * width, width, axis) for q in range(4)],
+        axis=axis,
+    )
 
 
 def per_device(
@@ -120,20 +234,18 @@
     tokens, features = out_grad.shape
     experts = lax.axis_size("e")
     slices = 2 * experts
-    cap = 5 * tokens // slices
+    cap = -(-(5 * tokens // slices) // 16) * 16
     quarter = features // 4
     mine, half, core = lax.axis_index("e"), lax.axis_index("j"), lax.axis_index("c")
     place = 2 * lax.axis_index("x") + core
-
-    outs = pl.pallas_call(
+    index = jnp.stack([mine, place]).astype(jnp.int32)
+
+    outs = in_vmem(
         functools.partial(prepare, experts, cap, quarter),
-        out_shape=[jax.ShapeDtypeStruct((2, cap, quarter), BF16)] * experts
-        + [jax.ShapeDtypeStruct((experts, cap, tokens), BF16)],
-        in_specs=[pl.BlockSpec(memory_space=pltpu.SMEM)]
-        + [pl.BlockSpec(memory_space=pltpu.VMEM)] * 4,
-        out_specs=[pl.BlockSpec(memory_space=pltpu.VMEM)] * (experts + 1),
-    )(
-        jnp.stack([mine, place]).astype(jnp.int32),
+        [((2, cap, quarter), BF16)] * experts + [((experts, cap, tokens), BF16)],
+        [],
+        4 * experts * cap * tokens * quarter,
+        index,
         routes.T,
         route_weights.T,
         residual,
@@ -143,70 +255,110 @@
     conv_f32 = conv_out.astype(F32)
     gate_f32 = out_gate.astype(F32)
     mixed = (gate_f32 * conv_f32).astype(BF16)
-    mixed_pair = jnp.stack([mixed, swap(mixed, "j")])
+    channels = mixed.shape[1]
+    fold = quarter // channels
+    mixed_rows = tokens // fold
+    mixed_wide = jnp.concatenate(
+        [mixed[i * mixed_rows : (i + 1) * mixed_rows] for i in range(fold)], axis=1
+    )
 
     came = exchange(sends, 1)
-    own_pair = jnp.stack([sends[0], swap(sends[0], "x")])
-    own_four = jnp.stack([own_pair, swap(own_pair, "j")])
-    came, own_four, mixed_pair = lax.optimization_barrier((came, own_four, mixed_pair))
+    own_rows, own_grads = sends[0][0], sends[0][1]
+    own_rows_x, own_grads_y = lax.optimization_barrier((swap(own_rows, "x"), swap(own_grads, "j")))
+    own_pair = jnp.concatenate([own_rows, own_rows_x, mixed_wide], axis=0)
+    own_near = jnp.stack([own_grads, own_grads_y])
+    own_y = swap(own_pair, "j")
+    own_far = swap(own_near, "x")
+    came = lax.optimization_barrier(came)
     rows_z = jnp.concatenate([b[0] for b in came], axis=0)
     grads_z = jnp.concatenate([b[1] for b in came], axis=0)
     count = experts * cap
 
-    rows_x, grads_y = lax.optimization_barrier((swap(rows_z, "x"), swap(grads_z, "j")))
-    rows_pair = jnp.stack([rows_z, rows_x])
-    grads_pair = jnp.stack([grads_z, grads_y])
-    own_sib = swap(own_four, "c")
-    mixed_rel = [mixed_pair] + exchange([mixed_pair] * experts, 1)
-    rows_y, grads_x, own_sib, mixed_rel = lax.optimization_barrier(
-        (swap(rows_pair, "j"), swap(grads_pair, "x"), own_sib, mixed_rel)
-    )
-    rows_four = jnp.stack([rows_pair, rows_y])
-    grads_four = jnp.stack([grads_pair, grads_x], axis=1)
-    rows_sib, grads_sib = swap(rows_four, "c"), swap(grads_four, "c")
-
-    def assemble(which, four, sib):
-        cells = []
-        for own, rest in ((own_four, four), (own_sib, sib)):
-            for dx in range(2):
-                cells.append(jnp.concatenate([own[:, dx, which], rest[:, dx]], axis=1))
-        return jnp.concatenate(cells, axis=-1).reshape(2 * count, features)
-
-    rows = assemble(0, rows_four, rows_sib)
-    grads = assemble(1, grads_four, grads_sib)
-
-    gate_w = jnp.concatenate(relative(w_gate[0], 0, place), axis=0)
-    up_w = jnp.concatenate(relative(w_up[0], 0, place), axis=0)
-    down_w = jnp.concatenate(relative(w_down[0], 1, place), axis=1)
-    pre_gate = dot(rows, gate_w, 1, 0)
-    pre_up = dot(rows, up_w, 1, 0)
-    sigmoid_gate = jax.nn.sigmoid(pre_gate)
-    activated = pre_gate * sigmoid_gate
-    hidden = (activated * pre_up).astype(BF16)
-    d_hidden = dot(grads, down_w, 1, 1)
-    d_gate = (d_hidden * pre_up * sigmoid_gate * (1.0 + pre_gate * (1.0 - sigmoid_gate))).astype(
-        BF16
-    )
-    d_up = (d_hidden * activated).astype(BF16)
-
-    split = features // 2
-    away = dot(d_gate, gate_w[split:], 1, 1) + dot(d_up, up_w[split:], 1, 1)
-    other = swap(away.astype(BF16), "c")
-    kept = dot(d_gate, gate_w[:split], 1, 1) + dot(d_up, up_w[:split], 1, 1)
+    rows_x, grads_y, own_y, own_far = lax.optimization_barrier(
+        (swap(rows_z, "x"), swap(grads_z, "j"), own_y, own_far)
+    )
+    pair = jnp.stack([rows_z, rows_x])
+    near = jnp.stack([grads_z, grads_y])
+    own_far_sib = swap(own_far, "c")
+    rows_y, far, own_far_sib = lax.optimization_barrier(
+        (swap(pair, "j"), swap(near, "x"), own_far_sib)
+    )
+    weights = (w_gate[0], w_up[0], w_down[0])
+    hidden_units = weights[0].shape[1]
+    early = count + cap
+    here = place.reshape(1).astype(jnp.int32)
+    sib = lambda value: (value, swap(value, "c"))
+    rows_early, pre_gate, pre_up, grads_near, d_half = in_vmem(
+        functools.partial(first_half, cap),
+        [
+            ((early, features), BF16),
+            ((early, hidden_units), F32),
+            ((early, hidden_units), F32),
+            ((2 * count, features // 2), BF16),
+            ((2 * count, hidden_units), F32),
+        ],
+        [],
+        (4 * early + 2 * count) * features * hidden_units,
+        here,
+        *sib(own_pair),
+        *sib(own_y),
+        *sib(pair),
+        *sib(own_near),
+        *sib(near),
+        *weights,
+    )
+    rows_late, grads_far, hidden, d_gate, d_up, away = in_vmem(
+        functools.partial(second_half, cap),
+        [
+            ((2 * count - early, features), BF16),
+            ((2 * count, features // 2), BF16),
+            ((2 * count, hidden_units), BF16),
+            ((2 * count, hidden_units), BF16),
+            ((2 * count, hidden_units), BF16),
+            ((2 * count, features // 2), BF16),
+        ],
+        [pltpu.VMEM((2 * count - early, hidden_units), F32)] * 2,
+        (4 * (2 * count - early) + 6 * count) * features * hidden_units,
+        here,
+        *sib(rows_y),
+        own_far,
+        own_far_sib,
+        *sib(far),
+        pre_gate,
+        pre_up,
+        d_half,
+        *weights,
+    )
+
+    keep = lambda value: jnp.concatenate(
+        [
+            lax.dynamic_slice_in_dim(value, (place ^ (2 * dx)) * quarter, quarter, 0)
+            for dx in range(2)
+        ],
+        axis=0,
+    )
+    other = swap(away, "c")
+    kept = dot(d_gate, keep(weights[0]), 1, 1) + dot(d_up, keep(weights[1]), 1, 1)
     total = (kept + other.astype(F32)).astype(BF16)
     block = lambda dj, dx: total[dj * count : (dj + 1) * count, dx * quarter : (dx + 1) * quarter]
+    mixed_mine = jnp.stack([own_pair[2 * cap :], own_y[2 * cap :]])
+    mixed_rel = [mixed_mine] + exchange([mixed_mine] * experts, 1)
     summed = (
         block(0, 0).astype(F32)
         + swap(block(0, 1), "x").astype(F32)
         + swap(block(1, 0), "j").astype(F32)
         + swap_both(block(1, 1)).astype(F32)
     ).astype(BF16)
+    summed, mixed_rel = lax.optimization_barrier((summed, mixed_rel))
     back = [summed[s * cap : (s + 1) * cap] for s in range(experts)]
     back = back[:1] + exchange(back, -1)
 
-    grad_up = dot(rows, d_up, 0, 0).astype(BF16)
-    grad_down = dot(hidden, grads, 0, 0).astype(BF16)
-    grad_up, grad_down = absolute(grad_up, 0, place), absolute(grad_down, 1, place)
+    grad_up = (dot(rows_early, d_up[:early], 0, 0) + dot(rows_late, d_up[early:], 0, 0)).astype(
+        BF16
+    )
+    down_near = dot(hidden, grads_near, 0, 0).astype(BF16)
+    down_far = dot(hidden, grads_far, 0, 0).astype(BF16)
+    grad_down = absolute(jnp.concatenate([down_near, down_far], axis=1), 1, place)
 
     d_part = dot(
         sel.reshape(experts * cap, tokens), jnp.concatenate(back, axis=0), 0, 0
@@ -218,9 +370,8 @@
     row_mean = jnp.mean(unit_rows * d_normed, axis=-1, keepdims=True)
     grad_resid = (out_grad.astype(F32) + inv_rms * (d_normed - unit_rows * row_mean)).astype(BF16)
 
-    mixed_rel = jnp.stack(mixed_rel)
-    channels = mixed.shape[1]
-    mixed_rel = mixed_rel.reshape(slices, tokens, channels)
+    mixed_rel = jnp.stack(mixed_rel).reshape(slices, mixed_rows, fold, channels)
+    mixed_rel = jnp.concatenate([mixed_rel[:, :, i] for i in range(fold)], axis=1)
     mixed_all = jnp.concatenate(
         [
             lax.dynamic_slice_in_dim(

time: 142 us -> 134 us (0.944)
  Pallas kernels: 2.48 us -> 10.1 us
  other arithmetic: 17.2 us -> 9.81 us
  matrix products: 15 us -> 9.78 us
  local copies, waits for them, and re-layouts: 10.4 us -> 7.68 us
    ppermute x9, waiting for transfers between devices: 12.7 us -> 4.23 us  [exchange(): lax.ppermute(b, 'e', [(i, (i + sign * s) % count) for i in range(count)])]
    all_to_all x1, waiting for transfers between devices: 0.46 us -> 8.11 us  [per_device(): lax.all_to_all(blocks, ('e', 'j'), 0, 0, tiled=True)]
    pallas_call x1 -> x3, Pallas kernels: 2.48 us -> 10.1 us  [in_vmem(): pl.pallas_call(kernel, out_shape=[jax.ShapeDtypeStruct(shape, kind) for s...]
    dot_general x13 -> x10, matrix products: 15 us -> 9.78 us  [dot(): lax.dot_general(a, b, (((ca,), (cb,)), ((), ())), preferred_element_type=...]
    another operation x11 -> x9, other arithmetic: 7.49 us -> 2.72 us  [the longest x2 0.87 us: per_device(): pair = jnp.stack([rows_z, rows_x])]
    ppermute x14 -> x20, waiting for transfers between devices: 19 us -> 23.1 us  [swap(): return lax.ppermute(value, axis, [(0, 1), (1, 0)])]
    dynamic_slice x4 -> x1, local copies, waits for them, and re-layouts: 5.44 us -> 1.34 us  [per_device(): lax.dynamic_slice_in_dim(value, (place ^ 2 * dx) * quarter, quarter, 0)]
    all_to_all x1, starting transfers between devices: 4.13 us -> 7.02 us  [per_device(): lax.all_to_all(blocks, ('e', 'j'), 0, 0, tiled=True)]
  transfers between devices with their start and end apart: 27 -> 33, of which waited for: 17 -> 13; matrix products, arithmetic and copies ran while one was open for 20% -> 14% of each run, Pallas kernels for 0% -> 7%
where the time goes in v3:
time: 134 us; the launch traced here: 133 us
  starting transfers between devices  47.5 us (35%)
  waiting for transfers between devices  40.6 us (30%)
  Pallas kernels  10.1 us (8%)
  other arithmetic  9.81 us (7%)
  matrix products  9.78 us (7%)
  local copies, waits for them, and re-layouts  7.68 us (6%)
  blocking collectives  6.63 us (5%)
    ppermute x20, waiting for transfers between devices, swap(): return lax.ppermute(value, axis, [(0, 1), (1, 0)])  23.1 us
    ppermute x9, starting transfers between devices, exchange(): lax.ppermute(b, 'e', [(i, (i + sign * s) % count) for i in range(count)])  19.4 us
    ppermute x20, starting transfers between devices, swap(): return lax.ppermute(value, axis, [(0, 1), (1, 0)])  14.5 us
    pallas_call x3, Pallas kernels, in_vmem(): pl.pallas_call(kernel, out_shape=[jax.ShapeDtypeStruct(shape, kind) for s...  10.1 us
    dot_general x10, matrix products, dot(): lax.dot_general(a, b, (((ca,), (cb,)), ((), ())), preferred_element_type=...  9.78 us
    all_to_all x1, waiting for transfers between devices, per_device(): lax.all_to_all(blocks, ('e', 'j'), 0, 0, tiled=True)  8.11 us
    all_to_all x1, starting transfers between devices, per_device(): lax.all_to_all(blocks, ('e', 'j'), 0, 0, tiled=True)  7.02 us
    all_gather x1, blocking collectives, per_device(): lax.all_gather(d_part, ('x', 'c'), axis=1, tiled=True).astype(F32)  6.63 us
  transfers between devices with their start and end apart: 33, of which 13 were waited for; matrix products, arithmetic and copies ran while one was open for 14% of the time, Pallas kernels for 7%

profile of v3, /device:TPU:0, one launch (start us, length us, event | category | flops | bytes accessed | tf_op | source)
XLA Modules:
  0.0 133.4 jit_solution(7367666820490772522)
XLA Ops:
  6.0 3.0 %collective-permute-start = (bf16[2,80,512]{2,1,0:T(8,128)(2,1)S(1)}, bf16[2,80,512]{2,1,0:T(8,128)(2,1)S(1)}, u32[]{:S(2)}, u32[]{:S(2)}) collective-permute-start(bf16[2,80,512]{2,1,0:T(8,128)(2,1)S(1)} %get-tuple-element.41), channel_id=1, source_target_pairs={{0,8},{8,16},{16,24},{24,0},{1,9},{9,17},{17,25},{25,1},{2,10},{10... | collective-permute-start | bytes 491528 | tf_op jit(solution)/shard_map/ppermute | solution.py:30
  9.0 2.6 %collective-permute-start.1 = (bf16[2,80,512]{2,1,0:T(8,128)(2,1)S(1)}, bf16[2,80,512]{2,1,0:T(8,128)(2,1)S(1)}, u32[]{:S(2)}, u32[]{:S(2)}) collective-permute-start(bf16[2,80,512]{2,1,0:T(8,128)(2,1)S(1)} %get-tuple-element.42), channel_id=1, source_target_pairs={{0,16},{8,24},{16,0},{24,8},{1,17},{9,25},{17,1},{25,9},{2,18},{10... | collective-permute-start | bytes 491528 | tf_op jit(solution)/shard_map/ppermute | solution.py:30
  19.0 1.6 %collective-permute-start.7 = (bf16[224,512]{1,0:T(8,128)(2,1)S(1)}, bf16[224,512]{1,0:T(8,128)(2,1)S(1)}, u32[]{:S(2)}, u32[]{:S(2)}) collective-permute-start(bf16[224,512]{1,0:T(8,128)(2,1)S(1)} %maximum_maximum_fusion.own_ref), channel_id=1, source_target_pairs={{0,4},{4,0},{1,5},{5,1},{2,6},{6,2},{3,7},{7,3},{8,12},{12,8},{9,1... | collective-permute-start | bytes 688136 | tf_op jit(solution)/shard_map/ppermute | solution.py:19
  20.6 1.8 %collective-permute-done.1 = bf16[2,80,512]{2,1,0:T(8,128)(2,1)S(1)} collective-permute-done((bf16[2,80,512]{2,1,0:T(8,128)(2,1)S(1)}, bf16[2,80,512]{2,1,0:T(8,128)(2,1)S(1)}, u32[]{:S(2)}, u32[]{:S(2)}) %collective-permute-start.1) | collective-permute-done | bytes 163872 | tf_op jit(solution)/shard_map/ppermute | solution.py:30
  22.4 1.6 %collective-permute-start.3 = (bf16[240,512]{1,0:T(8,128)(2,1)S(1)}, bf16[240,512]{1,0:T(8,128)(2,1)S(1)}, u32[]{:S(2)}, u32[]{:S(2)}) collective-permute-start(bf16[240,512]{1,0:T(8,128)(2,1)S(1)} %get-tuple-element.97), channel_id=1, source_target_pairs={{0,2},{2,0},{1,3},{3,1},{4,6},{6,4},{5,7},{7,5},{8,10},{10,8},{9,1... | collective-permute-start | bytes 737288 | tf_op jit(solution)/shard_map/ppermute | solution.py:19
  24.0 1.6 %collective-permute-start.4 = (bf16[240,512]{1,0:T(8,128)(2,1)S(1)}, bf16[240,512]{1,0:T(8,128)(2,1)S(1)}, u32[]{:S(2)}, u32[]{:S(2)}) collective-permute-start(bf16[240,512]{1,0:T(8,128)(2,1)S(1)} %get-tuple-element.95), channel_id=1, source_target_pairs={{0,4},{4,0},{1,5},{5,1},{2,6},{6,2},{3,7},{7,3},{8,12},{12,8},{9,1... | collective-permute-start | bytes 737288 | tf_op jit(solution)/shard_map/ppermute | solution.py:19
  26.2 7.7 %collective-permute-done.8.far_own_ref = bf16[2,80,512]{2,1,0:T(8,128)(2,1)} collective-permute-done((bf16[2,80,512]{2,1,0:T(8,128)(2,1)S(1)}, bf16[2,80,512]{2,1,0:T(8,128)(2,1)}, u32[]{:S(2)}, u32[]{:S(2)}) %collective-permute-start.8) | collective-permute-done | bytes 163872 | tf_op jit(solution)/shard_map/ppermute | solution.py:19
  40.7 6.5 %collective-permute-done.9.rows_y_ref = bf16[2,240,512]{2,1,0:T(8,128)(2,1)} collective-permute-done((bf16[2,240,512]{2,1,0:T(8,128)(2,1)}, bf16[2,240,512]{2,1,0:T(8,128)(2,1)}, u32[]{:S(2)}, u32[]{:S(2)}) %collective-permute-start.9) | collective-permute-done | bytes 491552 | tf_op jit(solution)/shard_map/ppermute | solution.py:19
  51.0 4.2 %collective-permute-start.23 = (bf16[2,64,512]{2,1,0:T(8,128)(2,1)S(1)}, bf16[2,64,512]{2,1,0:T(8,128)(2,1)S(1)}, u32[]{:S(2)}, u32[]{:S(2)}) collective-permute-start(bf16[2,64,512]{2,1,0:T(8,128)(2,1)S(1)} %pad_maximum_fusion.6), channel_id=1, source_target_pairs={{0,8},{8,16},{16,24},{24,0},{1,9},{9,17},{17,25},{25,1},{2,10},{10... | collective-permute-start | bytes 393224 | tf_op jit(solution)/shard_map/ppermute | solution.py:30
  55.2 3.9 %shard_map.181 = (bf16[400,2048]{1,0:T(8,128)(2,1)S(1)}, f32[400,512]{1,0:T(8,128)S(1)}, f32[400,512]{1,0:T(8,128)S(1)}, bf16[640,1024]{1,0:T(8,128)(2,1)S(1)}, f32[640,512]{1,0:T(8,128)S(1)}) custom-call(s32[1]{0:T(128)} %bitcast.1.place_ref, bf16[224,512]{1,0:T(8,128)(2,1)S(1)} %maximum_maximum_fusion.own_ref, ...), custom_call_target="tpu_custom_call" | custom-call | flops 2348810240 | tf_op jit(solution)/shard_map/pallas_call | solution.py:200
  59.1 5.2 %shard_map.182 = (bf16[240,2048]{1,0:T(8,128)(2,1)S(1)}, bf16[640,1024]{1,0:T(8,128)(2,1)S(1)}, bf16[640,512]{1,0:T(8,128)(2,1)S(1)}, bf16[640,512]{1,0:T(8,128)...) custom-call(s32[1]{0:T(128)} %bitcast.1.place_ref, ...), custom_call_target="tpu_custom_call" | custom-call | flops 3019898880 | tf_op jit(solution)/shard_map/pallas_call | solution.py:200
  68.9 2.7 %fusion = bf16[1,2048,512]{2,1,0:T(8,128)(2,1)} fusion(f32[2048,512]{1,0:T(8,128)S(1)} %fusion.28, bf16[400,2048]{1,0:T(8,128)(2,1)S(1)} %get-tuple-element.64, bf16[640,512]{1,0:T(8,128)(2,1)S(1)} %get-tuple-element.61), kind=kOutput, calls=%fused_computation.9 | convolution fusion | flops 840957952 | bytes 8339456 | tf_op jit(solution)/shard_map/dot_general | solution.py:42
  72.4 1.9 %collective-permute-start.22 = (bf16[320,512]{1,0:T(8,128)(2,1)S(1)}, bf16[320,512]{1,0:T(8,128)(2,1)S(1)}, u32[]{:S(2)}, u32[]{:S(2)}) collective-permute-start(bf16[320,512]{1,0:T(8,128)(2,1)S(1)} %get-tuple-element.86), channel_id=1, source_target_pairs={{0,6},{2,4},{4,2},{6,0},{1,7},{3,5},{5,3},{7,1},{8,14},{10,12},{12... | collective-permute-start | bytes 983048 | tf_op jit(solution)/shard_map/ppermute | solution.py:23
  77.2 1.6 %maximum_bitcast_fusion = bf16[1,512,2048]{2,1,0:T(8,128)(2,1)} fusion(bf16[512,512]{1,0:T(8,128)(2,1)S(1)} %get-tuple-element.80, bf16[512,512]{1,0:T(8,128)(2,1)S(1)} %get-tuple-element.79, bf16[512,512]{1,0:T(8,128)(2,1)S(1)} %get-tuple-element.78, bf16[512,512]{1,0:T(8,128)(2,1)S(1)} %get-tuple-element.77), kind=kLoop, calls=%fused_computation.11 | loop fusion | flops 8388608 | bytes 4194304 | tf_op jit(solution)/shard_map/broadcast_in_dim | solution.py:412
  78.8 5.2 %collective-permute-done.22 = bf16[320,512]{1,0:T(8,128)(2,1)S(1)} collective-permute-done((bf16[320,512]{1,0:T(8,128)(2,1)S(1)}, bf16[320,512]{1,0:T(8,128)(2,1)S(1)}, u32[]{:S(2)}, u32[]{:S(2)}) %collective-permute-start.22) | collective-permute-done | bytes 327712 | tf_op jit(solution)/shard_map/ppermute | solution.py:23
  84.0 2.4 %collective-permute-start.25 = (bf16[2,64,512]{2,1,0:T(8,128)(2,1)S(1)}, bf16[2,64,512]{2,1,0:T(8,128)(2,1)S(1)}, u32[]{:S(2)}, u32[]{:S(2)}) collective-permute-start(bf16[2,64,512]{2,1,0:T(8,128)(2,1)S(1)} %pad_maximum_fusion.6), channel_id=1, source_target_pairs={{0,24},{8,0},{16,8},{24,16},{1,25},{9,1},{17,9},{25,17},{2,26},{10... | collective-permute-start | bytes 393224 | tf_op jit(solution)/shard_map/ppermute | solution.py:30
  86.4 4.2 %collective-permute-done.21 = bf16[320,512]{1,0:T(8,128)(2,1)S(1)} collective-permute-done((bf16[320,512]{1,0:T(8,128)(2,1)S(1)}, bf16[320,512]{1,0:T(8,128)(2,1)S(1)}, u32[]{:S(2)}, u32[]{:S(2)}) %collective-permute-start.21) | collective-permute-done | bytes 327712 | tf_op jit(solution)/shard_map/ppermute | solution.py:19
  91.0 2.8 %collective-permute-start.27 = (bf16[80,512]{1,0:T(8,128)(2,1)S(1)}, bf16[80,512]{1,0:T(8,128)(2,1)S(1)}, u32[]{:S(2)}, u32[]{:S(2)}) collective-permute-start(bf16[80,512]{1,0:T(8,128)(2,1)S(1)} %get-tuple-element.92), channel_id=1, source_target_pairs={{0,16},{8,24},{16,0},{24,8},{1,17},{9,25},{17,1},{25,9},{2,18},{10... | collective-permute-start | bytes 245768 | tf_op jit(solution)/shard_map/ppermute | solution.py:30
  93.8 2.8 %collective-permute-start.26 = (bf16[80,512]{1,0:T(8,128)(2,1)S(1)}, bf16[80,512]{1,0:T(8,128)(2,1)S(1)}, u32[]{:S(2)}, u32[]{:S(2)}) collective-permute-start(bf16[80,512]{1,0:T(8,128)(2,1)S(1)} %get-tuple-element.93), channel_id=1, source_target_pairs={{0,24},{8,0},{16,8},{24,16},{1,25},{9,1},{17,9},{25,17},{2,26},{10... | collective-permute-start | bytes 245768 | tf_op jit(solution)/shard_map/ppermute | solution.py:30
  98.2 2.4 %collective-permute-done.27 = bf16[80,512]{1,0:T(8,128)(2,1)S(1)} collective-permute-done((bf16[80,512]{1,0:T(8,128)(2,1)S(1)}, bf16[80,512]{1,0:T(8,128)(2,1)S(1)}, u32[]{:S(2)}, u32[]{:S(2)}) %collective-permute-start.27) | collective-permute-done | bytes 81952 | tf_op jit(solution)/shard_map/ppermute | solution.py:30
  100.9 6.6 %all_gather.3 = bf16[128,2048]{1,0:T(8,128)(2,1)S(1)} all-gather(bf16[128,512]{1,0:T(8,128)(2,1)S(1)} %convolution_convert_fusion.2), channel_id=1, replica_groups=mesh['e'=4,'j'=2,'x'=2,'c'=2] {'x','c'}, dimensions={1}, use_global_device_ids=true | all-gather | bytes 655360 | tf_op jit(solution)/shard_map/all_gather | solution.py:366
  109.5 3.4 %collective-permute-start.30 = (bf16[1,256]{1,0:T(2,128)(2,1)S(1)}, bf16[1,256]{1,0:T(2,128)(2,1)S(1)}, u32[]{:S(2)}, u32[]{:S(2)}) collective-permute-start(bf16[1,256]{1,0:T(2,128)(2,1)S(1)} %get-tuple-element.111), channel_id=1, source_target_pairs={{0,4},{4,8},{8,12},{12,16},{16,20},{20,24},{24,28},{1,5},{5,9},{9,... | collective-permute-start | bytes 1544 | tf_op jit(solution)/shard_map/ppermute | solution.py:402
  114.9 7.0 %all-to-all-start = ((bf16[8,64,256]{2,1,0:T(8,128)(2,1)}), bf16[8,64,256]{2,1,0:T(8,128)(2,1)S(1)}, u32[]{:S(2)}, u32[]{:S(2)}) async-start(bf16[8,64,256]{2,1,0:T(8,128)(2,1)} %bitcast.84), calls=%async_computation | async-start | bytes 524288 | tf_op jit(solution)/shard_map/all_to_all | solution.py:393
  122.7 8.1 %all-to-all-done = bf16[8,64,256]{2,1,0:T(8,128)(2,1)S(1)} async-done(((bf16[8,64,256]{2,1,0:T(8,128)(2,1)}), bf16[8,64,256]{2,1,0:T(8,128)(2,1)S(1)}, u32[]{:S(2)}, u32[]{:S(2)}) %all-to-all-start) | async-done | bytes 262176 | tf_op jit(solution)/shard_map/all_to_all | solution.py:393
  (152 shorter events, 41.4 us)
Async XLA Ops:
  6.0 14.6 %collective-permute-start = (bf16[2,80,512]{2,1,0:T(8,128)(2,1)S(1)}, bf16[2,80,512]{2,1,0:T(8,128)(2,1)S(1)}, u32[]{:S(2)}, u32[]{:S(2)}) collective-permute-start(bf16[2,80,512]{2,1,0:T(8,128)(2,1)S(1)} %get-tuple-element.41), channel_id=1, source_target_pairs={{0,8},{8,16},{16,24},{24,0},{1,9},{9,17},{17,25},{25,1},{2,10},{10... | collective-permute-start | bytes 491528 | tf_op jit(solution)/shard_map/ppermute | solution.py:30
  9.0 13.3 %collective-permute-start.1 = (bf16[2,80,512]{2,1,0:T(8,128)(2,1)S(1)}, bf16[2,80,512]{2,1,0:T(8,128)(2,1)S(1)}, u32[]{:S(2)}, u32[]{:S(2)}) collective-permute-start(bf16[2,80,512]{2,1,0:T(8,128)(2,1)S(1)} %get-tuple-element.42), channel_id=1, source_target_pairs={{0,16},{8,24},{16,0},{24,8},{1,17},{9,25},{17,1},{25,9},{2,18},{10... | collective-permute-start | bytes 491528 | tf_op jit(solution)/shard_map/ppermute | solution.py:30
  11.6 10.7 %collective-permute-start.2 = (bf16[2,80,512]{2,1,0:T(8,128)(2,1)S(1)}, bf16[2,80,512]{2,1,0:T(8,128)(2,1)S(1)}, u32[]{:S(2)}, u32[]{:S(2)}) collective-permute-start(bf16[2,80,512]{2,1,0:T(8,128)(2,1)S(1)} %get-tuple-element.43), channel_id=1, source_target_pairs={{0,24},{8,0},{16,8},{24,16},{1,25},{9,1},{17,9},{25,17},{2,26},{10... | collective-permute-start | bytes 491528 | tf_op jit(solution)/shard_map/ppermute | solution.py:30
  19.0 14.9 %collective-permute-start.7 = (bf16[224,512]{1,0:T(8,128)(2,1)S(1)}, bf16[224,512]{1,0:T(8,128)(2,1)S(1)}, u32[]{:S(2)}, u32[]{:S(2)}) collective-permute-start(bf16[224,512]{1,0:T(8,128)(2,1)S(1)} %maximum_maximum_fusion.own_ref), channel_id=1, source_target_pairs={{0,4},{4,0},{1,5},{5,1},{2,6},{6,2},{3,7},{7,3},{8,12},{12,8},{9,1... | collective-permute-start | bytes 688136 | tf_op jit(solution)/shard_map/ppermute | solution.py:19
  22.4 11.5 %collective-permute-start.3 = (bf16[240,512]{1,0:T(8,128)(2,1)S(1)}, bf16[240,512]{1,0:T(8,128)(2,1)S(1)}, u32[]{:S(2)}, u32[]{:S(2)}) collective-permute-start(bf16[240,512]{1,0:T(8,128)(2,1)S(1)} %get-tuple-element.97), channel_id=1, source_target_pairs={{0,2},{2,0},{1,3},{3,1},{4,6},{6,4},{5,7},{7,5},{8,10},{10,8},{9,1... | collective-permute-start | bytes 737288 | tf_op jit(solution)/shard_map/ppermute | solution.py:19
  24.0 9.9 %collective-permute-start.4 = (bf16[240,512]{1,0:T(8,128)(2,1)S(1)}, bf16[240,512]{1,0:T(8,128)(2,1)S(1)}, u32[]{:S(2)}, u32[]{:S(2)}) collective-permute-start(bf16[240,512]{1,0:T(8,128)(2,1)S(1)} %get-tuple-element.95), channel_id=1, source_target_pairs={{0,4},{4,0},{1,5},{5,1},{2,6},{6,2},{3,7},{7,3},{8,12},{12,8},{9,1... | collective-permute-start | bytes 737288 | tf_op jit(solution)/shard_map/ppermute | solution.py:19
  25.6 8.3 %collective-permute-start.8 = (bf16[2,80,512]{2,1,0:T(8,128)(2,1)S(1)}, bf16[2,80,512]{2,1,0:T(8,128)(2,1)}, u32[]{:S(2)}, u32[]{:S(2)}) collective-permute-start(bf16[2,80,512]{2,1,0:T(8,128)(2,1)S(1)} %pad_maximum_fusion.5.near_own_ref), channel_id=1, source_target_pairs={{0,2},{2,0},{1,3},{3,1},{4,6},{6,4},{5,7},{7,5},{8,10},{10,8},{9,1... | collective-permute-start | bytes 491528 | tf_op jit(solution)/shard_map/ppermute | solution.py:19
  34.8 12.5 %collective-permute-start.9 = (bf16[2,240,512]{2,1,0:T(8,128)(2,1)}, bf16[2,240,512]{2,1,0:T(8,128)(2,1)}, u32[]{:S(2)}, u32[]{:S(2)}) collective-permute-start(bf16[2,240,512]{2,1,0:T(8,128)(2,1)} %pad_maximum_fusion.1.pair_ref), channel_id=1, source_target_pairs={{0,4},{4,0},{1,5},{5,1},{2,6},{6,2},{3,7},{7,3},{8,12},{12,8},{9,1... | collective-permute-start | bytes 1474568 | tf_op jit(solution)/shard_map/ppermute | solution.py:19
  37.3 12.2 %collective-permute-start.10 = (bf16[2,240,512]{2,1,0:T(8,128)(2,1)}, bf16[2,240,512]{2,1,0:T(8,128)(2,1)}, u32[]{:S(2)}, u32[]{:S(2)}) collective-permute-start(bf16[2,240,512]{2,1,0:T(8,128)(2,1)} %pad_maximum_fusion.2.near_ref), channel_id=1, source_target_pairs={{0,2},{2,0},{1,3},{3,1},{4,6},{6,4},{5,7},{7,5},{8,10},{10,8},{9,1... | collective-permute-start | bytes 1474568 | tf_op jit(solution)/shard_map/ppermute | solution.py:19
  38.8 11.2 %collective-permute-start.14 = (bf16[224,512]{1,0:T(8,128)(2,1)S(1)}, bf16[224,512]{1,0:T(8,128)(2,1)S(1)}, u32[]{:S(2)}, u32[]{:S(2)}) collective-permute-start(bf16[224,512]{1,0:T(8,128)(2,1)S(1)} %maximum_maximum_fusion.own_ref), channel_id=1, source_target_pairs={{0,1},{1,0},{2,3},{3,2},{4,5},{5,4},{6,7},{7,6},{8,9},{9,8},{10,11... | collective-permute-start | bytes 688136 | tf_op jit(solution)/shard_map/ppermute | solution.py:19
  40.1 9.4 %collective-permute-start.17 = (bf16[2,80,512]{2,1,0:T(8,128)(2,1)S(1)}, bf16[2,80,512]{2,1,0:T(8,128)(2,1)S(1)}, u32[]{:S(2)}, u32[]{:S(2)}) collective-permute-start(bf16[2,80,512]{2,1,0:T(8,128)(2,1)S(1)} %pad_maximum_fusion.5.near_own_ref), channel_id=1, source_target_pairs={{0,1},{1,0},{2,3},{3,2},{4,5},{5,4},{6,7},{7,6},{8,9},{9,8},{10,11... | collective-permute-start | bytes 491528 | tf_op jit(solution)/shard_map/ppermute | solution.py:19
  40.5 14.7 %collective-permute-start.16 = (bf16[2,240,512]{2,1,0:T(8,128)(2,1)}, bf16[2,240,512]{2,1,0:T(8,128)(2,1)S(1)}, u32[]{:S(2)}, u32[]{:S(2)}) collective-permute-start(bf16[2,240,512]{2,1,0:T(8,128)(2,1)} %pad_maximum_fusion.1.pair_ref), channel_id=1, source_target_pairs={{0,1},{1,0},{2,3},{3,2},{4,5},{5,4},{6,7},{7,6},{8,9},{9,8},{10,11... | collective-permute-start | bytes 1474568 | tf_op jit(solution)/shard_map/ppermute | solution.py:19
  47.3 7.9 %collective-permute-start.18 = (bf16[2,240,512]{2,1,0:T(8,128)(2,1)}, bf16[2,240,512]{2,1,0:T(8,128)(2,1)S(1)}, u32[]{:S(2)}, u32[]{:S(2)}) collective-permute-start(bf16[2,240,512]{2,1,0:T(8,128)(2,1)} %pad_maximum_fusion.2.near_ref), channel_id=1, source_target_pairs={{0,1},{1,0},{2,3},{3,2},{4,5},{5,4},{6,7},{7,6},{8,9},{9,8},{10,11... | collective-permute-start | bytes 1474568 | tf_op jit(solution)/shard_map/ppermute | solution.py:19
  49.5 9.5 %collective-permute-start.12 = (bf16[2,240,512]{2,1,0:T(8,128)(2,1)}, bf16[2,240,512]{2,1,0:T(8,128)(2,1)S(1)}, u32[]{:S(2)}, u32[]{:S(2)}) collective-permute-start(bf16[2,240,512]{2,1,0:T(8,128)(2,1)} %collective-permute-done.9.rows_y_ref), channel_id=1, source_target_pairs={{0,1},{1,0},{2,3},{3,2},{4,5},{5,4},{6,7},{7,6},{8,9},{9,8},{10,11... | collective-permute-start | bytes 1474568 | tf_op jit(solution)/shard_map/ppermute | solution.py:19
  50.1 9.0 %collective-permute-start.13 = (bf16[2,240,512]{2,1,0:T(8,128)(2,1)}, bf16[2,240,512]{2,1,0:T(8,128)(2,1)S(1)}, u32[]{:S(2)}, u32[]{:S(2)}) collective-permute-start(bf16[2,240,512]{2,1,0:T(8,128)(2,1)} %collective-permute-done.10.far_ref), channel_id=1, source_target_pairs={{0,1},{1,0},{2,3},{3,2},{4,5},{5,4},{6,7},{7,6},{8,9},{9,8},{10,11... | collective-permute-start | bytes 1474568 | tf_op jit(solution)/shard_map/ppermute | solution.py:19
  51.0 39.7 %collective-permute-start.23 = (bf16[2,64,512]{2,1,0:T(8,128)(2,1)S(1)}, bf16[2,64,512]{2,1,0:T(8,128)(2,1)S(1)}, u32[]{:S(2)}, u32[]{:S(2)}) collective-permute-start(bf16[2,64,512]{2,1,0:T(8,128)(2,1)S(1)} %pad_maximum_fusion.6), channel_id=1, source_target_pairs={{0,8},{8,16},{16,24},{24,0},{1,9},{9,17},{17,25},{25,1},{2,10},{10... | collective-permute-start | bytes 393224 | tf_op jit(solution)/shard_map/ppermute | solution.py:30
  55.2 35.6 %collective-permute-start.24 = (bf16[2,64,512]{2,1,0:T(8,128)(2,1)S(1)}, bf16[2,64,512]{2,1,0:T(8,128)(2,1)S(1)}, u32[]{:S(2)}, u32[]{:S(2)}) collective-permute-start(bf16[2,64,512]{2,1,0:T(8,128)(2,1)S(1)} %pad_maximum_fusion.6), channel_id=1, source_target_pairs={{0,16},{8,24},{16,0},{24,8},{1,17},{9,25},{17,1},{25,9},{2,18},{10... | collective-permute-start | bytes 393224 | tf_op jit(solution)/shard_map/ppermute | solution.py:30
  72.4 11.6 %collective-permute-start.22 = (bf16[320,512]{1,0:T(8,128)(2,1)S(1)}, bf16[320,512]{1,0:T(8,128)(2,1)S(1)}, u32[]{:S(2)}, u32[]{:S(2)}) collective-permute-start(bf16[320,512]{1,0:T(8,128)(2,1)S(1)} %get-tuple-element.86), channel_id=1, source_target_pairs={{0,6},{2,4},{4,2},{6,0},{1,7},{3,5},{5,3},{7,1},{8,14},{10,12},{12... | collective-permute-start | bytes 983048 | tf_op jit(solution)/shard_map/ppermute | solution.py:23
  74.3 16.2 %collective-permute-start.21 = (bf16[320,512]{1,0:T(8,128)(2,1)S(1)}, bf16[320,512]{1,0:T(8,128)(2,1)S(1)}, u32[]{:S(2)}, u32[]{:S(2)}) collective-permute-start(bf16[320,512]{1,0:T(8,128)(2,1)S(1)} %get-tuple-element.87), channel_id=1, source_target_pairs={{0,4},{4,0},{1,5},{5,1},{2,6},{6,2},{3,7},{7,3},{8,12},{12,8},{9,1... | collective-permute-start | bytes 983048 | tf_op jit(solution)/shard_map/ppermute | solution.py:19
  75.5 15.1 %collective-permute-start.20 = (bf16[320,512]{1,0:T(8,128)(2,1)S(1)}, bf16[320,512]{1,0:T(8,128)(2,1)S(1)}, u32[]{:S(2)}, u32[]{:S(2)}) collective-permute-start(bf16[320,512]{1,0:T(8,128)(2,1)S(1)} %get-tuple-element.85), channel_id=1, source_target_pairs={{0,2},{2,0},{1,3},{3,1},{4,6},{6,4},{5,7},{7,5},{8,10},{10,8},{9,1... | collective-permute-start | bytes 983048 | tf_op jit(solution)/shard_map/ppermute | solution.py:19
  91.0 9.6 %collective-permute-start.27 = (bf16[80,512]{1,0:T(8,128)(2,1)S(1)}, bf16[80,512]{1,0:T(8,128)(2,1)S(1)}, u32[]{:S(2)}, u32[]{:S(2)}) collective-permute-start(bf16[80,512]{1,0:T(8,128)(2,1)S(1)} %get-tuple-element.92), channel_id=1, source_target_pairs={{0,16},{8,24},{16,0},{24,8},{1,17},{9,25},{17,1},{25,9},{2,18},{10... | collective-permute-start | bytes 245768 | tf_op jit(solution)/shard_map/ppermute | solution.py:30
  109.5 12.5 %collective-permute-start.30 = (bf16[1,256]{1,0:T(2,128)(2,1)S(1)}, bf16[1,256]{1,0:T(2,128)(2,1)S(1)}, u32[]{:S(2)}, u32[]{:S(2)}) collective-permute-start(bf16[1,256]{1,0:T(2,128)(2,1)S(1)} %get-tuple-element.111), channel_id=1, source_target_pairs={{0,4},{4,8},{8,12},{12,16},{16,20},{20,24},{24,28},{1,5},{5,9},{9,... | collective-permute-start | bytes 1544 | tf_op jit(solution)/shard_map/ppermute | solution.py:402
  112.9 9.1 %collective-permute-start.29 = (bf16[1,256]{1,0:T(2,128)(2,1)S(1)}, bf16[1,256]{1,0:T(2,128)(2,1)S(1)}, u32[]{:S(2)}, u32[]{:S(2)}) collective-permute-start(bf16[1,256]{1,0:T(2,128)(2,1)S(1)} %get-tuple-element.110), channel_id=1, source_target_pairs={{4,0},{8,4},{12,8},{16,12},{20,16},{24,20},{28,24},{5,1},{9,5},{13... | collective-permute-start | bytes 1544 | tf_op jit(solution)/shard_map/ppermute | solution.py:403
  114.9 15.9 %all-to-all-start = ((bf16[8,64,256]{2,1,0:T(8,128)(2,1)}), bf16[8,64,256]{2,1,0:T(8,128)(2,1)S(1)}, u32[]{:S(2)}, u32[]{:S(2)}) async-start(bf16[8,64,256]{2,1,0:T(8,128)(2,1)} %bitcast.84), calls=%async_computation | async-start | bytes 524288 | tf_op jit(solution)/shard_map/all_to_all | solution.py:393
  (32 other events, 350.5 us)

commit v4 on v3

--- a/solution.py
+++ b/solution.py
@@ -12,7 +12,6 @@
 epsilon = 1e-06
 F32 = jnp.float32
 BF16 = jnp.bfloat16
-LIMIT = 8 * 2**20
 
 
 def swap(value, axis):
@@ -195,7 +194,22 @@
         ).astype(BF16)
 
 
-def in_vmem(kernel, outs, scratch, flops, scalars, *values):
+def finish(core_ref, d_normed_ref, resid_ref, grad_ref, out_ref, blocks_ref):
+    d_normed = d_normed_ref[...].astype(F32)
+    resid = resid_ref[...].astype(F32)
+    inv_rms = lax.rsqrt(jnp.mean(resid * resid, axis=-1, keepdims=True) + epsilon)
+    unit = resid * inv_rms
+    row_mean = jnp.mean(unit * d_normed, axis=-1, keepdims=True)
+    out_ref[...] = (
+        grad_ref[...].astype(F32) + inv_rms * (d_normed - unit * row_mean)
+    ).astype(BF16)
+    count, part, width = blocks_ref.shape
+    mine = pl.ds(pl.multiple_of(core_ref[0] * part, part), part)
+    for s in range(count):
+        blocks_ref[s] = out_ref[mine, s * width : (s + 1) * width]
+
+
+def in_vmem(kernel, outs, scratch, flops, limit, scalars, *values):
     vmem = pl.BlockSpec(memory_space=pltpu.VMEM)
     return pl.pallas_call(
         kernel,
@@ -204,8 +218,8 @@
         out_specs=[vmem] * len(outs),
         scratch_shapes=scratch,
         cost_estimate=pl.CostEstimate(flops=flops, bytes_accessed=0, transcendentals=0),
-        compiler_params=pltpu.CompilerParams(vmem_limit_bytes=LIMIT),
-    )(scalars, *[pltpu.with_memory_space_constraint(v, pltpu.VMEM) for v in values])
+        compiler_params=pltpu.CompilerParams(vmem_limit_bytes=limit),
+    )(scalars, *values)
 
 
 def absolute(value, axis, place):
@@ -245,6 +259,7 @@
         [((2, cap, quarter), BF16)] * experts + [((experts, cap, tokens), BF16)],
         [],
         4 * experts * cap * tokens * quarter,
+        60 * 2**20,
         index,
         routes.T,
         route_weights.T,
@@ -280,12 +295,15 @@
     pair = jnp.stack([rows_z, rows_x])
     near = jnp.stack([grads_z, grads_y])
     own_far_sib = swap(own_far, "c")
-    rows_y, far, own_far_sib = lax.optimization_barrier(
-        (swap(pair, "j"), swap(near, "x"), own_far_sib)
+    mixed_mine = jnp.stack([own_pair[2 * cap :], own_y[2 * cap :]])
+    mixed_rel = [mixed_mine] + exchange([mixed_mine] * experts, 1)
+    rows_y, far, own_far_sib, mixed_rel = lax.optimization_barrier(
+        (swap(pair, "j"), swap(near, "x"), own_far_sib, mixed_rel)
     )
     weights = (w_gate[0], w_up[0], w_down[0])
     hidden_units = weights[0].shape[1]
     early = count + cap
+    grant = 7 * 4 * 2 * count * hidden_units
     here = place.reshape(1).astype(jnp.int32)
     sib = lambda value: (value, swap(value, "c"))
     rows_early, pre_gate, pre_up, grads_near, d_half = in_vmem(
@@ -299,6 +317,7 @@
         ],
         [],
         (4 * early + 2 * count) * features * hidden_units,
+        grant,
         here,
         *sib(own_pair),
         *sib(own_y),
@@ -319,6 +338,7 @@
         ],
         [pltpu.VMEM((2 * count - early, hidden_units), F32)] * 2,
         (4 * (2 * count - early) + 6 * count) * features * hidden_units,
+        grant,
         here,
         *sib(rows_y),
         own_far,
@@ -340,16 +360,14 @@
     other = swap(away, "c")
     kept = dot(d_gate, keep(weights[0]), 1, 1) + dot(d_up, keep(weights[1]), 1, 1)
     total = (kept + other.astype(F32)).astype(BF16)
+    total, mixed_rel = lax.optimization_barrier((total, mixed_rel))
     block = lambda dj, dx: total[dj * count : (dj + 1) * count, dx * quarter : (dx + 1) * quarter]
-    mixed_mine = jnp.stack([own_pair[2 * cap :], own_y[2 * cap :]])
-    mixed_rel = [mixed_mine] + exchange([mixed_mine] * experts, 1)
     summed = (
         block(0, 0).astype(F32)
         + swap(block(0, 1), "x").astype(F32)
         + swap(block(1, 0), "j").astype(F32)
         + swap_both(block(1, 1)).astype(F32)
     ).astype(BF16)
-    summed, mixed_rel = lax.optimization_barrier((summed, mixed_rel))
     back = [summed[s * cap : (s + 1) * cap] for s in range(experts)]
     back = back[:1] + exchange(back, -1)
 
@@ -363,15 +381,26 @@
     d_part = dot(
         sel.reshape(experts * cap, tokens), jnp.concatenate(back, axis=0), 0, 0
     ).astype(BF16)
-    d_normed = lax.all_gather(d_part, ("x", "c"), axis=1, tiled=True).astype(F32)
-    resid_f32 = residual.astype(F32)
-    inv_rms = lax.rsqrt(jnp.mean(resid_f32 * resid_f32, axis=-1, keepdims=True) + epsilon)
-    unit_rows = resid_f32 * inv_rms
-    row_mean = jnp.mean(unit_rows * d_normed, axis=-1, keepdims=True)
-    grad_resid = (out_grad.astype(F32) + inv_rms * (d_normed - unit_rows * row_mean)).astype(BF16)
-
-    mixed_rel = jnp.stack(mixed_rel).reshape(slices, mixed_rows, fold, channels)
-    mixed_rel = jnp.concatenate([mixed_rel[:, :, i] for i in range(fold)], axis=1)
+    d_normed = lax.all_gather(d_part, ("x", "c"), axis=1, tiled=True)
+    part = tokens // 2
+    width = features // slices
+    cut = slices if width % 128 == 0 else 1
+    grad_resid, blocks = in_vmem(
+        finish,
+        [((tokens, features), BF16), ((cut, part, features // cut), BF16)],
+        [],
+        16 * tokens * features,
+        8 * 2**20,
+        core.reshape(1).astype(jnp.int32),
+        d_normed,
+        residual,
+        out_grad,
+    )
+
+    mixed_rel = jnp.stack(mixed_rel).reshape(slices, mixed_rows, quarter)
+    mixed_rel = jnp.concatenate(
+        [mixed_rel[:, :, i * channels : (i + 1) * channels] for i in range(fold)], axis=1
+    )
     mixed_all = jnp.concatenate(
         [
             lax.dynamic_slice_in_dim(
@@ -382,14 +411,12 @@
         ],
         axis=0,
     )
-    part = tokens // 2
     ordered = [
         lax.dynamic_slice_in_dim(mixed_all, (core ^ d) * part, part, 1).reshape(-1, channels)
         for d in range(2)
     ]
-    width = features // slices
-    mine_rows = lax.dynamic_slice_in_dim(grad_resid, core * part, part, 0)
-    blocks = jnp.transpose(mine_rows.reshape(part, slices, width), (1, 0, 2))
+    if cut == 1:
+        blocks = jnp.transpose(blocks.reshape(part, slices, width), (1, 0, 2))
     got = lax.all_to_all(blocks, ("e", "j"), 0, 0, tiled=True).reshape(slices * part, width)
     got_sib = swap(got, "c")
     grad_w_out = dot(got, ordered[0], 0, 0) + dot(got_sib, ordered[1], 0, 0)
@@ -399,8 +426,9 @@
     d_conv = d_mix * gate_f32
     edge = d_conv.astype(BF16)
     ends = slices - 1
-    above = lax.ppermute(edge[-1:], ("e", "j"), [(i, i + 1) for i in range(ends)]).astype(F32)
-    below = lax.ppermute(edge[:1], ("e", "j"), [(i + 1, i) for i in range(ends)]).astype(F32)
+    above = lax.ppermute(edge[-1:], ("e", "j"), [(i, i + 1) for i in range(ends)])
+    below = lax.ppermute(edge[:1], ("e", "j"), [(i + 1, i) for i in range(ends)])
+    above, below = above.astype(F32), below.astype(F32)
     later = jnp.concatenate([d_conv[1:], below], axis=0)
     earlier = jnp.concatenate([above, d_conv[:-1]], axis=0)
     d_inner = conv_taps[0] * later + conv_taps[1] * d_conv + conv_taps[2] * earlier

time: 134 us -> 142 us (1.060)
  Pallas kernels: 10.1 us -> 13.5 us
  waiting for transfers between devices: 40.6 us -> 43.4 us
    ppermute x9, waiting for transfers between devices: 4.23 us -> 11.9 us  [exchange(): lax.ppermute(b, 'e', [(i, (i + sign * s) % count) for i in range(count)])]
    ppermute x20, waiting for transfers between devices: 23.1 us -> 15.7 us  [swap(): return lax.ppermute(value, axis, [(0, 1), (1, 0)])]
    pallas_call x3 -> x4, Pallas kernels: 10.1 us -> 13.5 us  [in_vmem(): pl.pallas_call(kernel, out_shape=[jax.ShapeDtypeStruct(shape, kind) for s...]
    ppermute x1, waiting for transfers between devices: 5.19 us -> 7.69 us  [swap_both(): return lax.ppermute(value, ('j', 'x'), [(i, 3 - i) for i in range(4)])]
    ppermute x20, starting transfers between devices: 14.5 us -> 16.7 us  [swap(): return lax.ppermute(value, axis, [(0, 1), (1, 0)])]
    unnamed x48 -> x60, local copies, waits for them, and re-layouts: 4.3 us -> 5.04 us
  transfers between devices with their start and end apart: 33 -> 33, of which waited for: 13 -> 13; matrix products, arithmetic and copies ran while one was open for 14% -> 12% of each run, Pallas kernels for 7% -> 3%
where the time goes in v4:
time: 142 us; the launch traced here: 141 us
  starting transfers between devices  47.2 us (33%)
  waiting for transfers between devices  43.4 us (31%)
  Pallas kernels  13.5 us (10%)
  matrix products  10.9 us (8%)
  other arithmetic  8.94 us (6%)
  local copies, waits for them, and re-layouts  8.8 us (6%)
  blocking collectives  7.35 us (5%)
    ppermute x9, starting transfers between devices, exchange(): lax.ppermute(b, 'e', [(i, (i + sign * s) % count) for i in range(count)])  19.4 us
    ppermute x20, starting transfers between devices, swap(): return lax.ppermute(value, axis, [(0, 1), (1, 0)])  16.7 us
    ppermute x20, waiting for transfers between devices, swap(): return lax.ppermute(value, axis, [(0, 1), (1, 0)])  15.7 us
    pallas_call x4, Pallas kernels, in_vmem(): pl.pallas_call(kernel, out_shape=[jax.ShapeDtypeStruct(shape, kind) for s...  13.5 us
    ppermute x9, waiting for transfers between devices, exchange(): lax.ppermute(b, 'e', [(i, (i + sign * s) % count) for i in range(count)])  11.9 us
    dot_general x10, matrix products, dot(): lax.dot_general(a, b, (((ca,), (cb,)), ((), ())), preferred_element_type=...  10.9 us
    all_to_all x1, waiting for transfers between devices, per_device(): lax.all_to_all(blocks, ('e', 'j'), 0, 0, tiled=True)  8.11 us
    ppermute x1, waiting for transfers between devices, swap_both(): return lax.ppermute(value, ('j', 'x'), [(i, 3 - i) for i in range(4)])  7.69 us
  transfers between devices with their start and end apart: 33, of which 13 were waited for; matrix products, arithmetic and copies ran while one was open for 12% of the time, Pallas kernels for 3%

profile of v4, /device:TPU:0, one launch (start us, length us, event | category | flops | bytes accessed | tf_op | source)
XLA Modules:
  0.0 141.3 jit_solution(2652896214788872470)
XLA Ops:
  1.3 2.5 %shard_map.180 = (bf16[2,80,512]{2,1,0:T(8,128)(2,1)}, bf16[2,80,512]{2,1,0:T(8,128)(2,1)}, bf16[2,80,512]{2,1,0:T(8,128)(2,1)}, bf16[2,80,512]{2,1,0:T(8,128)(2,1)}, bf16[4,80,128]{2,1,0:T(8,128)(2,1)}) custom-call(s32[2]{0:T(128)} %pad_add_fusion.index_ref, s32[2,128]{1,0:T(2,128)} %bitcast.93, f32[2,128]{1,0:T(2,128)} %bitcast.94, ...), custom_call_target="tpu_custom_call" | custom-call | flops 83886080 | tf_op jit(solution)/shard_map/pallas_call | solution.py:214
  3.8 3.1 %collective-permute-start = (bf16[2,80,512]{2,1,0:T(8,128)(2,1)}, bf16[2,80,512]{2,1,0:T(8,128)(2,1)S(1)}, u32[]{:S(2)}, u32[]{:S(2)}) collective-permute-start(bf16[2,80,512]{2,1,0:T(8,128)(2,1)} %get-tuple-element.47), channel_id=1, source_target_pairs={{0,8},{8,16},{16,24},{24,0},{1,9},{9,17},{17,25},{25,1},{2,10},{10... | collective-permute-start | bytes 491528 | tf_op jit(solution)/shard_map/ppermute | solution.py:29
  6.8 2.6 %collective-permute-start.1 = (bf16[2,80,512]{2,1,0:T(8,128)(2,1)}, bf16[2,80,512]{2,1,0:T(8,128)(2,1)S(1)}, u32[]{:S(2)}, u32[]{:S(2)}) collective-permute-start(bf16[2,80,512]{2,1,0:T(8,128)(2,1)} %get-tuple-element.48), channel_id=1, source_target_pairs={{0,16},{8,24},{16,0},{24,8},{1,17},{9,25},{17,1},{25,9},{2,18},{10... | collective-permute-start | bytes 491528 | tf_op jit(solution)/shard_map/ppermute | solution.py:29
  24.3 7.6 %collective-permute-done.8.far_own_ref = bf16[2,80,512]{2,1,0:T(8,128)(2,1)S(1)} collective-permute-done((bf16[2,80,512]{2,1,0:T(8,128)(2,1)S(1)}, bf16[2,80,512]{2,1,0:T(8,128)(2,1)S(1)}, u32[]{:S(2)}, u32[]{:S(2)}) %collective-permute-start.8) | collective-permute-done | bytes 163872 | tf_op jit(solution)/shard_map/ppermute | solution.py:18
  36.7 4.1 %collective-permute-start.12 = (bf16[2,64,512]{2,1,0:T(8,128)(2,1)S(1)}, bf16[2,64,512]{2,1,0:T(8,128)(2,1)S(1)}, u32[]{:S(2)}, u32[]{:S(2)}) collective-permute-start(bf16[2,64,512]{2,1,0:T(8,128)(2,1)S(1)} %pad_maximum_fusion.6), channel_id=1, source_target_pairs={{0,8},{8,16},{16,24},{24,0},{1,9},{9,17},{17,25},{25,1},{2,10},{10... | collective-permute-start | bytes 393224 | tf_op jit(solution)/shard_map/ppermute | solution.py:29
  41.4 1.8 %collective-permute-start.14 = (bf16[2,64,512]{2,1,0:T(8,128)(2,1)S(1)}, bf16[2,64,512]{2,1,0:T(8,128)(2,1)S(1)}, u32[]{:S(2)}, u32[]{:S(2)}) collective-permute-start(bf16[2,64,512]{2,1,0:T(8,128)(2,1)S(1)} %pad_maximum_fusion.6), channel_id=1, source_target_pairs={{0,24},{8,0},{16,8},{24,16},{1,25},{9,1},{17,9},{25,17},{2,26},{10... | collective-permute-start | bytes 393224 | tf_op jit(solution)/shard_map/ppermute | solution.py:29
  43.2 2.0 %collective-permute-done.12 = bf16[2,64,512]{2,1,0:T(8,128)(2,1)S(1)} collective-permute-done((bf16[2,64,512]{2,1,0:T(8,128)(2,1)S(1)}, bf16[2,64,512]{2,1,0:T(8,128)(2,1)S(1)}, u32[]{:S(2)}, u32[]{:S(2)}) %collective-permute-start.12) | collective-permute-done | bytes 131104 | tf_op jit(solution)/shard_map/ppermute | solution.py:29
  45.2 4.2 %collective-permute-done.13 = bf16[2,64,512]{2,1,0:T(8,128)(2,1)S(1)} collective-permute-done((bf16[2,64,512]{2,1,0:T(8,128)(2,1)S(1)}, bf16[2,64,512]{2,1,0:T(8,128)(2,1)S(1)}, u32[]{:S(2)}, u32[]{:S(2)}) %collective-permute-start.13) | collective-permute-done | bytes 131104 | tf_op jit(solution)/shard_map/ppermute | solution.py:29
  52.0 2.6 %dynamic-slice_bitcast_fusion.1 = (bf16[512,512]{1,0:T(8,128)(2,1)}, bf16[512,512]{1,0:T(8,128)(2,1)}, bf16[512,512]{1,0:T(8,128)(2,1)}, bf16[512,512]{1,0:T(8,128)(2,1)}) fusion(bf16[1,2048,512]{2,1,0:T(8,128)(2,1)} %param.18, s32[]{:T(128)S(6)} %select_n.46, s32[]{:T(128)S(6)} %select_n.47, bf16[1,2048,512]{2,1,0:T(8,128)(2,1)S(1)} %copy-done.1), kind=kLoop, calls=%fused_computation.48 | loop fusion | bytes 4194312 | tf_op jit(solution)/shard_map/dynamic_slice | solution.py:355
  58.7 4.4 %shard_map.181 = (bf16[400,2048]{1,0:T(8,128)(2,1)S(1)}, f32[400,512]{1,0:T(8,128)S(1)}, f32[400,512]{1,0:T(8,128)S(1)}, bf16[640,1024]{1,0:T(8,128)(2,1)S(1)}, f32[640,512]{1,0:T(8,128)S(1)}) custom-call(s32[1]{0:T(128)} %bitcast.2.place_ref, bf16[224,512]{1,0:T(8,128)(2,1)S(1)} %maximum_maximum_fusion.own_ref, ...), custom_call_target="tpu_custom_call" | custom-call | flops 2348810240 | tf_op jit(solution)/shard_map/pallas_call | solution.py:214
  63.1 5.2 %shard_map.182 = (bf16[240,2048]{1,0:T(8,128)(2,1)S(1)}, bf16[640,1024]{1,0:T(8,128)(2,1)S(1)}, bf16[640,512]{1,0:T(8,128)(2,1)S(1)}, bf16[640,512]{1,0:T(8,128)...) custom-call(s32[1]{0:T(128)} %bitcast.2.place_ref, ...), custom_call_target="tpu_custom_call" | custom-call | flops 3019898880 | tf_op jit(solution)/shard_map/pallas_call | solution.py:214
  73.2 1.6 %maximum_bitcast_fusion = bf16[1,512,2048]{2,1,0:T(8,128)(2,1)} fusion(bf16[512,512]{1,0:T(8,128)(2,1)S(1)} %get-tuple-element.92, bf16[512,512]{1,0:T(8,128)(2,1)S(1)} %get-tuple-element.91, bf16[512,512]{1,0:T(8,128)(2,1)S(1)} %get-tuple-element.90, bf16[512,512]{1,0:T(8,128)(2,1)S(1)} %get-tuple-element.89), kind=kLoop, calls=%fused_computation.11 | loop fusion | flops 8388608 | bytes 4194304 | tf_op jit(solution)/shard_map/broadcast_in_dim | solution.py:440
  76.5 2.7 %fusion = bf16[1,2048,512]{2,1,0:T(8,128)(2,1)} fusion(f32[2048,512]{1,0:T(8,128)S(1)} %fusion.22, bf16[400,2048]{1,0:T(8,128)(2,1)S(1)} %get-tuple-element.75, bf16[640,512]{1,0:T(8,128)(2,1)S(1)} %get-tuple-element.67), kind=kOutput, calls=%fused_computation.9 | convolution fusion | flops 840957952 | bytes 8339456 | tf_op jit(solution)/shard_map/dot_general | solution.py:41
  84.2 7.7 %collective-permute-done.25 = bf16[320,512]{1,0:T(8,128)(2,1)S(1)} collective-permute-done((bf16[320,512]{1,0:T(8,128)(2,1)S(1)}, bf16[320,512]{1,0:T(8,128)(2,1)S(1)}, u32[]{:S(2)}, u32[]{:S(2)}) %collective-permute-start.25) | collective-permute-done | bytes 327712 | tf_op jit(solution)/shard_map/ppermute | solution.py:22
  91.9 5.4 %collective-permute-done.24 = bf16[320,512]{1,0:T(8,128)(2,1)S(1)} collective-permute-done((bf16[320,512]{1,0:T(8,128)(2,1)S(1)}, bf16[320,512]{1,0:T(8,128)(2,1)S(1)}, u32[]{:S(2)}, u32[]{:S(2)}) %collective-permute-start.24) | collective-permute-done | bytes 327712 | tf_op jit(solution)/shard_map/ppermute | solution.py:18
  97.6 3.1 %collective-permute-start.28 = (bf16[80,512]{1,0:T(8,128)(2,1)S(1)}, bf16[80,512]{1,0:T(8,128)(2,1)S(1)}, u32[]{:S(2)}, u32[]{:S(2)}) collective-permute-start(bf16[80,512]{1,0:T(8,128)(2,1)S(1)} %get-tuple-element.103), channel_id=1, source_target_pairs={{0,8},{8,16},{16,24},{24,0},{1,9},{9,17},{17,25},{25,1},{2,10},{10... | collective-permute-start | bytes 245768 | tf_op jit(solution)/shard_map/ppermute | solution.py:29
  100.7 1.8 %collective-permute-start.27 = (bf16[80,512]{1,0:T(8,128)(2,1)S(1)}, bf16[80,512]{1,0:T(8,128)(2,1)S(1)}, u32[]{:S(2)}, u32[]{:S(2)}) collective-permute-start(bf16[80,512]{1,0:T(8,128)(2,1)S(1)} %get-tuple-element.104), channel_id=1, source_target_pairs={{0,16},{8,24},{16,0},{24,8},{1,17},{9,25},{17,1},{25,9},{2,18},{10... | collective-permute-start | bytes 245768 | tf_op jit(solution)/shard_map/ppermute | solution.py:29
  103.5 1.7 %collective-permute-done.28 = bf16[80,512]{1,0:T(8,128)(2,1)S(1)} collective-permute-done((bf16[80,512]{1,0:T(8,128)(2,1)S(1)}, bf16[80,512]{1,0:T(8,128)(2,1)S(1)}, u32[]{:S(2)}, u32[]{:S(2)}) %collective-permute-start.28) | collective-permute-done | bytes 81952 | tf_op jit(solution)/shard_map/ppermute | solution.py:29
  105.2 2.6 %collective-permute-done.27 = bf16[80,512]{1,0:T(8,128)(2,1)S(1)} collective-permute-done((bf16[80,512]{1,0:T(8,128)(2,1)S(1)}, bf16[80,512]{1,0:T(8,128)(2,1)S(1)}, u32[]{:S(2)}, u32[]{:S(2)}) %collective-permute-start.27) | collective-permute-done | bytes 81952 | tf_op jit(solution)/shard_map/ppermute | solution.py:29
  108.3 7.4 %all_gather.3.d_normed_ref = bf16[128,2048]{1,0:T(8,128)(2,1)S(1)} all-gather(bf16[128,512]{1,0:T(8,128)(2,1)S(1)} %convolution_convert_fusion.2), channel_id=1, replica_groups=mesh['e'=4,'j'=2,'x'=2,'c'=2] {'x','c'}, dimensions={1}, use_global_device_ids=true | all-gather | bytes 655360 | tf_op jit(solution)/shard_map/all_gather | solution.py:384
  117.1 2.2 %fusion.51 = (bf16[128,256]{1,0:T(8,128)(2,1)S(1)}, f32[128,256]{1,0:T(8,128)S(1)}, bf16[128,256]{1,0:T(8,128)(2,1)}) fusion(bf16[128,256]{1,0:T(8,128)(2,1)S(1)} %copy-done.19, bf16[128,256]{1,0:T(8,128)(2,1)S(1)} %copy-done.18, bf16[128,2048]{1,0:T(8,128)(2,1)} %get-tuple-element.39, bf16[256,2048]{1,0:T(8,128)(2,1)S(1)} %copy-done), kind=kOutput, calls=%fused_computation.114 | convolution fusion | flops 134414336 | bytes 1966080 | tf_op jit(solution)/shard_map/dot_general | solution.py:41
  119.3 2.7 %collective-permute-start.30 = (bf16[1,256]{1,0:T(2,128)(2,1)S(1)}, bf16[1,256]{1,0:T(2,128)(2,1)S(1)}, u32[]{:S(2)}, u32[]{:S(2)}) collective-permute-start(bf16[1,256]{1,0:T(2,128)(2,1)S(1)} %get-tuple-element.123), channel_id=1, source_target_pairs={{0,4},{4,8},{8,12},{12,16},{16,20},{20,24},{24,28},{1,5},{5,9},{9,... | collective-permute-start | bytes 1544 | tf_op jit(solution)/shard_map/ppermute | solution.py:429
  123.3 6.6 %all-to-all-start = ((bf16[8,64,256]{2,1,0:T(8,128)(2,1)}), bf16[8,64,256]{2,1,0:T(8,128)(2,1)S(1)}, u32[]{:S(2)}, u32[]{:S(2)}) async-start(bf16[8,64,256]{2,1,0:T(8,128)(2,1)} %get-tuple-element.80), calls=%async_computation | async-start | bytes 524288 | tf_op jit(solution)/shard_map/all_to_all | solution.py:420
  130.7 8.1 %all-to-all-done = bf16[8,64,256]{2,1,0:T(8,128)(2,1)S(1)} async-done(((bf16[8,64,256]{2,1,0:T(8,128)(2,1)}), bf16[8,64,256]{2,1,0:T(8,128)(2,1)S(1)}, u32[]{:S(2)}, u32[]{:S(2)}) %all-to-all-start) | async-done | bytes 262176 | tf_op jit(solution)/shard_map/all_to_all | solution.py:420
  (157 shorter events, 46.2 us)
Async XLA Ops:
  3.8 15.5 %collective-permute-start = (bf16[2,80,512]{2,1,0:T(8,128)(2,1)}, bf16[2,80,512]{2,1,0:T(8,128)(2,1)S(1)}, u32[]{:S(2)}, u32[]{:S(2)}) collective-permute-start(bf16[2,80,512]{2,1,0:T(8,128)(2,1)} %get-tuple-element.47), channel_id=1, source_target_pairs={{0,8},{8,16},{16,24},{24,0},{1,9},{9,17},{17,25},{25,1},{2,10},{10... | collective-permute-start | bytes 491528 | tf_op jit(solution)/shard_map/ppermute | solution.py:29
  6.8 13.5 %collective-permute-start.1 = (bf16[2,80,512]{2,1,0:T(8,128)(2,1)}, bf16[2,80,512]{2,1,0:T(8,128)(2,1)S(1)}, u32[]{:S(2)}, u32[]{:S(2)}) collective-permute-start(bf16[2,80,512]{2,1,0:T(8,128)(2,1)} %get-tuple-element.48), channel_id=1, source_target_pairs={{0,16},{8,24},{16,0},{24,8},{1,17},{9,25},{17,1},{25,9},{2,18},{10... | collective-permute-start | bytes 491528 | tf_op jit(solution)/shard_map/ppermute | solution.py:29
  9.4 11.0 %collective-permute-start.2 = (bf16[2,80,512]{2,1,0:T(8,128)(2,1)}, bf16[2,80,512]{2,1,0:T(8,128)(2,1)S(1)}, u32[]{:S(2)}, u32[]{:S(2)}) collective-permute-start(bf16[2,80,512]{2,1,0:T(8,128)(2,1)} %get-tuple-element.49), channel_id=1, source_target_pairs={{0,24},{8,0},{16,8},{24,16},{1,25},{9,1},{17,9},{25,17},{2,26},{10... | collective-permute-start | bytes 491528 | tf_op jit(solution)/shard_map/ppermute | solution.py:29
  17.7 14.1 %collective-permute-start.7 = (bf16[224,512]{1,0:T(8,128)(2,1)S(1)}, bf16[224,512]{1,0:T(8,128)(2,1)S(1)}, u32[]{:S(2)}, u32[]{:S(2)}) collective-permute-start(bf16[224,512]{1,0:T(8,128)(2,1)S(1)} %maximum_maximum_fusion.own_ref), channel_id=1, source_target_pairs={{0,4},{4,0},{1,5},{5,1},{2,6},{6,2},{3,7},{7,3},{8,12},{12,8},{9,1... | collective-permute-start | bytes 688136 | tf_op jit(solution)/shard_map/ppermute | solution.py:18
  20.5 11.4 %collective-permute-start.3 = (bf16[240,512]{1,0:T(8,128)(2,1)S(1)}, bf16[240,512]{1,0:T(8,128)(2,1)S(1)}, u32[]{:S(2)}, u32[]{:S(2)}) collective-permute-start(bf16[240,512]{1,0:T(8,128)(2,1)S(1)} %get-tuple-element.109), channel_id=1, source_target_pairs={{0,2},{2,0},{1,3},{3,1},{4,6},{6,4},{5,7},{7,5},{8,10},{10,8},{9,1... | collective-permute-start | bytes 737288 | tf_op jit(solution)/shard_map/ppermute | solution.py:18
  22.1 9.8 %collective-permute-start.4 = (bf16[240,512]{1,0:T(8,128)(2,1)S(1)}, bf16[240,512]{1,0:T(8,128)(2,1)S(1)}, u32[]{:S(2)}, u32[]{:S(2)}) collective-permute-start(bf16[240,512]{1,0:T(8,128)(2,1)S(1)} %get-tuple-element.107), channel_id=1, source_target_pairs={{0,4},{4,0},{1,5},{5,1},{2,6},{6,2},{3,7},{7,3},{8,12},{12,8},{9,1... | collective-permute-start | bytes 737288 | tf_op jit(solution)/shard_map/ppermute | solution.py:18
  23.7 8.2 %collective-permute-start.8 = (bf16[2,80,512]{2,1,0:T(8,128)(2,1)S(1)}, bf16[2,80,512]{2,1,0:T(8,128)(2,1)S(1)}, u32[]{:S(2)}, u32[]{:S(2)}) collective-permute-start(bf16[2,80,512]{2,1,0:T(8,128)(2,1)S(1)} %pad_maximum_fusion.5.near_own_ref), channel_id=1, source_target_pairs={{0,2},{2,0},{1,3},{3,1},{4,6},{6,4},{5,7},{7,5},{8,10},{10,8},{9,1... | collective-permute-start | bytes 491528 | tf_op jit(solution)/shard_map/ppermute | solution.py:18
  32.8 18.0 %collective-permute-start.9 = (bf16[2,240,512]{2,1,0:T(8,128)(2,1)}, bf16[2,240,512]{2,1,0:T(8,128)(2,1)}, u32[]{:S(2)}, u32[]{:S(2)}) collective-permute-start(bf16[2,240,512]{2,1,0:T(8,128)(2,1)} %pad_maximum_fusion.1.pair_ref), channel_id=1, source_target_pairs={{0,4},{4,0},{1,5},{5,1},{2,6},{6,2},{3,7},{7,3},{8,12},{12,8},{9,1... | collective-permute-start | bytes 1474568 | tf_op jit(solution)/shard_map/ppermute | solution.py:18
  35.1 16.2 %collective-permute-start.10 = (bf16[2,240,512]{2,1,0:T(8,128)(2,1)}, bf16[2,240,512]{2,1,0:T(8,128)(2,1)}, u32[]{:S(2)}, u32[]{:S(2)}) collective-permute-start(bf16[2,240,512]{2,1,0:T(8,128)(2,1)} %pad_maximum_fusion.2.near_ref), channel_id=1, source_target_pairs={{0,2},{2,0},{1,3},{3,1},{4,6},{6,4},{5,7},{7,5},{8,10},{10,8},{9,1... | collective-permute-start | bytes 1474568 | tf_op jit(solution)/shard_map/ppermute | solution.py:18
  36.7 8.6 %collective-permute-start.12 = (bf16[2,64,512]{2,1,0:T(8,128)(2,1)S(1)}, bf16[2,64,512]{2,1,0:T(8,128)(2,1)S(1)}, u32[]{:S(2)}, u32[]{:S(2)}) collective-permute-start(bf16[2,64,512]{2,1,0:T(8,128)(2,1)S(1)} %pad_maximum_fusion.6), channel_id=1, source_target_pairs={{0,8},{8,16},{16,24},{24,0},{1,9},{9,17},{17,25},{25,1},{2,10},{10... | collective-permute-start | bytes 393224 | tf_op jit(solution)/shard_map/ppermute | solution.py:29
  40.8 8.7 %collective-permute-start.13 = (bf16[2,64,512]{2,1,0:T(8,128)(2,1)S(1)}, bf16[2,64,512]{2,1,0:T(8,128)(2,1)S(1)}, u32[]{:S(2)}, u32[]{:S(2)}) collective-permute-start(bf16[2,64,512]{2,1,0:T(8,128)(2,1)S(1)} %pad_maximum_fusion.6), channel_id=1, source_target_pairs={{0,16},{8,24},{16,0},{24,8},{1,17},{9,25},{17,1},{25,9},{2,18},{10... | collective-permute-start | bytes 393224 | tf_op jit(solution)/shard_map/ppermute | solution.py:29
  41.4 8.1 %collective-permute-start.14 = (bf16[2,64,512]{2,1,0:T(8,128)(2,1)S(1)}, bf16[2,64,512]{2,1,0:T(8,128)(2,1)S(1)}, u32[]{:S(2)}, u32[]{:S(2)}) collective-permute-start(bf16[2,64,512]{2,1,0:T(8,128)(2,1)S(1)} %pad_maximum_fusion.6), channel_id=1, source_target_pairs={{0,24},{8,0},{16,8},{24,16},{1,25},{9,1},{17,9},{25,17},{2,26},{10... | collective-permute-start | bytes 393224 | tf_op jit(solution)/shard_map/ppermute | solution.py:29
  51.4 11.7 %collective-permute-start.15 = (bf16[2,240,512]{2,1,0:T(8,128)(2,1)}, bf16[2,240,512]{2,1,0:T(8,128)(2,1)}, u32[]{:S(2)}, u32[]{:S(2)}) collective-permute-start(bf16[2,240,512]{2,1,0:T(8,128)(2,1)} %collective-permute-done.9.rows_y_ref), channel_id=1, source_target_pairs={{0,1},{1,0},{2,3},{3,2},{4,5},{5,4},{6,7},{7,6},{8,9},{9,8},{10,11... | collective-permute-start | bytes 1474568 | tf_op jit(solution)/shard_map/ppermute | solution.py:18
  51.9 11.3 %collective-permute-start.16 = (bf16[2,240,512]{2,1,0:T(8,128)(2,1)}, bf16[2,240,512]{2,1,0:T(8,128)(2,1)}, u32[]{:S(2)}, u32[]{:S(2)}) collective-permute-start(bf16[2,240,512]{2,1,0:T(8,128)(2,1)} %collective-permute-done.10.far_ref), channel_id=1, source_target_pairs={{0,1},{1,0},{2,3},{3,2},{4,5},{5,4},{6,7},{7,6},{8,9},{9,8},{10,11... | collective-permute-start | bytes 1474568 | tf_op jit(solution)/shard_map/ppermute | solution.py:18
  68.4 10.9 %collective-permute-start.22 = (bf16[640,1024]{1,0:T(8,128)(2,1)S(1)}, bf16[640,1024]{1,0:T(8,128)(2,1)S(1)}, u32[]{:S(2)}, u32[]{:S(2)}) collective-permute-start(bf16[640,1024]{1,0:T(8,128)(2,1)S(1)} %get-tuple-element.68), channel_id=1, source_target_pairs={{0,1},{1,0},{2,3},{3,2},{4,5},{5,4},{6,7},{7,6},{8,9},{9,8},{10,11... | collective-permute-start | bytes 3932168 | tf_op jit(solution)/shard_map/ppermute | solution.py:18
  80.3 11.6 %collective-permute-start.25 = (bf16[320,512]{1,0:T(8,128)(2,1)S(1)}, bf16[320,512]{1,0:T(8,128)(2,1)S(1)}, u32[]{:S(2)}, u32[]{:S(2)}) collective-permute-start(bf16[320,512]{1,0:T(8,128)(2,1)S(1)} %get-tuple-element.98), channel_id=1, source_target_pairs={{0,6},{2,4},{4,2},{6,0},{1,7},{3,5},{5,3},{7,1},{8,14},{10,12},{12... | collective-permute-start | bytes 983048 | tf_op jit(solution)/shard_map/ppermute | solution.py:22
  80.8 16.5 %collective-permute-start.24 = (bf16[320,512]{1,0:T(8,128)(2,1)S(1)}, bf16[320,512]{1,0:T(8,128)(2,1)S(1)}, u32[]{:S(2)}, u32[]{:S(2)}) collective-permute-start(bf16[320,512]{1,0:T(8,128)(2,1)S(1)} %get-tuple-element.99), channel_id=1, source_target_pairs={{0,4},{4,0},{1,5},{5,1},{2,6},{6,2},{3,7},{7,3},{8,12},{12,8},{9,1... | collective-permute-start | bytes 983048 | tf_op jit(solution)/shard_map/ppermute | solution.py:18
  82.3 15.0 %collective-permute-start.23 = (bf16[320,512]{1,0:T(8,128)(2,1)S(1)}, bf16[320,512]{1,0:T(8,128)(2,1)S(1)}, u32[]{:S(2)}, u32[]{:S(2)}) collective-permute-start(bf16[320,512]{1,0:T(8,128)(2,1)S(1)} %get-tuple-element.97), channel_id=1, source_target_pairs={{0,2},{2,0},{1,3},{3,1},{4,6},{6,4},{5,7},{7,5},{8,10},{10,8},{9,1... | collective-permute-start | bytes 983048 | tf_op jit(solution)/shard_map/ppermute | solution.py:18
  97.6 7.6 %collective-permute-start.28 = (bf16[80,512]{1,0:T(8,128)(2,1)S(1)}, bf16[80,512]{1,0:T(8,128)(2,1)S(1)}, u32[]{:S(2)}, u32[]{:S(2)}) collective-permute-start(bf16[80,512]{1,0:T(8,128)(2,1)S(1)} %get-tuple-element.103), channel_id=1, source_target_pairs={{0,8},{8,16},{16,24},{24,0},{1,9},{9,17},{17,25},{25,1},{2,10},{10... | collective-permute-start | bytes 245768 | tf_op jit(solution)/shard_map/ppermute | solution.py:29
  100.7 7.1 %collective-permute-start.27 = (bf16[80,512]{1,0:T(8,128)(2,1)S(1)}, bf16[80,512]{1,0:T(8,128)(2,1)S(1)}, u32[]{:S(2)}, u32[]{:S(2)}) collective-permute-start(bf16[80,512]{1,0:T(8,128)(2,1)S(1)} %get-tuple-element.104), channel_id=1, source_target_pairs={{0,16},{8,24},{16,0},{24,8},{1,17},{9,25},{17,1},{25,9},{2,18},{10... | collective-permute-start | bytes 245768 | tf_op jit(solution)/shard_map/ppermute | solution.py:29
  102.6 5.5 %collective-permute-start.26 = (bf16[80,512]{1,0:T(8,128)(2,1)S(1)}, bf16[80,512]{1,0:T(8,128)(2,1)S(1)}, u32[]{:S(2)}, u32[]{:S(2)}) collective-permute-start(bf16[80,512]{1,0:T(8,128)(2,1)S(1)} %get-tuple-element.105), channel_id=1, source_target_pairs={{0,24},{8,0},{16,8},{24,16},{1,25},{9,1},{17,9},{25,17},{2,26},{10... | collective-permute-start | bytes 245768 | tf_op jit(solution)/shard_map/ppermute | solution.py:29
  119.3 10.7 %collective-permute-start.30 = (bf16[1,256]{1,0:T(2,128)(2,1)S(1)}, bf16[1,256]{1,0:T(2,128)(2,1)S(1)}, u32[]{:S(2)}, u32[]{:S(2)}) collective-permute-start(bf16[1,256]{1,0:T(2,128)(2,1)S(1)} %get-tuple-element.123), channel_id=1, source_target_pairs={{0,4},{4,8},{8,12},{12,16},{16,20},{20,24},{24,28},{1,5},{5,9},{9,... | collective-permute-start | bytes 1544 | tf_op jit(solution)/shard_map/ppermute | solution.py:429
  122.0 8.0 %collective-permute-start.29 = (bf16[1,256]{1,0:T(2,128)(2,1)S(1)}, bf16[1,256]{1,0:T(2,128)(2,1)S(1)}, u32[]{:S(2)}, u32[]{:S(2)}) collective-permute-start(bf16[1,256]{1,0:T(2,128)(2,1)S(1)} %get-tuple-element.122), channel_id=1, source_target_pairs={{4,0},{8,4},{12,8},{16,12},{20,16},{24,20},{28,24},{5,1},{9,5},{13... | collective-permute-start | bytes 1544 | tf_op jit(solution)/shard_map/ppermute | solution.py:430
  123.3 15.5 %all-to-all-start = ((bf16[8,64,256]{2,1,0:T(8,128)(2,1)}), bf16[8,64,256]{2,1,0:T(8,128)(2,1)S(1)}, u32[]{:S(2)}, u32[]{:S(2)}) async-start(bf16[8,64,256]{2,1,0:T(8,128)(2,1)} %get-tuple-element.80), calls=%async_computation | async-start | bytes 524288 | tf_op jit(solution)/shard_map/all_to_all | solution.py:420
  (39 other events, 438.3 us)

commit v5 on v4

--- a/solution.py
+++ b/solution.py
@@ -106,7 +106,7 @@
     near_out_ref,
     half_ref,
 ):
-    place = place_ref[0]
+    place = place_ref[1]
     quarter = pair_ref.shape[-1]
     count = cap + pair_ref.shape[1]
     sides = (
@@ -155,7 +155,7 @@
     late_gate_ref,
     late_up_ref,
 ):
-    place = place_ref[0]
+    place = place_ref[1]
     quarter = far_ref.shape[-1]
     count = cap + far_ref.shape[1]
     early = pre_gate_ref.shape[0]
@@ -194,6 +194,59 @@
         ).astype(BF16)
 
 
+def kept_part(place_ref, d_gate_ref, d_up_ref, gate_ref, up_ref, kept_ref):
+    place = place_ref[1]
+    quarter = kept_ref.shape[1] // 2
+    for dx in range(2):
+        block = columns(place, 2 * dx, quarter)
+        kept_ref[:, dx * quarter : (dx + 1) * quarter] = dot(
+            d_gate_ref[...], gate_ref[block], 1, 1
+        ) + dot(d_up_ref[...], up_ref[block], 1, 1)
+
+
+def join(place_ref, kept_ref, other_ref, *block_refs):
+    count, quarter = block_refs[0].shape
+    for i, block_ref in enumerate(block_refs):
+        rows, cols = divmod(i, 2)
+        rows = slice(rows * count, (rows + 1) * count)
+        cols = slice(cols * quarter, (cols + 1) * quarter)
+        block_ref[...] = (kept_ref[rows, cols] + other_ref[rows, cols].astype(F32)).astype(BF16)
+
+
+def weight_grads(
+    place_ref, early_ref, late_ref, near_ref, far_ref, hidden_ref, d_up_ref, up_ref, down_ref
+):
+    place = place_ref[1]
+    early, features = early_ref.shape
+    quarter = features // 4
+    for dx, grads in enumerate((near_ref, far_ref)):
+        for dc in range(2):
+            down_ref[0, :, columns(place, 2 * dx + dc, quarter)] = dot(
+                hidden_ref[...], grads[:, dc * quarter : (dc + 1) * quarter], 0, 0
+            ).astype(BF16)
+    for q in range(4):
+        cols = slice(q * quarter, (q + 1) * quarter)
+        up_ref[0, cols, :] = (
+            dot(early_ref[:, cols], d_up_ref[:early], 0, 0)
+            + dot(late_ref[:, cols], d_up_ref[early:], 0, 0)
+        ).astype(BF16)
+
+
+def order_mixed(index_ref, *refs):
+    came, outs = refs[:-2], refs[-2:]
+    experts = len(came)
+    mine, half, core = index_ref[0], index_ref[2], index_ref[3]
+    _, part, quarter = came[0].shape
+    channels = quarter // 2
+    for s in range(experts):
+        source = jnp.where(mine >= s, mine - s, mine - s + experts)
+        for dj in range(2):
+            rows = pl.ds(pl.multiple_of((source * 2 + (half ^ dj)) * part, part), part)
+            for d in range(2):
+                lanes = pl.ds(pl.multiple_of((core ^ d) * channels, channels), channels)
+                outs[d][rows] = came[s][dj, :, lanes]
+
+
 def finish(core_ref, d_normed_ref, resid_ref, grad_ref, out_ref, blocks_ref):
     d_normed = d_normed_ref[...].astype(F32)
     resid = resid_ref[...].astype(F32)
@@ -204,7 +257,7 @@
         grad_ref[...].astype(F32) + inv_rms * (d_normed - unit * row_mean)
     ).astype(BF16)
     count, part, width = blocks_ref.shape
-    mine = pl.ds(pl.multiple_of(core_ref[0] * part, part), part)
+    mine = pl.ds(pl.multiple_of(core_ref[3] * part, part), part)
     for s in range(count):
         blocks_ref[s] = out_ref[mine, s * width : (s + 1) * width]
 
@@ -220,14 +273,6 @@
         cost_estimate=pl.CostEstimate(flops=flops, bytes_accessed=0, transcendentals=0),
         compiler_params=pltpu.CompilerParams(vmem_limit_bytes=limit),
     )(scalars, *values)
-
-
-def absolute(value, axis, place):
-    width = value.shape[axis] // 4
-    return jnp.concatenate(
-        [lax.dynamic_slice_in_dim(value, (place ^ q) * width, width, axis) for q in range(4)],
-        axis=axis,
-    )
 
 
 def per_device(
@@ -252,7 +297,7 @@
     quarter = features // 4
     mine, half, core = lax.axis_index("e"), lax.axis_index("j"), lax.axis_index("c")
     place = 2 * lax.axis_index("x") + core
-    index = jnp.stack([mine, place]).astype(jnp.int32)
+    index = jnp.stack([mine, place, half, core]).astype(jnp.int32)
 
     outs = in_vmem(
         functools.partial(prepare, experts, cap, quarter),
@@ -271,11 +316,9 @@
     gate_f32 = out_gate.astype(F32)
     mixed = (gate_f32 * conv_f32).astype(BF16)
     channels = mixed.shape[1]
-    fold = quarter // channels
-    mixed_rows = tokens // fold
-    mixed_wide = jnp.concatenate(
-        [mixed[i * mixed_rows : (i + 1) * mixed_rows] for i in range(fold)], axis=1
-    )
+    part = tokens // 2
+    assert 2 * channels == quarter
+    mixed_wide = jnp.concatenate([mixed[:part], mixed[part:]], axis=1)
 
     came = exchange(sends, 1)
     own_rows, own_grads = sends[0][0], sends[0][1]
@@ -295,16 +338,13 @@
     pair = jnp.stack([rows_z, rows_x])
     near = jnp.stack([grads_z, grads_y])
     own_far_sib = swap(own_far, "c")
-    mixed_mine = jnp.stack([own_pair[2 * cap :], own_y[2 * cap :]])
-    mixed_rel = [mixed_mine] + exchange([mixed_mine] * experts, 1)
-    rows_y, far, own_far_sib, mixed_rel = lax.optimization_barrier(
-        (swap(pair, "j"), swap(near, "x"), own_far_sib, mixed_rel)
+    rows_y, far, own_far_sib = lax.optimization_barrier(
+        (swap(pair, "j"), swap(near, "x"), own_far_sib)
     )
     weights = (w_gate[0], w_up[0], w_down[0])
     hidden_units = weights[0].shape[1]
     early = count + cap
     grant = 7 * 4 * 2 * count * hidden_units
-    here = place.reshape(1).astype(jnp.int32)
     sib = lambda value: (value, swap(value, "c"))
     rows_early, pre_gate, pre_up, grads_near, d_half = in_vmem(
         functools.partial(first_half, cap),
@@ -318,7 +358,7 @@
         [],
         (4 * early + 2 * count) * features * hidden_units,
         grant,
-        here,
+        index,
         *sib(own_pair),
         *sib(own_y),
         *sib(pair),
@@ -339,7 +379,7 @@
         [pltpu.VMEM((2 * count - early, hidden_units), F32)] * 2,
         (4 * (2 * count - early) + 6 * count) * features * hidden_units,
         grant,
-        here,
+        index,
         *sib(rows_y),
         own_far,
         own_far_sib,
@@ -350,39 +390,52 @@
         *weights,
     )
 
-    keep = lambda value: jnp.concatenate(
-        [
-            lax.dynamic_slice_in_dim(value, (place ^ (2 * dx)) * quarter, quarter, 0)
-            for dx in range(2)
-        ],
-        axis=0,
-    )
     other = swap(away, "c")
-    kept = dot(d_gate, keep(weights[0]), 1, 1) + dot(d_up, keep(weights[1]), 1, 1)
-    total = (kept + other.astype(F32)).astype(BF16)
-    total, mixed_rel = lax.optimization_barrier((total, mixed_rel))
-    block = lambda dj, dx: total[dj * count : (dj + 1) * count, dx * quarter : (dx + 1) * quarter]
+    (kept,) = in_vmem(
+        kept_part,
+        [((2 * count, features // 2), F32)],
+        [],
+        4 * count * features * hidden_units,
+        grant,
+        index,
+        d_gate,
+        d_up,
+        *weights[:2],
+    )
+    blocks = in_vmem(
+        join, [((count, quarter), BF16)] * 4, [], 2 * count * features, grant, index, kept, other
+    )
+    mixed_mine = jnp.stack([own_pair[2 * cap :], own_y[2 * cap :]])
+    mixed_rel = [mixed_mine] + exchange([mixed_mine] * experts, 1)
     summed = (
-        block(0, 0).astype(F32)
-        + swap(block(0, 1), "x").astype(F32)
-        + swap(block(1, 0), "j").astype(F32)
-        + swap_both(block(1, 1)).astype(F32)
+        blocks[0].astype(F32)
+        + swap(blocks[1], "x").astype(F32)
+        + swap(blocks[2], "j").astype(F32)
+        + swap_both(blocks[3]).astype(F32)
     ).astype(BF16)
+    summed, mixed_rel = lax.optimization_barrier((summed, mixed_rel))
     back = [summed[s * cap : (s + 1) * cap] for s in range(experts)]
     back = back[:1] + exchange(back, -1)
 
-    grad_up = (dot(rows_early, d_up[:early], 0, 0) + dot(rows_late, d_up[early:], 0, 0)).astype(
-        BF16
-    )
-    down_near = dot(hidden, grads_near, 0, 0).astype(BF16)
-    down_far = dot(hidden, grads_far, 0, 0).astype(BF16)
-    grad_down = absolute(jnp.concatenate([down_near, down_far], axis=1), 1, place)
+    grad_up, grad_down = in_vmem(
+        weight_grads,
+        [((1, features, hidden_units), BF16), ((1, hidden_units, features), BF16)],
+        [],
+        8 * count * features * hidden_units,
+        3 * grant,
+        index,
+        rows_early,
+        rows_late,
+        grads_near,
+        grads_far,
+        hidden,
+        d_up,
+    )
 
     d_part = dot(
         sel.reshape(experts * cap, tokens), jnp.concatenate(back, axis=0), 0, 0
     ).astype(BF16)
     d_normed = lax.all_gather(d_part, ("x", "c"), axis=1, tiled=True)
-    part = tokens // 2
     width = features // slices
     cut = slices if width % 128 == 0 else 1
     grad_resid, blocks = in_vmem(
@@ -391,35 +444,27 @@
         [],
         16 * tokens * features,
         8 * 2**20,
-        core.reshape(1).astype(jnp.int32),
+        index,
         d_normed,
         residual,
         out_grad,
     )
 
-    mixed_rel = jnp.stack(mixed_rel).reshape(slices, mixed_rows, quarter)
-    mixed_rel = jnp.concatenate(
-        [mixed_rel[:, :, i * channels : (i + 1) * channels] for i in range(fold)], axis=1
-    )
-    mixed_all = jnp.concatenate(
-        [
-            lax.dynamic_slice_in_dim(
-                mixed_rel, lax.rem(mine - e + experts, experts) * 2 + (half ^ j), 1, 0
-            )
-            for e in range(experts)
-            for j in range(2)
-        ],
-        axis=0,
-    )
-    ordered = [
-        lax.dynamic_slice_in_dim(mixed_all, (core ^ d) * part, part, 1).reshape(-1, channels)
-        for d in range(2)
-    ]
+    ordered = in_vmem(
+        order_mixed,
+        [((slices * part, channels), BF16)] * 2,
+        [],
+        2 * slices * part * channels,
+        grant,
+        index,
+        *mixed_rel,
+    )
     if cut == 1:
         blocks = jnp.transpose(blocks.reshape(part, slices, width), (1, 0, 2))
     got = lax.all_to_all(blocks, ("e", "j"), 0, 0, tiled=True).reshape(slices * part, width)
     got_sib = swap(got, "c")
-    grad_w_out = dot(got, ordered[0], 0, 0) + dot(got_sib, ordered[1], 0, 0)
+    grad_w_out = dot(got, ordered[0], 0, 0)
+    grad_w_out = grad_w_out + dot(got_sib, ordered[1], 0, 0)
 
     d_mix = dot(grad_resid, w_out, 1, 1)
     grad_out_gate = (d_mix * conv_f32).astype(BF16)
@@ -436,8 +481,8 @@
     grad_conv_input = (d_inner * in_gate.astype(F32)).astype(BF16)
     return (
         grad_resid,
-        grad_up[None],
-        grad_down[None],
+        grad_up,
+        grad_down,
         grad_out_gate,
         grad_in_gate,
         grad_conv_input,

time: 142 us -> 124 us (0.87)
  Pallas kernels: 13.5 us -> 21.3 us
  local copies, waits for them, and re-layouts: 8.8 us -> 1.11 us
  matrix products: 10.9 us -> 3.68 us
  other arithmetic: 8.94 us -> 3.22 us
  waiting for transfers between devices: 43.4 us -> 39.9 us
    ppermute x20, waiting for transfers between devices: 15.7 us -> 26.1 us  [swap(): return lax.ppermute(value, axis, [(0, 1), (1, 0)])]
    ppermute x9, waiting for transfers between devices: 11.9 us -> 1.95 us  [exchange(): lax.ppermute(b, 'e', [(i, (i + sign * s) % count) for i in range(count)])]
    pallas_call x4 -> x8, Pallas kernels: 13.5 us -> 21.3 us  [in_vmem(): pl.pallas_call(kernel, out_shape=[jax.ShapeDtypeStruct(shape, kind) for s...]
    dot_general x10 -> x4, matrix products: 10.9 us -> 3.68 us  [dot(): lax.dot_general(a, b, (((ca,), (cb,)), ((), ())), preferred_element_type=...]
    unnamed x60 -> x26, local copies, waits for them, and re-layouts: 5.04 us -> 0.06 us
    ppermute x1, waiting for transfers between devices: 7.69 us -> 3.79 us  [swap_both(): return lax.ppermute(value, ('j', 'x'), [(i, 3 - i) for i in range(4)])]
    dynamic_slice x2 -> x0, local copies, waits for them, and re-layouts: 2.59 us -> none  [the longest x1 2.57 us: per_device(): lax.dynamic_slice_in_dim(value, (place ^ 2 * dx) * quarter, quarter, 0)]
    ppermute x20, starting transfers between devices: 16.7 us -> 14.7 us  [swap(): return lax.ppermute(value, axis, [(0, 1), (1, 0)])]
  transfers between devices with their start and end apart: 33 -> 33, of which waited for: 13 -> 14; matrix products, arithmetic and copies ran while one was open for 12% -> 3% of each run, Pallas kernels for 3% -> 9%
where the time goes in v5:
time: 124 us
  starting transfers between devices  46.6 us (38%)
  waiting for transfers between devices  39.9 us (32%)
  Pallas kernels  21.3 us (17%)
  blocking collectives  6.82 us (6%)
  matrix products  3.68 us (3%)
  other arithmetic  3.22 us (3%)
    ppermute x20, waiting for transfers between devices, swap(): return lax.ppermute(value, axis, [(0, 1), (1, 0)])  26.1 us
    pallas_call x8, Pallas kernels, in_vmem(): pl.pallas_call(kernel, out_shape=[jax.ShapeDtypeStruct(shape, kind) for s...  21.3 us
    ppermute x9, starting transfers between devices, exchange(): lax.ppermute(b, 'e', [(i, (i + sign * s) % count) for i in range(count)])  20.2 us
    ppermute x20, starting transfers between devices, swap(): return lax.ppermute(value, axis, [(0, 1), (1, 0)])  14.7 us
    all_to_all x1, waiting for transfers between devices, per_device(): lax.all_to_all(blocks, ('e', 'j'), 0, 0, tiled=True)  8.11 us
    all_gather x1, blocking collectives, per_device(): d_normed = lax.all_gather(d_part, ('x', 'c'), axis=1, tiled=True)  6.82 us
    all_to_all x1, starting transfers between devices, per_device(): lax.all_to_all(blocks, ('e', 'j'), 0, 0, tiled=True)  5.61 us
    ppermute x1, waiting for transfers between devices, swap_both(): return lax.ppermute(value, ('j', 'x'), [(i, 3 - i) for i in range(4)])  3.79 us
  transfers between devices with their start and end apart: 33, of which 14 were waited for; matrix products, arithmetic and copies ran while one was open for 3% of the time, Pallas kernels for 9%

profile of v5, /device:TPU:0, one launch (start us, length us, event | category | flops | bytes accessed | tf_op | source)
XLA Modules:
  0.0 123.7 jit_solution(9386582683863598260)
XLA Ops:
  1.3 2.6 %shard_map.180 = (bf16[2,80,512]{2,1,0:T(8,128)(2,1)}, bf16[2,80,512]{2,1,0:T(8,128)(2,1)}, bf16[2,80,512]{2,1,0:T(8,128)(2,1)}, bf16[2,80,512]{2,1,0:T(8,128)(2,1)}, bf16[4,80,128]{2,1,0:T(8,128)(2,1)}) custom-call(s32[4]{0:T(128)} %pad_add_fusion.index_ref.place_ref.core_ref, s32[2,128]{1,0:T(2,128)} %bitcast.64, f32[2,128]{1,0:T(2,128)} %bitcast.65, ...), custom_call_target="tpu_custom_call" | custom-call | flops 83886080 | tf_op jit(solution)/shard_map/pallas_call | solution.py:267
  3.9 3.1 %collective-permute-start = (bf16[2,80,512]{2,1,0:T(8,128)(2,1)}, bf16[2,80,512]{2,1,0:T(8,128)(2,1)S(1)}, u32[]{:S(2)}, u32[]{:S(2)}) collective-permute-start(bf16[2,80,512]{2,1,0:T(8,128)(2,1)} %get-tuple-element.51), channel_id=1, source_target_pairs={{0,8},{8,16},{16,24},{24,0},{1,9},{9,17},{17,25},{25,1},{2,10},{10... | collective-permute-start | bytes 491528 | tf_op jit(solution)/shard_map/ppermute | solution.py:29
  7.0 2.6 %collective-permute-start.1 = (bf16[2,80,512]{2,1,0:T(8,128)(2,1)}, bf16[2,80,512]{2,1,0:T(8,128)(2,1)S(1)}, u32[]{:S(2)}, u32[]{:S(2)}) collective-permute-start(bf16[2,80,512]{2,1,0:T(8,128)(2,1)} %get-tuple-element.52), channel_id=1, source_target_pairs={{0,16},{8,24},{16,0},{24,8},{1,17},{9,25},{17,1},{25,9},{2,18},{10... | collective-permute-start | bytes 491528 | tf_op jit(solution)/shard_map/ppermute | solution.py:29
  24.4 7.6 %collective-permute-done.8.far_own_ref = bf16[2,80,512]{2,1,0:T(8,128)(2,1)S(1)} collective-permute-done((bf16[2,80,512]{2,1,0:T(8,128)(2,1)S(1)}, bf16[2,80,512]{2,1,0:T(8,128)(2,1)S(1)}, u32[]{:S(2)}, u32[]{:S(2)}) %collective-permute-start.8) | collective-permute-done | bytes 163872 | tf_op jit(solution)/shard_map/ppermute | solution.py:18
  32.1 1.6 %collective-permute-start.9 = (bf16[2,240,512]{2,1,0:T(8,128)(2,1)S(1)}, bf16[2,240,512]{2,1,0:T(8,128)(2,1)S(1)}, u32[]{:S(2)}, u32[]{:S(2)}) collective-permute-start(bf16[2,240,512]{2,1,0:T(8,128)(2,1)S(1)} %pad_maximum_fusion.pair_ref), channel_id=1, source_target_pairs={{0,4},{4,0},{1,5},{5,1},{2,6},{6,2},{3,7},{7,3},{8,12},{12,8},{9,1... | collective-permute-start | bytes 1474568 | tf_op jit(solution)/shard_map/ppermute | solution.py:18
  36.8 7.5 %collective-permute-done.9.rows_y_ref = bf16[2,240,512]{2,1,0:T(8,128)(2,1)S(1)} collective-permute-done((bf16[2,240,512]{2,1,0:T(8,128)(2,1)S(1)}, bf16[2,240,512]{2,1,0:T(8,128)(2,1)S(1)}, u32[]{:S(2)}, u32[]{:S(2)}) %collective-permute-start.9) | collective-permute-done | bytes 491552 | tf_op jit(solution)/shard_map/ppermute | solution.py:18
  46.3 2.3 %collective-permute-done.15.own_y_sib_ref = bf16[224,512]{1,0:T(8,128)(2,1)S(1)} collective-permute-done((bf16[224,512]{1,0:T(8,128)(2,1)S(1)}, bf16[224,512]{1,0:T(8,128)(2,1)S(1)}, u32[]{:S(2)}, u32[]{:S(2)}) %collective-permute-start.15) | collective-permute-done | bytes 229408 | tf_op jit(solution)/shard_map/ppermute | solution.py:18
  48.6 3.2 %shard_map.181 = (bf16[400,2048]{1,0:T(8,128)(2,1)S(1)}, f32[400,512]{1,0:T(8,128)S(1)}, f32[400,512]{1,0:T(8,128)S(1)}, bf16[640,1024]{1,0:T(8,128)(2,1)S(1)}, f32[640,512]{1,0:T(8,128)S(1)}) custom-call(s32[4]{0:T(128)S(1)} %copy-done.6, bf16[224,512]{1,0:T(8,128)(2,1)S(1)} %maximum_maximum_fusion.own_ref, ...), custom_call_target="tpu_custom_call" | custom-call | flops 2348810240 | tf_op jit(solution)/shard_map/pallas_call | solution.py:267
  51.9 4.4 %shard_map.182 = (bf16[240,2048]{1,0:T(8,128)(2,1)S(1)}, bf16[640,1024]{1,0:T(8,128)(2,1)S(1)}, bf16[640,512]{1,0:T(8,128)(2,1)S(1)}, bf16[640,512]{1,0:T(8,128)...) custom-call(s32[4]{0:T(128)S(1)} %copy-done.6, ...), custom_call_target="tpu_custom_call" | custom-call | flops 3019898880 | tf_op jit(solution)/shard_map/pallas_call | solution.py:267
  56.5 2.1 %shard_map.183.kept_ref = f32[640,1024]{1,0:T(8,128)S(1)} custom-call(s32[4]{0:T(128)S(1)} %copy-done.6, bf16[640,512]{1,0:T(8,128)(2,1)S(1)} %get-tuple-element.70.d_gate_ref, bf16[640,512]{1,0:T(8,128)(2,1)S(1)} %get-tuple-element.71.d_up_ref, bf16[2048,512]{1,0:T(8,128)(2,1)S(1)} %bitcast.50, bf16[2048,512]{1,0:T(8,128)(2,1)S(1)} %bitcast.53), custom_call_target="tpu_custom_call" | custom-call | flops 1342177280 | tf_op jit(solution)/shard_map/pallas_call | solution.py:267
  60.2 1.8 %collective-permute-start.22 = (bf16[320,512]{1,0:T(8,128)(2,1)S(1)}, bf16[320,512]{1,0:T(8,128)(2,1)S(1)}, u32[]{:S(2)}, u32[]{:S(2)}) collective-permute-start(bf16[320,512]{1,0:T(8,128)(2,1)S(1)} %get-tuple-element.76), channel_id=1, source_target_pairs={{0,6},{2,4},{4,2},{6,0},{1,7},{3,5},{5,3},{7,1},{8,14},{10,12},{12... | collective-permute-start | bytes 983048 | tf_op jit(solution)/shard_map/ppermute | solution.py:22
  63.7 4.2 %collective-permute-start.23 = (bf16[2,64,512]{2,1,0:T(8,128)(2,1)S(1)}, bf16[2,64,512]{2,1,0:T(8,128)(2,1)S(1)}, u32[]{:S(2)}, u32[]{:S(2)}) collective-permute-start(bf16[2,64,512]{2,1,0:T(8,128)(2,1)S(1)} %pad_maximum_fusion.5.refs_0_), channel_id=1, source_target_pairs={{0,8},{8,16},{16,24},{24,0},{1,9},{9,17},{17,25},{25,1},{2,10},{10... | collective-permute-start | bytes 393224 | tf_op jit(solution)/shard_map/ppermute | solution.py:29
  68.0 3.8 %collective-permute-done.22 = bf16[320,512]{1,0:T(8,128)(2,1)S(1)} collective-permute-done((bf16[320,512]{1,0:T(8,128)(2,1)S(1)}, bf16[320,512]{1,0:T(8,128)(2,1)S(1)}, u32[]{:S(2)}, u32[]{:S(2)}) %collective-permute-start.22) | collective-permute-done | bytes 327712 | tf_op jit(solution)/shard_map/ppermute | solution.py:22
  71.7 3.2 %collective-permute-start.25 = (bf16[2,64,512]{2,1,0:T(8,128)(2,1)S(1)}, bf16[2,64,512]{2,1,0:T(8,128)(2,1)S(1)}, u32[]{:S(2)}, u32[]{:S(2)}) collective-permute-start(bf16[2,64,512]{2,1,0:T(8,128)(2,1)S(1)} %pad_maximum_fusion.5.refs_0_), channel_id=1, source_target_pairs={{0,24},{8,0},{16,8},{24,16},{1,25},{9,1},{17,9},{25,17},{2,26},{10... | collective-permute-start | bytes 393224 | tf_op jit(solution)/shard_map/ppermute | solution.py:29
  74.9 3.0 %collective-permute-done.21 = bf16[320,512]{1,0:T(8,128)(2,1)S(1)} collective-permute-done((bf16[320,512]{1,0:T(8,128)(2,1)S(1)}, bf16[320,512]{1,0:T(8,128)(2,1)S(1)}, u32[]{:S(2)}, u32[]{:S(2)}) %collective-permute-start.21) | collective-permute-done | bytes 327712 | tf_op jit(solution)/shard_map/ppermute | solution.py:18
  79.0 3.3 %collective-permute-start.28 = (bf16[80,512]{1,0:T(8,128)(2,1)S(1)}, bf16[80,512]{1,0:T(8,128)(2,1)S(1)}, u32[]{:S(2)}, u32[]{:S(2)}) collective-permute-start(bf16[80,512]{1,0:T(8,128)(2,1)S(1)} %get-tuple-element.98), channel_id=1, source_target_pairs={{0,8},{8,16},{16,24},{24,0},{1,9},{9,17},{17,25},{25,1},{2,10},{10... | collective-permute-start | bytes 245768 | tf_op jit(solution)/shard_map/ppermute | solution.py:29
  82.4 2.4 %collective-permute-start.26 = (bf16[80,512]{1,0:T(8,128)(2,1)S(1)}, bf16[80,512]{1,0:T(8,128)(2,1)S(1)}, u32[]{:S(2)}, u32[]{:S(2)}) collective-permute-start(bf16[80,512]{1,0:T(8,128)(2,1)S(1)} %get-tuple-element.100), channel_id=1, source_target_pairs={{0,24},{8,0},{16,8},{24,16},{1,25},{9,1},{17,9},{25,17},{2,26},{10... | collective-permute-start | bytes 245768 | tf_op jit(solution)/shard_map/ppermute | solution.py:29
  84.8 5.7 %shard_map.186 = (bf16[1,2048,512]{2,1,0:T(8,128)(2,1)}, bf16[1,512,2048]{2,1,0:T(8,128)(2,1)}) custom-call(s32[4]{0:T(128)S(1)} %copy-done.6, bf16[400,2048]{1,0:T(8,128)(2,1)S(1)} %get-tuple-element.79.early_ref, bf16[240,2048]{1,0:T(8,128)(2,1)S(1)} %get-tuple-element.80.late_ref, bf16[640,1024]{1,0:T(8,128)(2,1)S(1)} %get-tuple-element.81.near_ref, ...), custom_call_target="tpu_custom_call" | custom-call | flops 2684354560 | tf_op jit(solution)/shard_map/pallas_call | solution.py:267
  91.4 6.8 %all_gather.3.d_normed_ref = bf16[128,2048]{1,0:T(8,128)(2,1)S(1)} all-gather(bf16[128,512]{1,0:T(8,128)(2,1)S(1)} %convolution_convert_fusion), channel_id=1, replica_groups=mesh['e'=4,'j'=2,'x'=2,'c'=2] {'x','c'}, dimensions={1}, use_global_device_ids=true | all-gather | bytes 655360 | tf_op jit(solution)/shard_map/all_gather | solution.py:438
  98.2 1.9 %shard_map.185 = (bf16[128,2048]{1,0:T(8,128)(2,1)}, bf16[8,64,256]{2,1,0:T(8,128)(2,1)}) custom-call(s32[4]{0:T(128)S(1)} %copy-done.6, bf16[128,2048]{1,0:T(8,128)(2,1)S(1)} %all_gather.3.d_normed_ref, bf16[128,2048]{1,0:T(8,128)(2,1)S(1)} %copy-done.4, bf16[128,2048]{1,0:T(8,128)(2,1)S(1)} %copy-done.5), custom_call_target="tpu_custom_call" | custom-call | flops 4194304 | tf_op jit(solution)/shard_map/pallas_call | solution.py:267
  100.2 2.2 %fusion.15 = (bf16[128,256]{1,0:T(8,128)(2,1)S(1)}, f32[128,256]{1,0:T(8,128)S(1)}, bf16[128,256]{1,0:T(8,128)(2,1)}) fusion(bf16[128,256]{1,0:T(8,128)(2,1)S(1)} %copy-done.8, bf16[128,256]{1,0:T(8,128)(2,1)S(1)} %copy-done.7, bf16[128,2048]{1,0:T(8,128)(2,1)} %get-tuple-element.43, bf16[256,2048]{1,0:T(8,128)(2,1)S(1)} %copy-done), kind=kOutput, calls=%fused_computation.42 | convolution fusion | flops 134414336 | bytes 1966080 | tf_op jit(solution)/shard_map/dot_general | solution.py:41
  102.4 3.1 %collective-permute-start.30 = (bf16[1,256]{1,0:T(2,128)(2,1)S(1)}, bf16[1,256]{1,0:T(2,128)(2,1)S(1)}, u32[]{:S(2)}, u32[]{:S(2)}) collective-permute-start(bf16[1,256]{1,0:T(2,128)(2,1)S(1)} %get-tuple-element.118), channel_id=1, source_target_pairs={{0,4},{4,8},{8,12},{12,16},{16,20},{20,24},{24,28},{1,5},{5,9},{9,... | collective-permute-start | bytes 1544 | tf_op jit(solution)/shard_map/ppermute | solution.py:474
  106.7 5.6 %all-to-all-start = ((bf16[8,64,256]{2,1,0:T(8,128)(2,1)}), bf16[8,64,256]{2,1,0:T(8,128)(2,1)S(1)}, u32[]{:S(2)}, u32[]{:S(2)}) async-start(bf16[8,64,256]{2,1,0:T(8,128)(2,1)} %get-tuple-element.86), calls=%async_computation | async-start | bytes 524288 | tf_op jit(solution)/shard_map/all_to_all | solution.py:464
  113.1 8.1 %all-to-all-done = bf16[8,64,256]{2,1,0:T(8,128)(2,1)S(1)} async-done(((bf16[8,64,256]{2,1,0:T(8,128)(2,1)}), bf16[8,64,256]{2,1,0:T(8,128)(2,1)S(1)}, u32[]{:S(2)}, u32[]{:S(2)}) %all-to-all-start) | async-done | bytes 262176 | tf_op jit(solution)/shard_map/all_to_all | solution.py:464
  (105 shorter events, 30.6 us)
Async XLA Ops:
  3.9 15.5 %collective-permute-start = (bf16[2,80,512]{2,1,0:T(8,128)(2,1)}, bf16[2,80,512]{2,1,0:T(8,128)(2,1)S(1)}, u32[]{:S(2)}, u32[]{:S(2)}) collective-permute-start(bf16[2,80,512]{2,1,0:T(8,128)(2,1)} %get-tuple-element.51), channel_id=1, source_target_pairs={{0,8},{8,16},{16,24},{24,0},{1,9},{9,17},{17,25},{25,1},{2,10},{10... | collective-permute-start | bytes 491528 | tf_op jit(solution)/shard_map/ppermute | solution.py:29
  7.0 13.5 %collective-permute-start.1 = (bf16[2,80,512]{2,1,0:T(8,128)(2,1)}, bf16[2,80,512]{2,1,0:T(8,128)(2,1)S(1)}, u32[]{:S(2)}, u32[]{:S(2)}) collective-permute-start(bf16[2,80,512]{2,1,0:T(8,128)(2,1)} %get-tuple-element.52), channel_id=1, source_target_pairs={{0,16},{8,24},{16,0},{24,8},{1,17},{9,25},{17,1},{25,9},{2,18},{10... | collective-permute-start | bytes 491528 | tf_op jit(solution)/shard_map/ppermute | solution.py:29
  9.5 11.0 %collective-permute-start.2 = (bf16[2,80,512]{2,1,0:T(8,128)(2,1)}, bf16[2,80,512]{2,1,0:T(8,128)(2,1)S(1)}, u32[]{:S(2)}, u32[]{:S(2)}) collective-permute-start(bf16[2,80,512]{2,1,0:T(8,128)(2,1)} %get-tuple-element.53), channel_id=1, source_target_pairs={{0,24},{8,0},{16,8},{24,16},{1,25},{9,1},{17,9},{25,17},{2,26},{10... | collective-permute-start | bytes 491528 | tf_op jit(solution)/shard_map/ppermute | solution.py:29
  17.9 14.1 %collective-permute-start.7 = (bf16[224,512]{1,0:T(8,128)(2,1)S(1)}, bf16[224,512]{1,0:T(8,128)(2,1)S(1)}, u32[]{:S(2)}, u32[]{:S(2)}) collective-permute-start(bf16[224,512]{1,0:T(8,128)(2,1)S(1)} %maximum_maximum_fusion.own_ref), channel_id=1, source_target_pairs={{0,4},{4,0},{1,5},{5,1},{2,6},{6,2},{3,7},{7,3},{8,12},{12,8},{9,1... | collective-permute-start | bytes 688136 | tf_op jit(solution)/shard_map/ppermute | solution.py:18
  20.6 11.4 %collective-permute-start.3 = (bf16[240,512]{1,0:T(8,128)(2,1)S(1)}, bf16[240,512]{1,0:T(8,128)(2,1)S(1)}, u32[]{:S(2)}, u32[]{:S(2)}) collective-permute-start(bf16[240,512]{1,0:T(8,128)(2,1)S(1)} %get-tuple-element.104), channel_id=1, source_target_pairs={{0,2},{2,0},{1,3},{3,1},{4,6},{6,4},{5,7},{7,5},{8,10},{10,8},{9,1... | collective-permute-start | bytes 737288 | tf_op jit(solution)/shard_map/ppermute | solution.py:18
  22.2 9.8 %collective-permute-start.4 = (bf16[240,512]{1,0:T(8,128)(2,1)S(1)}, bf16[240,512]{1,0:T(8,128)(2,1)S(1)}, u32[]{:S(2)}, u32[]{:S(2)}) collective-permute-start(bf16[240,512]{1,0:T(8,128)(2,1)S(1)} %get-tuple-element.102), channel_id=1, source_target_pairs={{0,4},{4,0},{1,5},{5,1},{2,6},{6,2},{3,7},{7,3},{8,12},{12,8},{9,1... | collective-permute-start | bytes 737288 | tf_op jit(solution)/shard_map/ppermute | solution.py:18
  23.8 8.2 %collective-permute-start.8 = (bf16[2,80,512]{2,1,0:T(8,128)(2,1)S(1)}, bf16[2,80,512]{2,1,0:T(8,128)(2,1)S(1)}, u32[]{:S(2)}, u32[]{:S(2)}) collective-permute-start(bf16[2,80,512]{2,1,0:T(8,128)(2,1)S(1)} %pad_maximum_fusion.4.near_own_ref), channel_id=1, source_target_pairs={{0,2},{2,0},{1,3},{3,1},{4,6},{6,4},{5,7},{7,5},{8,10},{10,8},{9,1... | collective-permute-start | bytes 491528 | tf_op jit(solution)/shard_map/ppermute | solution.py:18
  32.1 12.3 %collective-permute-start.9 = (bf16[2,240,512]{2,1,0:T(8,128)(2,1)S(1)}, bf16[2,240,512]{2,1,0:T(8,128)(2,1)S(1)}, u32[]{:S(2)}, u32[]{:S(2)}) collective-permute-start(bf16[2,240,512]{2,1,0:T(8,128)(2,1)S(1)} %pad_maximum_fusion.pair_ref), channel_id=1, source_target_pairs={{0,4},{4,0},{1,5},{5,1},{2,6},{6,2},{3,7},{7,3},{8,12},{12,8},{9,1... | collective-permute-start | bytes 1474568 | tf_op jit(solution)/shard_map/ppermute | solution.py:18
  33.7 12.0 %collective-permute-start.10 = (bf16[2,240,512]{2,1,0:T(8,128)(2,1)S(1)}, bf16[2,240,512]{2,1,0:T(8,128)(2,1)S(1)}, u32[]{:S(2)}, u32[]{:S(2)}) collective-permute-start(bf16[2,240,512]{2,1,0:T(8,128)(2,1)S(1)} %pad_maximum_fusion.1.near_ref), channel_id=1, source_target_pairs={{0,2},{2,0},{1,3},{3,1},{4,6},{6,4},{5,7},{7,5},{8,10},{10,8},{9,1... | collective-permute-start | bytes 1474568 | tf_op jit(solution)/shard_map/ppermute | solution.py:18
  35.3 13.3 %collective-permute-start.16 = (bf16[2,240,512]{2,1,0:T(8,128)(2,1)S(1)}, bf16[2,240,512]{2,1,0:T(8,128)(2,1)S(1)}, u32[]{:S(2)}, u32[]{:S(2)}) collective-permute-start(bf16[2,240,512]{2,1,0:T(8,128)(2,1)S(1)} %pad_maximum_fusion.pair_ref), channel_id=1, source_target_pairs={{0,1},{1,0},{2,3},{3,2},{4,5},{5,4},{6,7},{7,6},{8,9},{9,8},{10,11... | collective-permute-start | bytes 1474568 | tf_op jit(solution)/shard_map/ppermute | solution.py:18
  35.8 12.8 %collective-permute-start.18 = (bf16[2,240,512]{2,1,0:T(8,128)(2,1)S(1)}, bf16[2,240,512]{2,1,0:T(8,128)(2,1)S(1)}, u32[]{:S(2)}, u32[]{:S(2)}) collective-permute-start(bf16[2,240,512]{2,1,0:T(8,128)(2,1)S(1)} %pad_maximum_fusion.1.near_ref), channel_id=1, source_target_pairs={{0,1},{1,0},{2,3},{3,2},{4,5},{5,4},{6,7},{7,6},{8,9},{9,8},{10,11... | collective-permute-start | bytes 1474568 | tf_op jit(solution)/shard_map/ppermute | solution.py:18
  36.7 9.5 %collective-permute-start.14 = (bf16[224,512]{1,0:T(8,128)(2,1)S(1)}, bf16[224,512]{1,0:T(8,128)(2,1)S(1)}, u32[]{:S(2)}, u32[]{:S(2)}) collective-permute-start(bf16[224,512]{1,0:T(8,128)(2,1)S(1)} %maximum_maximum_fusion.own_ref), channel_id=1, source_target_pairs={{0,1},{1,0},{2,3},{3,2},{4,5},{5,4},{6,7},{7,6},{8,9},{9,8},{10,11... | collective-permute-start | bytes 688136 | tf_op jit(solution)/shard_map/ppermute | solution.py:18
  60.2 11.6 %collective-permute-start.22 = (bf16[320,512]{1,0:T(8,128)(2,1)S(1)}, bf16[320,512]{1,0:T(8,128)(2,1)S(1)}, u32[]{:S(2)}, u32[]{:S(2)}) collective-permute-start(bf16[320,512]{1,0:T(8,128)(2,1)S(1)} %get-tuple-element.76), channel_id=1, source_target_pairs={{0,6},{2,4},{4,2},{6,0},{1,7},{3,5},{5,3},{7,1},{8,14},{10,12},{12... | collective-permute-start | bytes 983048 | tf_op jit(solution)/shard_map/ppermute | solution.py:22
  62.0 15.9 %collective-permute-start.21 = (bf16[320,512]{1,0:T(8,128)(2,1)S(1)}, bf16[320,512]{1,0:T(8,128)(2,1)S(1)}, u32[]{:S(2)}, u32[]{:S(2)}) collective-permute-start(bf16[320,512]{1,0:T(8,128)(2,1)S(1)} %get-tuple-element.75), channel_id=1, source_target_pairs={{0,4},{4,0},{1,5},{5,1},{2,6},{6,2},{3,7},{7,3},{8,12},{12,8},{9,1... | collective-permute-start | bytes 983048 | tf_op jit(solution)/shard_map/ppermute | solution.py:18
  63.2 14.7 %collective-permute-start.20 = (bf16[320,512]{1,0:T(8,128)(2,1)S(1)}, bf16[320,512]{1,0:T(8,128)(2,1)S(1)}, u32[]{:S(2)}, u32[]{:S(2)}) collective-permute-start(bf16[320,512]{1,0:T(8,128)(2,1)S(1)} %get-tuple-element.74), channel_id=1, source_target_pairs={{0,2},{2,0},{1,3},{3,1},{4,6},{6,4},{5,7},{7,5},{8,10},{10,8},{9,1... | collective-permute-start | bytes 983048 | tf_op jit(solution)/shard_map/ppermute | solution.py:18
  63.7 14.3 %collective-permute-start.23 = (bf16[2,64,512]{2,1,0:T(8,128)(2,1)S(1)}, bf16[2,64,512]{2,1,0:T(8,128)(2,1)S(1)}, u32[]{:S(2)}, u32[]{:S(2)}) collective-permute-start(bf16[2,64,512]{2,1,0:T(8,128)(2,1)S(1)} %pad_maximum_fusion.5.refs_0_), channel_id=1, source_target_pairs={{0,8},{8,16},{16,24},{24,0},{1,9},{9,17},{17,25},{25,1},{2,10},{10... | collective-permute-start | bytes 393224 | tf_op jit(solution)/shard_map/ppermute | solution.py:29
  67.9 10.1 %collective-permute-start.24 = (bf16[2,64,512]{2,1,0:T(8,128)(2,1)S(1)}, bf16[2,64,512]{2,1,0:T(8,128)(2,1)S(1)}, u32[]{:S(2)}, u32[]{:S(2)}) collective-permute-start(bf16[2,64,512]{2,1,0:T(8,128)(2,1)S(1)} %pad_maximum_fusion.5.refs_0_), channel_id=1, source_target_pairs={{0,16},{8,24},{16,0},{24,8},{1,17},{9,25},{17,1},{25,9},{2,18},{10... | collective-permute-start | bytes 393224 | tf_op jit(solution)/shard_map/ppermute | solution.py:29
  71.7 7.2 %collective-permute-start.25 = (bf16[2,64,512]{2,1,0:T(8,128)(2,1)S(1)}, bf16[2,64,512]{2,1,0:T(8,128)(2,1)S(1)}, u32[]{:S(2)}, u32[]{:S(2)}) collective-permute-start(bf16[2,64,512]{2,1,0:T(8,128)(2,1)S(1)} %pad_maximum_fusion.5.refs_0_), channel_id=1, source_target_pairs={{0,24},{8,0},{16,8},{24,16},{1,25},{9,1},{17,9},{25,17},{2,26},{10... | collective-permute-start | bytes 393224 | tf_op jit(solution)/shard_map/ppermute | solution.py:29
  79.0 12.1 %collective-permute-start.28 = (bf16[80,512]{1,0:T(8,128)(2,1)S(1)}, bf16[80,512]{1,0:T(8,128)(2,1)S(1)}, u32[]{:S(2)}, u32[]{:S(2)}) collective-permute-start(bf16[80,512]{1,0:T(8,128)(2,1)S(1)} %get-tuple-element.98), channel_id=1, source_target_pairs={{0,8},{8,16},{16,24},{24,0},{1,9},{9,17},{17,25},{25,1},{2,10},{10... | collective-permute-start | bytes 245768 | tf_op jit(solution)/shard_map/ppermute | solution.py:29
  82.3 8.8 %collective-permute-start.27 = (bf16[80,512]{1,0:T(8,128)(2,1)S(1)}, bf16[80,512]{1,0:T(8,128)(2,1)S(1)}, u32[]{:S(2)}, u32[]{:S(2)}) collective-permute-start(bf16[80,512]{1,0:T(8,128)(2,1)S(1)} %get-tuple-element.99), channel_id=1, source_target_pairs={{0,16},{8,24},{16,0},{24,8},{1,17},{9,25},{17,1},{25,9},{2,18},{10... | collective-permute-start | bytes 245768 | tf_op jit(solution)/shard_map/ppermute | solution.py:29
  82.4 8.8 %collective-permute-start.26 = (bf16[80,512]{1,0:T(8,128)(2,1)S(1)}, bf16[80,512]{1,0:T(8,128)(2,1)S(1)}, u32[]{:S(2)}, u32[]{:S(2)}) collective-permute-start(bf16[80,512]{1,0:T(8,128)(2,1)S(1)} %get-tuple-element.100), channel_id=1, source_target_pairs={{0,24},{8,0},{16,8},{24,16},{1,25},{9,1},{17,9},{25,17},{2,26},{10... | collective-permute-start | bytes 245768 | tf_op jit(solution)/shard_map/ppermute | solution.py:29
  102.4 10.0 %collective-permute-start.30 = (bf16[1,256]{1,0:T(2,128)(2,1)S(1)}, bf16[1,256]{1,0:T(2,128)(2,1)S(1)}, u32[]{:S(2)}, u32[]{:S(2)}) collective-permute-start(bf16[1,256]{1,0:T(2,128)(2,1)S(1)} %get-tuple-element.118), channel_id=1, source_target_pairs={{0,4},{4,8},{8,12},{12,16},{16,20},{20,24},{24,28},{1,5},{5,9},{9,... | collective-permute-start | bytes 1544 | tf_op jit(solution)/shard_map/ppermute | solution.py:474
  105.4 7.0 %collective-permute-start.29 = (bf16[1,256]{1,0:T(2,128)(2,1)S(1)}, bf16[1,256]{1,0:T(2,128)(2,1)S(1)}, u32[]{:S(2)}, u32[]{:S(2)}) collective-permute-start(bf16[1,256]{1,0:T(2,128)(2,1)S(1)} %get-tuple-element.117), channel_id=1, source_target_pairs={{4,0},{8,4},{12,8},{16,12},{20,16},{24,20},{28,24},{5,1},{9,5},{13... | collective-permute-start | bytes 1544 | tf_op jit(solution)/shard_map/ppermute | solution.py:475
  106.7 14.5 %all-to-all-start = ((bf16[8,64,256]{2,1,0:T(8,128)(2,1)}), bf16[8,64,256]{2,1,0:T(8,128)(2,1)S(1)}, u32[]{:S(2)}, u32[]{:S(2)}) async-start(bf16[8,64,256]{2,1,0:T(8,128)(2,1)} %get-tuple-element.86), calls=%async_computation | async-start | bytes 524288 | tf_op jit(solution)/shard_map/all_to_all | solution.py:464
  (22 other events, 343.1 us)

commit v6 on v5

--- a/solution.py
+++ b/solution.py
@@ -25,13 +25,12 @@
 def exchange(blocks, sign):
     count = lax.axis_size("e")
     if count <= 8:
-        return [
-            lax.ppermute(b, "e", [(i, (i + sign * s) % count) for i in range(count)])
-            for s, b in enumerate(blocks)
-            if s
-        ]
+        came = []
+        for s, b in enumerate(blocks, 1):
+            came.append(lax.ppermute(b, "e", [(i, (i + sign * s) % count) for i in range(count)]))
+        return came
     mine, order = lax.axis_index("e"), jnp.arange(count)
-    to = jnp.take(jnp.stack(blocks), sign * (order - mine) % count, axis=0)
+    to = jnp.take(jnp.stack([blocks[0], *blocks]), sign * (order - mine) % count, axis=0)
     came = lax.all_to_all(to, "e", 0, 0, tiled=True)
     came = jnp.take(came, (mine - sign * order) % count, axis=0)
     return [came[s] for s in range(1, count)]
@@ -42,7 +41,8 @@
 
 
 def prepare(experts, cap, quarter, index_ref, routes_ref, weights_ref, resid_ref, grad_ref, *outs):
-    sends, sel_ref = outs[:-1], outs[-1]
+    sel_ref = outs[-1]
+    sends = ((outs[0], outs[1]), *[(send.at[0], send.at[1]) for send in outs[2:-1]])
     tokens = resid_ref.shape[0]
     mine, column = index_ref[0], index_ref[1]
     resid = resid_ref[...].astype(F32)
@@ -76,12 +76,23 @@
         )
         share = jnp.sum(share, axis=1, keepdims=True)
         sel_ref[step] = pick
-        sends[step][0] = dot(pick, normed, 1, 0).astype(BF16)
-        sends[step][1] = (share * dot(pick, grad, 1, 0)).astype(BF16)
+        rows_ref, grads_ref = sends[step]
+        rows_ref[...] = dot(pick, normed, 1, 0).astype(BF16)
+        grads_ref[...] = (share * dot(pick, grad, 1, 0)).astype(BF16)
 
 
 def columns(place, step, width):
     return pl.ds(pl.multiple_of((place ^ step) * width, width), width)
+
+
+def activation(rows, gate_ref, up_ref, slope_ref, active_ref, hidden_ref):
+    pre_gate = dot(rows, gate_ref[...], 1, 0)
+    pre_up = dot(rows, up_ref[...], 1, 0)
+    sigmoid_gate = jax.nn.sigmoid(pre_gate)
+    activated = pre_gate * sigmoid_gate
+    slope_ref[...] = pre_up * sigmoid_gate * (1.0 + pre_gate * (1.0 - sigmoid_gate))
+    active_ref[...] = activated
+    hidden_ref[...] = (activated * pre_up).astype(BF16)
 
 
 def first_half(
@@ -101,8 +112,9 @@
     up_ref,
     down_ref,
     rows_ref,
-    pre_gate_ref,
-    pre_up_ref,
+    slope_ref,
+    active_ref,
+    hidden_ref,
     near_out_ref,
     half_ref,
 ):
@@ -123,9 +135,7 @@
         for dj in range(2):
             near_out_ref[dj * count : dj * count + cap, cols] = near_own[dj]
             near_out_ref[dj * count + cap : (dj + 1) * count, cols] = near[dj]
-    rows = rows_ref[...]
-    pre_gate_ref[...] = dot(rows, gate_ref[...], 1, 0)
-    pre_up_ref[...] = dot(rows, up_ref[...], 1, 0)
+    activation(rows_ref[...], gate_ref, up_ref, slope_ref, active_ref, hidden_ref)
     half_ref[...] = dot(
         near_out_ref[:, :quarter], down_ref[:, columns(place, 0, quarter)], 1, 1
     ) + dot(near_out_ref[:, quarter:], down_ref[:, columns(place, 1, quarter)], 1, 1)
@@ -140,8 +150,8 @@
     far_own_sib_ref,
     far_ref,
     far_sib_ref,
-    pre_gate_ref,
-    pre_up_ref,
+    slope_ref,
+    active_ref,
     half_ref,
     gate_ref,
     up_ref,
@@ -152,13 +162,13 @@
     d_gate_ref,
     d_up_ref,
     away_ref,
-    late_gate_ref,
-    late_up_ref,
+    late_slope_ref,
+    late_active_ref,
 ):
     place = place_ref[1]
     quarter = far_ref.shape[-1]
     count = cap + far_ref.shape[1]
-    early = pre_gate_ref.shape[0]
+    early = slope_ref.shape[0]
     sides = ((rows_y_ref, far_own_ref, far_ref), (rows_y_sib_ref, far_own_sib_ref, far_sib_ref))
     for dc, (rows_y, far_own, far) in enumerate(sides):
         for dx in range(2):
@@ -167,26 +177,18 @@
         for dj in range(2):
             far_out_ref[dj * count : dj * count + cap, cols] = far_own[dj]
             far_out_ref[dj * count + cap : (dj + 1) * count, cols] = far[dj]
-    rows = rows_ref[...]
-    late_gate_ref[...] = dot(rows, gate_ref[...], 1, 0)
-    late_up_ref[...] = dot(rows, up_ref[...], 1, 0)
-    for low, high, gate_at, up_at in (
-        (0, early, pre_gate_ref, pre_up_ref),
-        (early, 2 * count, late_gate_ref, late_up_ref),
+    activation(rows_ref[...], gate_ref, up_ref, late_slope_ref, late_active_ref, hidden_ref)
+    for low, high, slope, active in (
+        (0, early, slope_ref, active_ref),
+        (early, 2 * count, late_slope_ref, late_active_ref),
     ):
         part = slice(low, high)
         d_hidden = half_ref[part] + (
             dot(far_out_ref[part, :quarter], down_ref[:, columns(place, 2, quarter)], 1, 1)
             + dot(far_out_ref[part, quarter:], down_ref[:, columns(place, 3, quarter)], 1, 1)
         )
-        pre_gate, pre_up = gate_at[...], up_at[...]
-        sigmoid_gate = jax.nn.sigmoid(pre_gate)
-        activated = pre_gate * sigmoid_gate
-        hidden_ref[part] = (activated * pre_up).astype(BF16)
-        d_gate_ref[part] = (
-            d_hidden * pre_up * sigmoid_gate * (1.0 + pre_gate * (1.0 - sigmoid_gate))
-        ).astype(BF16)
-        d_up_ref[part] = (d_hidden * activated).astype(BF16)
+        d_gate_ref[part] = (d_hidden * slope[...]).astype(BF16)
+        d_up_ref[part] = (d_hidden * active[...]).astype(BF16)
     for dx in range(2):
         block = columns(place, 2 * dx + 1, quarter)
         away_ref[:, dx * quarter : (dx + 1) * quarter] = (
@@ -205,25 +207,36 @@
 
 
 def join(place_ref, kept_ref, other_ref, *block_refs):
-    count, quarter = block_refs[0].shape
-    for i, block_ref in enumerate(block_refs):
-        rows, cols = divmod(i, 2)
-        rows = slice(rows * count, (rows + 1) * count)
-        cols = slice(cols * quarter, (cols + 1) * quarter)
-        block_ref[...] = (kept_ref[rows, cols] + other_ref[rows, cols].astype(F32)).astype(BF16)
-
-
-def weight_grads(
-    place_ref, early_ref, late_ref, near_ref, far_ref, hidden_ref, d_up_ref, up_ref, down_ref
-):
+    cap, rest, quarter = block_refs[0].shape[0], block_refs[4].shape[0], block_refs[0].shape[1]
+    for i in range(4):
+        dj, dx = divmod(i, 2)
+        cols = slice(dx * quarter, (dx + 1) * quarter)
+        start = dj * (cap + rest)
+        for block_ref, low, high in (
+            (block_refs[i], start, start + cap),
+            (block_refs[4 + i], start + cap, start + cap + rest),
+        ):
+            block_ref[...] = (
+                kept_ref[low:high, cols] + other_ref[low:high, cols].astype(F32)
+            ).astype(BF16)
+
+
+def grad_of_down(place_ref, near_ref, far_ref, early_ref, late_ref, down_ref):
     place = place_ref[1]
+    early = early_ref.shape[0]
+    quarter = near_ref.shape[1] // 2
+    for dx, grads in enumerate((near_ref, far_ref)):
+        for dc in range(2):
+            cols = slice(dc * quarter, (dc + 1) * quarter)
+            down_ref[0, :, columns(place, 2 * dx + dc, quarter)] = (
+                dot(early_ref[...], grads[:early, cols], 0, 0)
+                + dot(late_ref[...], grads[early:, cols], 0, 0)
+            ).astype(BF16)
+
+
+def grad_of_up(place_ref, early_ref, late_ref, d_up_ref, up_ref):
     early, features = early_ref.shape
     quarter = features // 4
-    for dx, grads in enumerate((near_ref, far_ref)):
-        for dc in range(2):
-            down_ref[0, :, columns(place, 2 * dx + dc, quarter)] = dot(
-                hidden_ref[...], grads[:, dc * quarter : (dc + 1) * quarter], 0, 0
-            ).astype(BF16)
     for q in range(4):
         cols = slice(q * quarter, (q + 1) * quarter)
         up_ref[0, cols, :] = (
@@ -247,19 +260,40 @@
                 outs[d][rows] = came[s][dj, :, lanes]
 
 
-def finish(core_ref, d_normed_ref, resid_ref, grad_ref, out_ref, blocks_ref):
+def finish(
+    core_ref,
+    d_normed_ref,
+    resid_ref,
+    grad_ref,
+    w_out_ref,
+    conv_ref,
+    gate_ref,
+    out_ref,
+    blocks_ref,
+    out_gate_ref,
+    d_conv_ref,
+    first_ref,
+    last_ref,
+):
     d_normed = d_normed_ref[...].astype(F32)
     resid = resid_ref[...].astype(F32)
     inv_rms = lax.rsqrt(jnp.mean(resid * resid, axis=-1, keepdims=True) + epsilon)
     unit = resid * inv_rms
     row_mean = jnp.mean(unit * d_normed, axis=-1, keepdims=True)
-    out_ref[...] = (
+    grad_resid = (
         grad_ref[...].astype(F32) + inv_rms * (d_normed - unit * row_mean)
     ).astype(BF16)
+    out_ref[...] = grad_resid
     count, part, width = blocks_ref.shape
     mine = pl.ds(pl.multiple_of(core_ref[3] * part, part), part)
     for s in range(count):
         blocks_ref[s] = out_ref[mine, s * width : (s + 1) * width]
+    d_mix = dot(grad_resid, w_out_ref[...], 1, 1)
+    out_gate_ref[...] = (d_mix * conv_ref[...].astype(F32)).astype(BF16)
+    d_conv = d_mix * gate_ref[...].astype(F32)
+    d_conv_ref[...] = d_conv
+    first_ref[...] = d_conv[:1].astype(BF16)
+    last_ref[...] = d_conv[-1:].astype(BF16)
 
 
 def in_vmem(kernel, outs, scratch, flops, limit, scalars, *values):
@@ -301,7 +335,9 @@
 
     outs = in_vmem(
         functools.partial(prepare, experts, cap, quarter),
-        [((2, cap, quarter), BF16)] * experts + [((experts, cap, tokens), BF16)],
+        [((cap, quarter), BF16)] * 2
+        + [((2, cap, quarter), BF16)] * (experts - 1)
+        + [((experts, cap, tokens), BF16)],
         [],
         4 * experts * cap * tokens * quarter,
         60 * 2**20,
@@ -311,7 +347,7 @@
         residual,
         out_grad,
     )
-    sends, sel = outs[:-1], outs[-1]
+    own_rows, own_grads, sends, sel = outs[0], outs[1], outs[2:-1], outs[-1]
     conv_f32 = conv_out.astype(F32)
     gate_f32 = out_gate.astype(F32)
     mixed = (gate_f32 * conv_f32).astype(BF16)
@@ -321,7 +357,6 @@
     mixed_wide = jnp.concatenate([mixed[:part], mixed[part:]], axis=1)
 
     came = exchange(sends, 1)
-    own_rows, own_grads = sends[0][0], sends[0][1]
     own_rows_x, own_grads_y = lax.optimization_barrier((swap(own_rows, "x"), swap(own_grads, "j")))
     own_pair = jnp.concatenate([own_rows, own_rows_x, mixed_wide], axis=0)
     own_near = jnp.stack([own_grads, own_grads_y])
@@ -346,12 +381,13 @@
     early = count + cap
     grant = 7 * 4 * 2 * count * hidden_units
     sib = lambda value: (value, swap(value, "c"))
-    rows_early, pre_gate, pre_up, grads_near, d_half = in_vmem(
+    rows_early, slope, active, hidden_early, grads_near, d_half = in_vmem(
         functools.partial(first_half, cap),
         [
             ((early, features), BF16),
             ((early, hidden_units), F32),
             ((early, hidden_units), F32),
+            ((early, hidden_units), BF16),
             ((2 * count, features // 2), BF16),
             ((2 * count, hidden_units), F32),
         ],
@@ -366,12 +402,12 @@
         *sib(near),
         *weights,
     )
-    rows_late, grads_far, hidden, d_gate, d_up, away = in_vmem(
+    rows_late, grads_far, hidden_late, d_gate, d_up, away = in_vmem(
         functools.partial(second_half, cap),
         [
             ((2 * count - early, features), BF16),
             ((2 * count, features // 2), BF16),
-            ((2 * count, hidden_units), BF16),
+            ((2 * count - early, hidden_units), BF16),
             ((2 * count, hidden_units), BF16),
             ((2 * count, hidden_units), BF16),
             ((2 * count, features // 2), BF16),
@@ -384,8 +420,8 @@
         own_far,
         own_far_sib,
         *sib(far),
-        pre_gate,
-        pre_up,
+        slope,
+        active,
         d_half,
         *weights,
     )
@@ -403,32 +439,51 @@
         *weights[:2],
     )
     blocks = in_vmem(
-        join, [((count, quarter), BF16)] * 4, [], 2 * count * features, grant, index, kept, other
+        join,
+        [((cap, quarter), BF16)] * 4 + [((count - cap, quarter), BF16)] * 4,
+        [],
+        2 * count * features,
+        grant,
+        index,
+        kept,
+        other,
     )
     mixed_mine = jnp.stack([own_pair[2 * cap :], own_y[2 * cap :]])
-    mixed_rel = [mixed_mine] + exchange([mixed_mine] * experts, 1)
-    summed = (
-        blocks[0].astype(F32)
-        + swap(blocks[1], "x").astype(F32)
-        + swap(blocks[2], "j").astype(F32)
-        + swap_both(blocks[3]).astype(F32)
-    ).astype(BF16)
-    summed, mixed_rel = lax.optimization_barrier((summed, mixed_rel))
-    back = [summed[s * cap : (s + 1) * cap] for s in range(experts)]
-    back = back[:1] + exchange(back, -1)
-
-    grad_up, grad_down = in_vmem(
-        weight_grads,
-        [((1, features, hidden_units), BF16), ((1, hidden_units, features), BF16)],
-        [],
-        8 * count * features * hidden_units,
-        3 * grant,
+    mixed_rel = [mixed_mine] + exchange([mixed_mine] * (experts - 1), 1)
+
+    def spread(parts):
+        return [parts[0], swap(parts[1], "x"), swap(parts[2], "j"), swap_both(parts[3])]
+
+    def total(parts):
+        return sum(part.astype(F32) for part in parts).astype(BF16)
+
+    own_layer = spread(blocks[:4])
+    rest, mixed_rel = lax.optimization_barrier((total(spread(blocks[4:])), mixed_rel))
+    back = exchange([rest[s * cap : (s + 1) * cap] for s in range(experts - 1)], -1)
+    own_layer, back = lax.optimization_barrier((own_layer, back))
+    back = [total(own_layer), *back]
+
+    (grad_down,) = in_vmem(
+        grad_of_down,
+        [((1, hidden_units, features), BF16)],
+        [],
+        4 * count * features * hidden_units,
+        2 * grant,
+        index,
+        grads_near,
+        grads_far,
+        hidden_early,
+        hidden_late,
+    )
+    (grad_up,) = in_vmem(
+        grad_of_up,
+        [((1, features, hidden_units), BF16)],
+        [],
+        4 * count * features * hidden_units,
+        2 * grant,
         index,
         rows_early,
         rows_late,
-        grads_near,
-        grads_far,
-        hidden,
         d_up,
     )
 
@@ -438,9 +493,16 @@
     d_normed = lax.all_gather(d_part, ("x", "c"), axis=1, tiled=True)
     width = features // slices
     cut = slices if width % 128 == 0 else 1
-    grad_resid, blocks = in_vmem(
+    grad_resid, blocks, grad_out_gate, d_conv, first, last = in_vmem(
         finish,
-        [((tokens, features), BF16), ((cut, part, features // cut), BF16)],
+        [
+            ((tokens, features), BF16),
+            ((cut, part, features // cut), BF16),
+            ((tokens, channels), BF16),
+            ((tokens, channels), F32),
+            ((1, channels), BF16),
+            ((1, channels), BF16),
+        ],
         [],
         16 * tokens * features,
         8 * 2**20,
@@ -448,6 +510,9 @@
         d_normed,
         residual,
         out_grad,
+        w_out,
+        conv_out,
+        out_gate,
     )
 
     ordered = in_vmem(
@@ -466,13 +531,9 @@
     grad_w_out = dot(got, ordered[0], 0, 0)
     grad_w_out = grad_w_out + dot(got_sib, ordered[1], 0, 0)
 
-    d_mix = dot(grad_resid, w_out, 1, 1)
-    grad_out_gate = (d_mix * conv_f32).astype(BF16)
-    d_conv = d_mix * gate_f32
-    edge = d_conv.astype(BF16)
     ends = slices - 1
-    above = lax.ppermute(edge[-1:], ("e", "j"), [(i, i + 1) for i in range(ends)])
-    below = lax.ppermute(edge[:1], ("e", "j"), [(i + 1, i) for i in range(ends)])
+    above = lax.ppermute(last, ("e", "j"), [(i, i + 1) for i in range(ends)])
+    below = lax.ppermute(first, ("e", "j"), [(i + 1, i) for i in range(ends)])
     above, below = above.astype(F32), below.astype(F32)
     later = jnp.concatenate([d_conv[1:], below], axis=0)
     earlier = jnp.concatenate([above, d_conv[:-1]], axis=0)

time: 124 us -> 121 us (0.976)
  waiting for transfers between devices: 39.9 us -> 36 us
  matrix products: 3.68 us -> 1.49 us
  Pallas kernels: 21.3 us -> 23.2 us
  starting transfers between devices: 46.6 us -> 48.1 us
    ppermute x1 -> x2, waiting for transfers between devices: 3.79 us -> 0.01 us  [swap_both(): return lax.ppermute(value, ('j', 'x'), [(i, 3 - i) for i in range(4)])]
    ppermute x20 -> x22, waiting for transfers between devices: 26.1 us -> 23.6 us  [swap(): return lax.ppermute(value, axis, [(0, 1), (1, 0)])]
    ppermute x9, waiting for transfers between devices: 1.95 us -> 4.26 us  [exchange(): lax.ppermute(b, 'e', [(i, (i + sign * s) % count) for i in range(count)])]
    ppermute x20 -> x22, starting transfers between devices: 14.7 us -> 16.9 us  [swap(): return lax.ppermute(value, axis, [(0, 1), (1, 0)])]
    dot_general x4 -> x3, matrix products: 3.68 us -> 1.49 us  [dot(): lax.dot_general(a, b, (((ca,), (cb,)), ((), ())), preferred_element_type=...]
    pallas_call x8 -> x9, Pallas kernels: 21.3 us -> 23.2 us  [in_vmem(): pl.pallas_call(kernel, out_shape=[jax.ShapeDtypeStruct(shape, kind) for s...]
    ppermute x9, starting transfers between devices: 20.2 us -> 18.4 us  [exchange(): lax.ppermute(b, 'e', [(i, (i + sign * s) % count) for i in range(count)])]
    ppermute x1 -> x2, starting transfers between devices: 1.85 us -> 3.08 us  [swap_both(): return lax.ppermute(value, ('j', 'x'), [(i, 3 - i) for i in range(4)])]
  transfers between devices with their start and end apart: 33 -> 36, of which waited for: 14 -> 14; matrix products, arithmetic and copies ran while one was open for 3% -> 3% of each run, Pallas kernels for 9% -> 11%
where the time goes in v6:
time: 121 us
  starting transfers between devices  48.1 us (40%)
  waiting for transfers between devices  36 us (30%)
  Pallas kernels  23.2 us (19%)
  blocking collectives  6.63 us (5%)
  other arithmetic  4.08 us (3%)
  matrix products  1.49 us (1%)
    ppermute x22, waiting for transfers between devices, swap(): return lax.ppermute(value, axis, [(0, 1), (1, 0)])  23.6 us
    pallas_call x9, Pallas kernels, in_vmem(): pl.pallas_call(kernel, out_shape=[jax.ShapeDtypeStruct(shape, kind) for s...  23.2 us
    ppermute x9, starting transfers between devices, exchange(): lax.ppermute(b, 'e', [(i, (i + sign * s) % count) for i in range(count)])  18.4 us
    ppermute x22, starting transfers between devices, swap(): return lax.ppermute(value, axis, [(0, 1), (1, 0)])  16.9 us
    all_to_all x1, waiting for transfers between devices, per_device(): lax.all_to_all(blocks, ('e', 'j'), 0, 0, tiled=True)  8.12 us
    all_gather x1, blocking collectives, per_device(): d_normed = lax.all_gather(d_part, ('x', 'c'), axis=1, tiled=True)  6.63 us
    all_to_all x1, starting transfers between devices, per_device(): lax.all_to_all(blocks, ('e', 'j'), 0, 0, tiled=True)  5.02 us
    ppermute x9, waiting for transfers between devices, exchange(): lax.ppermute(b, 'e', [(i, (i + sign * s) % count) for i in range(count)])  4.26 us
  transfers between devices with their start and end apart: 36, of which 14 were waited for; matrix products, arithmetic and copies ran while one was open for 3% of the time, Pallas kernels for 11%

profile of v6, /device:TPU:0, one launch (start us, length us, event | category | flops | bytes accessed | tf_op | source)
XLA Modules:
  0.0 120.6 jit_solution(6407630490912509836)
XLA Ops:
  1.2 2.6 %shard_map.180 = (bf16[80,512]{1,0:T(8,128)(2,1)}, bf16[80,512]{1,0:T(8,128)(2,1)}, bf16[2,80,512]{2,1,0:T(8,128)(2,1)}, bf16[2,80,512]{2,1,0:T(8,128)(2,1)}, bf...) custom-call(s32[4]{0:T(128)} %pad_add_fusion.index_ref.place_ref.core_ref, s32[2,128]{1,0:T(2,128)} %bitcast.60, ...), custom_call_target="tpu_custom_call" | custom-call | flops 83886080 | tf_op jit(solution)/shard_map/pallas_call | solution.py:301
  3.8 3.1 %collective-permute-start = (bf16[2,80,512]{2,1,0:T(8,128)(2,1)}, bf16[2,80,512]{2,1,0:T(8,128)(2,1)S(1)}, u32[]{:S(2)}, u32[]{:S(2)}) collective-permute-start(bf16[2,80,512]{2,1,0:T(8,128)(2,1)} %get-tuple-element.66), channel_id=1, source_target_pairs={{0,8},{8,16},{16,24},{24,0},{1,9},{9,17},{17,25},{25,1},{2,10},{10... | collective-permute-start | bytes 491528 | tf_op jit(solution)/shard_map/ppermute | solution.py:30
  6.9 2.6 %collective-permute-start.1 = (bf16[2,80,512]{2,1,0:T(8,128)(2,1)}, bf16[2,80,512]{2,1,0:T(8,128)(2,1)S(1)}, u32[]{:S(2)}, u32[]{:S(2)}) collective-permute-start(bf16[2,80,512]{2,1,0:T(8,128)(2,1)} %get-tuple-element.67), channel_id=1, source_target_pairs={{0,16},{8,24},{16,0},{24,8},{1,17},{9,25},{17,1},{25,9},{2,18},{10... | collective-permute-start | bytes 491528 | tf_op jit(solution)/shard_map/ppermute | solution.py:30
  17.9 1.6 %collective-permute-start.7 = (bf16[224,512]{1,0:T(8,128)(2,1)S(1)}, bf16[224,512]{1,0:T(8,128)(2,1)S(1)}, u32[]{:S(2)}, u32[]{:S(2)}) collective-permute-start(bf16[224,512]{1,0:T(8,128)(2,1)S(1)} %maximum_maximum_fusion.own_ref), channel_id=1, source_target_pairs={{0,4},{4,0},{1,5},{5,1},{2,6},{6,2},{3,7},{7,3},{8,12},{12,8},{9,1... | collective-permute-start | bytes 688136 | tf_op jit(solution)/shard_map/ppermute | solution.py:18
  22.2 1.6 %collective-permute-start.4 = (bf16[240,512]{1,0:T(8,128)(2,1)S(1)}, bf16[240,512]{1,0:T(8,128)(2,1)S(1)}, u32[]{:S(2)}, u32[]{:S(2)}) collective-permute-start(bf16[240,512]{1,0:T(8,128)(2,1)S(1)} %get-tuple-element.129), channel_id=1, source_target_pairs={{0,4},{4,0},{1,5},{5,1},{2,6},{6,2},{3,7},{7,3},{8,12},{12,8},{9,1... | collective-permute-start | bytes 737288 | tf_op jit(solution)/shard_map/ppermute | solution.py:18
  24.4 7.6 %collective-permute-done.8.far_own_ref = bf16[2,80,512]{2,1,0:T(8,128)(2,1)S(1)} collective-permute-done((bf16[2,80,512]{2,1,0:T(8,128)(2,1)S(1)}, bf16[2,80,512]{2,1,0:T(8,128)(2,1)S(1)}, u32[]{:S(2)}, u32[]{:S(2)}) %collective-permute-start.8) | collective-permute-done | bytes 163872 | tf_op jit(solution)/shard_map/ppermute | solution.py:18
  36.7 7.5 %collective-permute-done.9.rows_y_ref = bf16[2,240,512]{2,1,0:T(8,128)(2,1)S(1)} collective-permute-done((bf16[2,240,512]{2,1,0:T(8,128)(2,1)S(1)}, bf16[2,240,512]{2,1,0:T(8,128)(2,1)S(1)}, u32[]{:S(2)}, u32[]{:S(2)}) %collective-permute-start.9) | collective-permute-done | bytes 491552 | tf_op jit(solution)/shard_map/ppermute | solution.py:18
  46.2 2.3 %collective-permute-done.15.own_y_sib_ref = bf16[224,512]{1,0:T(8,128)(2,1)S(1)} collective-permute-done((bf16[224,512]{1,0:T(8,128)(2,1)S(1)}, bf16[224,512]{1,0:T(8,128)(2,1)S(1)}, u32[]{:S(2)}, u32[]{:S(2)}) %collective-permute-start.15) | collective-permute-done | bytes 229408 | tf_op jit(solution)/shard_map/ppermute | solution.py:18
  48.6 3.4 %shard_map.181 = (bf16[400,2048]{1,0:T(8,128)(2,1)S(1)}, f32[400,512]{1,0:T(8,128)S(1)}, f32[400,512]{1,0:T(8,128)S(1)}, bf16[400,512]{1,0:T(8,128)(2,1)S(1)}, b...) custom-call(s32[4]{0:T(128)S(1)} %copy-done.8, bf16[224,512]{1,0:T(8,128)(2,1)S(1)} %maximum_maximum_fusion.own_ref, ...), custom_call_target="tpu_custom_call" | custom-call | flops 2348810240 | tf_op jit(solution)/shard_map/pallas_call | solution.py:301
  52.0 4.1 %shard_map.182 = (bf16[240,2048]{1,0:T(8,128)(2,1)S(1)}, bf16[640,1024]{1,0:T(8,128)(2,1)S(1)}, bf16[240,512]{1,0:T(8,128)(2,1)S(1)}, bf16[640,512]{1,0:T(8,128)...) custom-call(s32[4]{0:T(128)S(1)} %copy-done.8, ...), custom_call_target="tpu_custom_call" | custom-call | flops 3019898880 | tf_op jit(solution)/shard_map/pallas_call | solution.py:301
  56.3 2.1 %shard_map.183.kept_ref = f32[640,1024]{1,0:T(8,128)S(1)} custom-call(s32[4]{0:T(128)S(1)} %copy-done.8, bf16[640,512]{1,0:T(8,128)(2,1)S(1)} %get-tuple-element.86.d_gate_ref, bf16[640,512]{1,0:T(8,128)(2,1)S(1)} %get-tuple-element.87.d_up_ref, bf16[2048,512]{1,0:T(8,128)(2,1)S(1)} %bitcast.45, bf16[2048,512]{1,0:T(8,128)(2,1)S(1)} %bitcast.48), custom_call_target="tpu_custom_call" | custom-call | flops 1342177280 | tf_op jit(solution)/shard_map/pallas_call | solution.py:301
  60.0 1.8 %collective-permute-start.25 = (bf16[240,512]{1,0:T(8,128)(2,1)S(1)}, bf16[240,512]{1,0:T(8,128)(2,1)S(1)}, u32[]{:S(2)}, u32[]{:S(2)}) collective-permute-start(bf16[240,512]{1,0:T(8,128)(2,1)S(1)} %get-tuple-element.96), channel_id=1, source_target_pairs={{0,6},{2,4},{4,2},{6,0},{1,7},{3,5},{5,3},{7,1},{8,14},{10,12},{12... | collective-permute-start | bytes 737288 | tf_op jit(solution)/shard_map/ppermute | solution.py:22
  63.6 4.2 %collective-permute-start.26 = (bf16[2,64,512]{2,1,0:T(8,128)(2,1)S(1)}, bf16[2,64,512]{2,1,0:T(8,128)(2,1)S(1)}, u32[]{:S(2)}, u32[]{:S(2)}) collective-permute-start(bf16[2,64,512]{2,1,0:T(8,128)(2,1)S(1)} %pad_maximum_fusion.5.refs_0_), channel_id=1, source_target_pairs={{0,8},{8,16},{16,24},{24,0},{1,9},{9,17},{17,25},{25,1},{2,10},{10... | collective-permute-start | bytes 393224 | tf_op jit(solution)/shard_map/ppermute | solution.py:30
  67.8 3.7 %shard_map.186 = bf16[1,2048,512]{2,1,0:T(8,128)(2,1)} custom-call(s32[4]{0:T(128)S(1)} %copy-done.8, bf16[400,2048]{1,0:T(8,128)(2,1)S(1)} %get-tuple-element.106.early_ref, bf16[240,2048]{1,0:T(8,128)(2,1)S(1)} %get-tuple-element.107.late_ref, bf16[640,512]{1,0:T(8,128)(2,1)S(1)} %get-tuple-element.87.d_up_ref), custom_call_target="tpu_custom_call" | custom-call | flops 1342177280 | tf_op jit(solution)/shard_map/pallas_call | solution.py:301
  71.5 2.4 %collective-permute-start.28 = (bf16[2,64,512]{2,1,0:T(8,128)(2,1)S(1)}, bf16[2,64,512]{2,1,0:T(8,128)(2,1)S(1)}, u32[]{:S(2)}, u32[]{:S(2)}) collective-permute-start(bf16[2,64,512]{2,1,0:T(8,128)(2,1)S(1)} %pad_maximum_fusion.5.refs_0_), channel_id=1, source_target_pairs={{0,24},{8,0},{16,8},{24,16},{1,25},{9,1},{17,9},{25,17},{2,26},{10... | collective-permute-start | bytes 393224 | tf_op jit(solution)/shard_map/ppermute | solution.py:30
  78.9 2.8 %collective-permute-start.29 = (bf16[80,512]{1,0:T(8,128)(2,1)S(1)}, bf16[80,512]{1,0:T(8,128)(2,1)S(1)}, u32[]{:S(2)}, u32[]{:S(2)}) collective-permute-start(bf16[80,512]{1,0:T(8,128)(2,1)S(1)} %get-tuple-element.127), channel_id=1, source_target_pairs={{0,24},{8,0},{16,8},{24,16},{1,25},{9,1},{17,9},{25,17},{2,26},{10... | collective-permute-start | bytes 245768 | tf_op jit(solution)/shard_map/ppermute | solution.py:30
  81.6 2.0 %collective-permute-start.30 = (bf16[80,512]{1,0:T(8,128)(2,1)S(1)}, bf16[80,512]{1,0:T(8,128)(2,1)S(1)}, u32[]{:S(2)}, u32[]{:S(2)}) collective-permute-start(bf16[80,512]{1,0:T(8,128)(2,1)S(1)} %get-tuple-element.126), channel_id=1, source_target_pairs={{0,16},{8,24},{16,0},{24,8},{1,17},{9,25},{17,1},{25,9},{2,18},{10... | collective-permute-start | bytes 245768 | tf_op jit(solution)/shard_map/ppermute | solution.py:30
  83.7 3.7 %shard_map.187 = bf16[1,512,2048]{2,1,0:T(8,128)(2,1)} custom-call(s32[4]{0:T(128)S(1)} %copy-done.8, bf16[640,1024]{1,0:T(8,128)(2,1)S(1)} %get-tuple-element.108.near_ref, bf16[640,1024]{1,0:T(8,128)(2,1)S(1)} %get-tuple-element.109.far_ref, bf16[400,512]{1,0:T(8,128)(2,1)S(1)} %get-tuple-element.110.early_ref, ...), custom_call_target="tpu_custom_call" | custom-call | flops 1342177280 | tf_op jit(solution)/shard_map/pallas_call | solution.py:301
  88.0 2.4 %collective-permute-done.30 = bf16[80,512]{1,0:T(8,128)(2,1)S(1)} collective-permute-done((bf16[80,512]{1,0:T(8,128)(2,1)S(1)}, bf16[80,512]{1,0:T(8,128)(2,1)S(1)}, u32[]{:S(2)}, u32[]{:S(2)}) %collective-permute-start.30) | collective-permute-done | bytes 81952 | tf_op jit(solution)/shard_map/ppermute | solution.py:30
  90.7 6.6 %all_gather.3.d_normed_ref = bf16[128,2048]{1,0:T(8,128)(2,1)S(1)} all-gather(bf16[128,512]{1,0:T(8,128)(2,1)S(1)} %convolution_convert_fusion), channel_id=1, replica_groups=mesh['e'=4,'j'=2,'x'=2,'c'=2] {'x','c'}, dimensions={1}, use_global_device_ids=true | all-gather | bytes 655360 | tf_op jit(solution)/shard_map/all_gather | solution.py:493
  97.4 2.1 %shard_map.185 = (bf16[128,2048]{1,0:T(8,128)(2,1)}, bf16[8,64,256]{2,1,0:T(8,128)(2,1)}, bf16[128,256]{1,0:T(8,128)(2,1)}, f32[128,256]{1,0:T(8,128)S(1)}, bf16...) custom-call(s32[4]{0:T(128)S(1)} %copy-done.8, bf16[128,2048]{1,0:T(8,128)(2,1)S(1)} %all_gather.3.d_normed_ref, ...), custom_call_target="tpu_custom_call" | custom-call | flops 4194304 | tf_op jit(solution)/shard_map/pallas_call | solution.py:301
  99.5 3.4 %collective-permute-start.33 = (bf16[1,256]{1,0:T(2,128)(2,1)S(1)}, bf16[1,256]{1,0:T(2,128)(2,1)S(1)}, u32[]{:S(2)}, u32[]{:S(2)}) collective-permute-start(bf16[1,256]{1,0:T(2,128)(2,1)S(1)} %get-tuple-element.115), channel_id=1, source_target_pairs={{0,4},{4,8},{8,12},{12,16},{16,20},{20,24},{24,28},{1,5},{5,9},{9,... | collective-permute-start | bytes 1544 | tf_op jit(solution)/shard_map/ppermute | solution.py:535
  104.2 5.0 %all-to-all-start = ((bf16[8,64,256]{2,1,0:T(8,128)(2,1)}), bf16[8,64,256]{2,1,0:T(8,128)(2,1)S(1)}, u32[]{:S(2)}, u32[]{:S(2)}) async-start(bf16[8,64,256]{2,1,0:T(8,128)(2,1)} %get-tuple-element.116), calls=%async_computation | async-start | bytes 524288 | tf_op jit(solution)/shard_map/all_to_all | solution.py:529
  110.0 8.1 %all-to-all-done = bf16[8,64,256]{2,1,0:T(8,128)(2,1)S(1)} async-done(((bf16[8,64,256]{2,1,0:T(8,128)(2,1)}), bf16[8,64,256]{2,1,0:T(8,128)(2,1)S(1)}, u32[]{:S(2)}, u32[]{:S(2)}) %all-to-all-start) | async-done | bytes 262176 | tf_op jit(solution)/shard_map/all_to_all | solution.py:529
  (112 shorter events, 32.8 us)
Async XLA Ops:
  3.8 15.6 %collective-permute-start = (bf16[2,80,512]{2,1,0:T(8,128)(2,1)}, bf16[2,80,512]{2,1,0:T(8,128)(2,1)S(1)}, u32[]{:S(2)}, u32[]{:S(2)}) collective-permute-start(bf16[2,80,512]{2,1,0:T(8,128)(2,1)} %get-tuple-element.66), channel_id=1, source_target_pairs={{0,8},{8,16},{16,24},{24,0},{1,9},{9,17},{17,25},{25,1},{2,10},{10... | collective-permute-start | bytes 491528 | tf_op jit(solution)/shard_map/ppermute | solution.py:30
  6.9 13.5 %collective-permute-start.1 = (bf16[2,80,512]{2,1,0:T(8,128)(2,1)}, bf16[2,80,512]{2,1,0:T(8,128)(2,1)S(1)}, u32[]{:S(2)}, u32[]{:S(2)}) collective-permute-start(bf16[2,80,512]{2,1,0:T(8,128)(2,1)} %get-tuple-element.67), channel_id=1, source_target_pairs={{0,16},{8,24},{16,0},{24,8},{1,17},{9,25},{17,1},{25,9},{2,18},{10... | collective-permute-start | bytes 491528 | tf_op jit(solution)/shard_map/ppermute | solution.py:30
  9.5 11.0 %collective-permute-start.2 = (bf16[2,80,512]{2,1,0:T(8,128)(2,1)}, bf16[2,80,512]{2,1,0:T(8,128)(2,1)S(1)}, u32[]{:S(2)}, u32[]{:S(2)}) collective-permute-start(bf16[2,80,512]{2,1,0:T(8,128)(2,1)} %get-tuple-element.68), channel_id=1, source_target_pairs={{0,24},{8,0},{16,8},{24,16},{1,25},{9,1},{17,9},{25,17},{2,26},{10... | collective-permute-start | bytes 491528 | tf_op jit(solution)/shard_map/ppermute | solution.py:30
  17.9 14.1 %collective-permute-start.7 = (bf16[224,512]{1,0:T(8,128)(2,1)S(1)}, bf16[224,512]{1,0:T(8,128)(2,1)S(1)}, u32[]{:S(2)}, u32[]{:S(2)}) collective-permute-start(bf16[224,512]{1,0:T(8,128)(2,1)S(1)} %maximum_maximum_fusion.own_ref), channel_id=1, source_target_pairs={{0,4},{4,0},{1,5},{5,1},{2,6},{6,2},{3,7},{7,3},{8,12},{12,8},{9,1... | collective-permute-start | bytes 688136 | tf_op jit(solution)/shard_map/ppermute | solution.py:18
  20.6 11.4 %collective-permute-start.3 = (bf16[240,512]{1,0:T(8,128)(2,1)S(1)}, bf16[240,512]{1,0:T(8,128)(2,1)S(1)}, u32[]{:S(2)}, u32[]{:S(2)}) collective-permute-start(bf16[240,512]{1,0:T(8,128)(2,1)S(1)} %get-tuple-element.131), channel_id=1, source_target_pairs={{0,2},{2,0},{1,3},{3,1},{4,6},{6,4},{5,7},{7,5},{8,10},{10,8},{9,1... | collective-permute-start | bytes 737288 | tf_op jit(solution)/shard_map/ppermute | solution.py:18
  22.2 9.8 %collective-permute-start.4 = (bf16[240,512]{1,0:T(8,128)(2,1)S(1)}, bf16[240,512]{1,0:T(8,128)(2,1)S(1)}, u32[]{:S(2)}, u32[]{:S(2)}) collective-permute-start(bf16[240,512]{1,0:T(8,128)(2,1)S(1)} %get-tuple-element.129), channel_id=1, source_target_pairs={{0,4},{4,0},{1,5},{5,1},{2,6},{6,2},{3,7},{7,3},{8,12},{12,8},{9,1... | collective-permute-start | bytes 737288 | tf_op jit(solution)/shard_map/ppermute | solution.py:18
  23.8 8.2 %collective-permute-start.8 = (bf16[2,80,512]{2,1,0:T(8,128)(2,1)S(1)}, bf16[2,80,512]{2,1,0:T(8,128)(2,1)S(1)}, u32[]{:S(2)}, u32[]{:S(2)}) collective-permute-start(bf16[2,80,512]{2,1,0:T(8,128)(2,1)S(1)} %pad_maximum_fusion.4.near_own_ref), channel_id=1, source_target_pairs={{0,2},{2,0},{1,3},{3,1},{4,6},{6,4},{5,7},{7,5},{8,10},{10,8},{9,1... | collective-permute-start | bytes 491528 | tf_op jit(solution)/shard_map/ppermute | solution.py:18
  32.0 12.3 %collective-permute-start.9 = (bf16[2,240,512]{2,1,0:T(8,128)(2,1)S(1)}, bf16[2,240,512]{2,1,0:T(8,128)(2,1)S(1)}, u32[]{:S(2)}, u32[]{:S(2)}) collective-permute-start(bf16[2,240,512]{2,1,0:T(8,128)(2,1)S(1)} %pad_maximum_fusion.pair_ref), channel_id=1, source_target_pairs={{0,4},{4,0},{1,5},{5,1},{2,6},{6,2},{3,7},{7,3},{8,12},{12,8},{9,1... | collective-permute-start | bytes 1474568 | tf_op jit(solution)/shard_map/ppermute | solution.py:18
  33.6 12.0 %collective-permute-start.10 = (bf16[2,240,512]{2,1,0:T(8,128)(2,1)S(1)}, bf16[2,240,512]{2,1,0:T(8,128)(2,1)S(1)}, u32[]{:S(2)}, u32[]{:S(2)}) collective-permute-start(bf16[2,240,512]{2,1,0:T(8,128)(2,1)S(1)} %pad_maximum_fusion.1.near_ref), channel_id=1, source_target_pairs={{0,2},{2,0},{1,3},{3,1},{4,6},{6,4},{5,7},{7,5},{8,10},{10,8},{9,1... | collective-permute-start | bytes 1474568 | tf_op jit(solution)/shard_map/ppermute | solution.py:18
  35.2 13.3 %collective-permute-start.16 = (bf16[2,240,512]{2,1,0:T(8,128)(2,1)S(1)}, bf16[2,240,512]{2,1,0:T(8,128)(2,1)S(1)}, u32[]{:S(2)}, u32[]{:S(2)}) collective-permute-start(bf16[2,240,512]{2,1,0:T(8,128)(2,1)S(1)} %pad_maximum_fusion.pair_ref), channel_id=1, source_target_pairs={{0,1},{1,0},{2,3},{3,2},{4,5},{5,4},{6,7},{7,6},{8,9},{9,8},{10,11... | collective-permute-start | bytes 1474568 | tf_op jit(solution)/shard_map/ppermute | solution.py:18
  35.7 12.8 %collective-permute-start.18 = (bf16[2,240,512]{2,1,0:T(8,128)(2,1)S(1)}, bf16[2,240,512]{2,1,0:T(8,128)(2,1)S(1)}, u32[]{:S(2)}, u32[]{:S(2)}) collective-permute-start(bf16[2,240,512]{2,1,0:T(8,128)(2,1)S(1)} %pad_maximum_fusion.1.near_ref), channel_id=1, source_target_pairs={{0,1},{1,0},{2,3},{3,2},{4,5},{5,4},{6,7},{7,6},{8,9},{9,8},{10,11... | collective-permute-start | bytes 1474568 | tf_op jit(solution)/shard_map/ppermute | solution.py:18
  36.6 9.5 %collective-permute-start.14 = (bf16[224,512]{1,0:T(8,128)(2,1)S(1)}, bf16[224,512]{1,0:T(8,128)(2,1)S(1)}, u32[]{:S(2)}, u32[]{:S(2)}) collective-permute-start(bf16[224,512]{1,0:T(8,128)(2,1)S(1)} %maximum_maximum_fusion.own_ref), channel_id=1, source_target_pairs={{0,1},{1,0},{2,3},{3,2},{4,5},{5,4},{6,7},{7,6},{8,9},{9,8},{10,11... | collective-permute-start | bytes 688136 | tf_op jit(solution)/shard_map/ppermute | solution.py:18
  60.0 11.5 %collective-permute-start.25 = (bf16[240,512]{1,0:T(8,128)(2,1)S(1)}, bf16[240,512]{1,0:T(8,128)(2,1)S(1)}, u32[]{:S(2)}, u32[]{:S(2)}) collective-permute-start(bf16[240,512]{1,0:T(8,128)(2,1)S(1)} %get-tuple-element.96), channel_id=1, source_target_pairs={{0,6},{2,4},{4,2},{6,0},{1,7},{3,5},{5,3},{7,1},{8,14},{10,12},{12... | collective-permute-start | bytes 737288 | tf_op jit(solution)/shard_map/ppermute | solution.py:22
  61.9 12.4 %collective-permute-start.24 = (bf16[240,512]{1,0:T(8,128)(2,1)S(1)}, bf16[240,512]{1,0:T(8,128)(2,1)S(1)}, u32[]{:S(2)}, u32[]{:S(2)}) collective-permute-start(bf16[240,512]{1,0:T(8,128)(2,1)S(1)} %get-tuple-element.95), channel_id=1, source_target_pairs={{0,4},{4,0},{1,5},{5,1},{2,6},{6,2},{3,7},{7,3},{8,12},{12,8},{9,1... | collective-permute-start | bytes 737288 | tf_op jit(solution)/shard_map/ppermute | solution.py:18
  63.0 12.4 %collective-permute-start.23 = (bf16[240,512]{1,0:T(8,128)(2,1)S(1)}, bf16[240,512]{1,0:T(8,128)(2,1)S(1)}, u32[]{:S(2)}, u32[]{:S(2)}) collective-permute-start(bf16[240,512]{1,0:T(8,128)(2,1)S(1)} %get-tuple-element.94), channel_id=1, source_target_pairs={{0,2},{2,0},{1,3},{3,1},{4,6},{6,4},{5,7},{7,5},{8,10},{10,8},{9,1... | collective-permute-start | bytes 737288 | tf_op jit(solution)/shard_map/ppermute | solution.py:18
  63.6 13.1 %collective-permute-start.26 = (bf16[2,64,512]{2,1,0:T(8,128)(2,1)S(1)}, bf16[2,64,512]{2,1,0:T(8,128)(2,1)S(1)}, u32[]{:S(2)}, u32[]{:S(2)}) collective-permute-start(bf16[2,64,512]{2,1,0:T(8,128)(2,1)S(1)} %pad_maximum_fusion.5.refs_0_), channel_id=1, source_target_pairs={{0,8},{8,16},{16,24},{24,0},{1,9},{9,17},{17,25},{25,1},{2,10},{10... | collective-permute-start | bytes 393224 | tf_op jit(solution)/shard_map/ppermute | solution.py:30
  67.8 10.1 %collective-permute-start.27 = (bf16[2,64,512]{2,1,0:T(8,128)(2,1)S(1)}, bf16[2,64,512]{2,1,0:T(8,128)(2,1)S(1)}, u32[]{:S(2)}, u32[]{:S(2)}) collective-permute-start(bf16[2,64,512]{2,1,0:T(8,128)(2,1)S(1)} %pad_maximum_fusion.5.refs_0_), channel_id=1, source_target_pairs={{0,16},{8,24},{16,0},{24,8},{1,17},{9,25},{17,1},{25,9},{2,18},{10... | collective-permute-start | bytes 393224 | tf_op jit(solution)/shard_map/ppermute | solution.py:30
  74.2 9.4 %collective-permute-start.20 = (bf16[80,512]{1,0:T(8,128)(2,1)S(1)}, bf16[80,512]{1,0:T(8,128)(2,1)S(1)}, u32[]{:S(2)}, u32[]{:S(2)}) collective-permute-start(bf16[80,512]{1,0:T(8,128)(2,1)S(1)} %get-tuple-element.90), channel_id=1, source_target_pairs={{0,2},{2,0},{1,3},{3,1},{4,6},{6,4},{5,7},{7,5},{8,10},{10,8},{9,1... | collective-permute-start | bytes 245768 | tf_op jit(solution)/shard_map/ppermute | solution.py:18
  75.5 12.5 %collective-permute-start.21 = (bf16[80,512]{1,0:T(8,128)(2,1)S(1)}, bf16[80,512]{1,0:T(8,128)(2,1)S(1)}, u32[]{:S(2)}, u32[]{:S(2)}) collective-permute-start(bf16[80,512]{1,0:T(8,128)(2,1)S(1)} %get-tuple-element.91), channel_id=1, source_target_pairs={{0,4},{4,0},{1,5},{5,1},{2,6},{6,2},{3,7},{7,3},{8,12},{12,8},{9,1... | collective-permute-start | bytes 245768 | tf_op jit(solution)/shard_map/ppermute | solution.py:18
  76.7 11.3 %collective-permute-start.22 = (bf16[80,512]{1,0:T(8,128)(2,1)S(1)}, bf16[80,512]{1,0:T(8,128)(2,1)S(1)}, u32[]{:S(2)}, u32[]{:S(2)}) collective-permute-start(bf16[80,512]{1,0:T(8,128)(2,1)S(1)} %get-tuple-element.92), channel_id=1, source_target_pairs={{0,6},{2,4},{4,2},{6,0},{1,7},{3,5},{5,3},{7,1},{8,14},{10,12},{12... | collective-permute-start | bytes 245768 | tf_op jit(solution)/shard_map/ppermute | solution.py:22
  78.9 9.2 %collective-permute-start.29 = (bf16[80,512]{1,0:T(8,128)(2,1)S(1)}, bf16[80,512]{1,0:T(8,128)(2,1)S(1)}, u32[]{:S(2)}, u32[]{:S(2)}) collective-permute-start(bf16[80,512]{1,0:T(8,128)(2,1)S(1)} %get-tuple-element.127), channel_id=1, source_target_pairs={{0,24},{8,0},{16,8},{24,16},{1,25},{9,1},{17,9},{25,17},{2,26},{10... | collective-permute-start | bytes 245768 | tf_op jit(solution)/shard_map/ppermute | solution.py:30
  81.6 8.8 %collective-permute-start.30 = (bf16[80,512]{1,0:T(8,128)(2,1)S(1)}, bf16[80,512]{1,0:T(8,128)(2,1)S(1)}, u32[]{:S(2)}, u32[]{:S(2)}) collective-permute-start(bf16[80,512]{1,0:T(8,128)(2,1)S(1)} %get-tuple-element.126), channel_id=1, source_target_pairs={{0,16},{8,24},{16,0},{24,8},{1,17},{9,25},{17,1},{25,9},{2,18},{10... | collective-permute-start | bytes 245768 | tf_op jit(solution)/shard_map/ppermute | solution.py:30
  99.5 9.7 %collective-permute-start.33 = (bf16[1,256]{1,0:T(2,128)(2,1)S(1)}, bf16[1,256]{1,0:T(2,128)(2,1)S(1)}, u32[]{:S(2)}, u32[]{:S(2)}) collective-permute-start(bf16[1,256]{1,0:T(2,128)(2,1)S(1)} %get-tuple-element.115), channel_id=1, source_target_pairs={{0,4},{4,8},{8,12},{12,16},{16,20},{20,24},{24,28},{1,5},{5,9},{9,... | collective-permute-start | bytes 1544 | tf_op jit(solution)/shard_map/ppermute | solution.py:535
  104.2 13.9 %all-to-all-start = ((bf16[8,64,256]{2,1,0:T(8,128)(2,1)}), bf16[8,64,256]{2,1,0:T(8,128)(2,1)S(1)}, u32[]{:S(2)}, u32[]{:S(2)}) async-start(bf16[8,64,256]{2,1,0:T(8,128)(2,1)} %get-tuple-element.116), calls=%async_computation | async-start | bytes 524288 | tf_op jit(solution)/shard_map/all_to_all | solution.py:529
  (26 other events, 304.0 us)

commit v7 on v6

--- a/solution.py
+++ b/solution.py
@@ -40,11 +40,11 @@
     return lax.dot_general(a, b, (((ca,), (cb,)), ((), ())), preferred_element_type=F32)
 
 
-def prepare(experts, cap, quarter, index_ref, routes_ref, weights_ref, resid_ref, grad_ref, *outs):
+def prepare(experts, cap, quarter, routes_ref, weights_ref, resid_ref, grad_ref, *outs):
     sel_ref = outs[-1]
     sends = ((outs[0], outs[1]), *[(send.at[0], send.at[1]) for send in outs[2:-1]])
     tokens = resid_ref.shape[0]
-    mine, column = index_ref[0], index_ref[1]
+    mine, column = lax.axis_index("e"), 2 * lax.axis_index("x") + lax.axis_index("c")
     resid = resid_ref[...].astype(F32)
     inv_rms = lax.rsqrt(jnp.mean(resid * resid, axis=-1, keepdims=True) + epsilon)
     cols = pl.ds(pl.multiple_of(column * quarter, quarter), quarter)
@@ -97,7 +97,6 @@
 
 def first_half(
     cap,
-    place_ref,
     own_ref,
     own_sib_ref,
     own_y_ref,
@@ -118,7 +117,7 @@
     near_out_ref,
     half_ref,
 ):
-    place = place_ref[1]
+    place = 2 * lax.axis_index("x") + lax.axis_index("c")
     quarter = pair_ref.shape[-1]
     count = cap + pair_ref.shape[1]
     sides = (
@@ -143,7 +142,6 @@
 
 def second_half(
     cap,
-    place_ref,
     rows_y_ref,
     rows_y_sib_ref,
     far_own_ref,
@@ -165,7 +163,7 @@
     late_slope_ref,
     late_active_ref,
 ):
-    place = place_ref[1]
+    place = 2 * lax.axis_index("x") + lax.axis_index("c")
     quarter = far_ref.shape[-1]
     count = cap + far_ref.shape[1]
     early = slope_ref.shape[0]
@@ -196,8 +194,8 @@
         ).astype(BF16)
 
 
-def kept_part(place_ref, d_gate_ref, d_up_ref, gate_ref, up_ref, kept_ref):
-    place = place_ref[1]
+def kept_part(d_gate_ref, d_up_ref, gate_ref, up_ref, kept_ref):
+    place = 2 * lax.axis_index("x") + lax.axis_index("c")
     quarter = kept_ref.shape[1] // 2
     for dx in range(2):
         block = columns(place, 2 * dx, quarter)
@@ -206,7 +204,7 @@
         ) + dot(d_up_ref[...], up_ref[block], 1, 1)
 
 
-def join(place_ref, kept_ref, other_ref, *block_refs):
+def join(kept_ref, other_ref, *block_refs):
     cap, rest, quarter = block_refs[0].shape[0], block_refs[4].shape[0], block_refs[0].shape[1]
     for i in range(4):
         dj, dx = divmod(i, 2)
@@ -221,8 +219,8 @@
             ).astype(BF16)
 
 
-def grad_of_down(place_ref, near_ref, far_ref, early_ref, late_ref, down_ref):
-    place = place_ref[1]
+def grad_of_down(near_ref, far_ref, early_ref, late_ref, down_ref):
+    place = 2 * lax.axis_index("x") + lax.axis_index("c")
     early = early_ref.shape[0]
     quarter = near_ref.shape[1] // 2
     for dx, grads in enumerate((near_ref, far_ref)):
@@ -234,7 +232,7 @@
             ).astype(BF16)
 
 
-def grad_of_up(place_ref, early_ref, late_ref, d_up_ref, up_ref):
+def grad_of_up(early_ref, late_ref, d_up_ref, up_ref):
     early, features = early_ref.shape
     quarter = features // 4
     for q in range(4):
@@ -245,10 +243,10 @@
         ).astype(BF16)
 
 
-def order_mixed(index_ref, *refs):
+def order_mixed(*refs):
     came, outs = refs[:-2], refs[-2:]
     experts = len(came)
-    mine, half, core = index_ref[0], index_ref[2], index_ref[3]
+    mine, half, core = lax.axis_index("e"), lax.axis_index("j"), lax.axis_index("c")
     _, part, quarter = came[0].shape
     channels = quarter // 2
     for s in range(experts):
@@ -261,7 +259,6 @@
 
 
 def finish(
-    core_ref,
     d_normed_ref,
     resid_ref,
     grad_ref,
@@ -285,7 +282,7 @@
     ).astype(BF16)
     out_ref[...] = grad_resid
     count, part, width = blocks_ref.shape
-    mine = pl.ds(pl.multiple_of(core_ref[3] * part, part), part)
+    mine = pl.ds(pl.multiple_of(lax.axis_index("c") * part, part), part)
     for s in range(count):
         blocks_ref[s] = out_ref[mine, s * width : (s + 1) * width]
     d_mix = dot(grad_resid, w_out_ref[...], 1, 1)
@@ -296,17 +293,17 @@
     last_ref[...] = d_conv[-1:].astype(BF16)
 
 
-def in_vmem(kernel, outs, scratch, flops, limit, scalars, *values):
+def in_vmem(kernel, outs, scratch, flops, limit, *values):
     vmem = pl.BlockSpec(memory_space=pltpu.VMEM)
     return pl.pallas_call(
         kernel,
         out_shape=[jax.ShapeDtypeStruct(shape, kind) for shape, kind in outs],
-        in_specs=[pl.BlockSpec(memory_space=pltpu.SMEM)] + [vmem] * len(values),
+        in_specs=[vmem] * len(values),
         out_specs=[vmem] * len(outs),
         scratch_shapes=scratch,
         cost_estimate=pl.CostEstimate(flops=flops, bytes_accessed=0, transcendentals=0),
         compiler_params=pltpu.CompilerParams(vmem_limit_bytes=limit),
-    )(scalars, *values)
+    )(*values)
 
 
 def per_device(
@@ -329,10 +326,6 @@
     slices = 2 * experts
     cap = -(-(5 * tokens // slices) // 16) * 16
     quarter = features // 4
-    mine, half, core = lax.axis_index("e"), lax.axis_index("j"), lax.axis_index("c")
-    place = 2 * lax.axis_index("x") + core
-    index = jnp.stack([mine, place, half, core]).astype(jnp.int32)
-
     outs = in_vmem(
         functools.partial(prepare, experts, cap, quarter),
         [((cap, quarter), BF16)] * 2
@@ -341,7 +334,6 @@
         [],
         4 * experts * cap * tokens * quarter,
         60 * 2**20,
-        index,
         routes.T,
         route_weights.T,
         residual,
@@ -367,8 +359,10 @@
     grads_z = jnp.concatenate([b[1] for b in came], axis=0)
     count = experts * cap
 
-    rows_x, grads_y, own_y, own_far = lax.optimization_barrier(
-        (swap(rows_z, "x"), swap(grads_z, "j"), own_y, own_far)
+    mixed_mine = jnp.stack([own_pair[2 * cap :], own_y[2 * cap :]])
+    mixed_rel = [mixed_mine] + exchange([mixed_mine] * (experts - 1), 1)
+    rows_x, grads_y, own_far = lax.optimization_barrier(
+        (swap(rows_z, "x"), swap(grads_z, "j"), own_far)
     )
     pair = jnp.stack([rows_z, rows_x])
     near = jnp.stack([grads_z, grads_y])
@@ -394,7 +388,6 @@
         [],
         (4 * early + 2 * count) * features * hidden_units,
         grant,
-        index,
         *sib(own_pair),
         *sib(own_y),
         *sib(pair),
@@ -415,7 +408,6 @@
         [pltpu.VMEM((2 * count - early, hidden_units), F32)] * 2,
         (4 * (2 * count - early) + 6 * count) * features * hidden_units,
         grant,
-        index,
         *sib(rows_y),
         own_far,
         own_far_sib,
@@ -433,7 +425,6 @@
         [],
         4 * count * features * hidden_units,
         grant,
-        index,
         d_gate,
         d_up,
         *weights[:2],
@@ -444,12 +435,9 @@
         [],
         2 * count * features,
         grant,
-        index,
         kept,
         other,
     )
-    mixed_mine = jnp.stack([own_pair[2 * cap :], own_y[2 * cap :]])
-    mixed_rel = [mixed_mine] + exchange([mixed_mine] * (experts - 1), 1)
 
     def spread(parts):
         return [parts[0], swap(parts[1], "x"), swap(parts[2], "j"), swap_both(parts[3])]
@@ -469,7 +457,6 @@
         [],
         4 * count * features * hidden_units,
         2 * grant,
-        index,
         grads_near,
         grads_far,
         hidden_early,
@@ -481,7 +468,6 @@
         [],
         4 * count * features * hidden_units,
         2 * grant,
-        index,
         rows_early,
         rows_late,
         d_up,
@@ -506,7 +492,6 @@
         [],
         16 * tokens * features,
         8 * 2**20,
-        index,
         d_normed,
         residual,
         out_grad,
@@ -521,7 +506,6 @@
         [],
         2 * slices * part * channels,
         grant,
-        index,
         *mixed_rel,
     )
     if cut == 1:

time: 121 us -> 121 us (level)
  waiting for transfers between devices: 36 us -> 43.1 us
  Pallas kernels: 23.2 us -> 18.8 us
  other arithmetic: 4.08 us -> 1.74 us
    pallas_call x9, Pallas kernels: 23.2 us -> 18.8 us  [in_vmem(): pl.pallas_call(kernel, out_shape=[jax.ShapeDtypeStruct(shape, kind) for s...]
    ppermute x9, waiting for transfers between devices: 4.26 us -> 7.87 us  [exchange(): lax.ppermute(b, 'e', [(i, (i + sign * s) % count) for i in range(count)])]
    ppermute x22, waiting for transfers between devices: 23.6 us -> 27.1 us  [swap(): return lax.ppermute(value, axis, [(0, 1), (1, 0)])]
  transfers between devices with their start and end apart: 36 -> 36, of which waited for: 14 -> 15; matrix products, arithmetic and copies ran while one was open for 3% -> 2% of each run, Pallas kernels for 11% -> 9%
where the time goes in v7:
time: 121 us
  starting transfers between devices  47.1 us (39%)
  waiting for transfers between devices  43.1 us (36%)
  Pallas kernels  18.8 us (16%)
  blocking collectives  7.31 us (6%)
  other arithmetic  1.74 us (1%)
  matrix products  1.49 us (1%)
    ppermute x22, waiting for transfers between devices, swap(): return lax.ppermute(value, axis, [(0, 1), (1, 0)])  27.1 us
    pallas_call x9, Pallas kernels, in_vmem(): pl.pallas_call(kernel, out_shape=[jax.ShapeDtypeStruct(shape, kind) for s...  18.8 us
    ppermute x9, starting transfers between devices, exchange(): lax.ppermute(b, 'e', [(i, (i + sign * s) % count) for i in range(count)])  18.4 us
    ppermute x22, starting transfers between devices, swap(): return lax.ppermute(value, axis, [(0, 1), (1, 0)])  16.3 us
    all_to_all x1, waiting for transfers between devices, per_device(): lax.all_to_all(blocks, ('e', 'j'), 0, 0, tiled=True)  8.12 us
    ppermute x9, waiting for transfers between devices, exchange(): lax.ppermute(b, 'e', [(i, (i + sign * s) % count) for i in range(count)])  7.87 us
    all_gather x1, blocking collectives, per_device(): d_normed = lax.all_gather(d_part, ('x', 'c'), axis=1, tiled=True)  7.31 us
    all_to_all x1, starting transfers between devices, per_device(): lax.all_to_all(blocks, ('e', 'j'), 0, 0, tiled=True)  4.56 us
  transfers between devices with their start and end apart: 36, of which 15 were waited for; matrix products, arithmetic and copies ran while one was open for 2% of the time, Pallas kernels for 9%

profile of v7, /device:TPU:0, one launch (start us, length us, event | category | flops | bytes accessed | tf_op | source)
XLA Modules:
  0.0 120.7 jit_solution(11043907677529087180)
XLA Ops:
  0.6 2.6 %shard_map.180 = (bf16[80,512]{1,0:T(8,128)(2,1)}, bf16[80,512]{1,0:T(8,128)(2,1)}, bf16[2,80,512]{2,1,0:T(8,128)(2,1)}, bf16[2,80,512]{2,1,0:T(8,128)(2,1)}, bf...) custom-call(s32[2,128]{1,0:T(2,128)} %bitcast.56, f32[2,128]{1,0:T(2,128)} %bitcast.57, ...), custom_call_target="tpu_custom_call" | custom-call | flops 83886080 | tf_op jit(solution)/shard_map/pallas_call | solution.py:298
  3.3 3.1 %collective-permute-start = (bf16[2,80,512]{2,1,0:T(8,128)(2,1)}, bf16[2,80,512]{2,1,0:T(8,128)(2,1)S(1)}, u32[]{:S(2)}, u32[]{:S(2)}) collective-permute-start(bf16[2,80,512]{2,1,0:T(8,128)(2,1)} %get-tuple-element.65), channel_id=1, source_target_pairs={{0,8},{8,16},{16,24},{24,0},{1,9},{9,17},{17,25},{25,1},{2,10},{10... | collective-permute-start | bytes 491528 | tf_op jit(solution)/shard_map/ppermute | solution.py:30
  6.3 2.6 %collective-permute-start.1 = (bf16[2,80,512]{2,1,0:T(8,128)(2,1)}, bf16[2,80,512]{2,1,0:T(8,128)(2,1)S(1)}, u32[]{:S(2)}, u32[]{:S(2)}) collective-permute-start(bf16[2,80,512]{2,1,0:T(8,128)(2,1)} %get-tuple-element.66), channel_id=1, source_target_pairs={{0,16},{8,24},{16,0},{24,8},{1,17},{9,25},{17,1},{25,9},{2,18},{10... | collective-permute-start | bytes 491528 | tf_op jit(solution)/shard_map/ppermute | solution.py:30
  13.3 1.6 %collective-permute-done.5 = bf16[80,512]{1,0:T(8,128)(2,1)S(1)} collective-permute-done((bf16[80,512]{1,0:T(8,128)(2,1)}, bf16[80,512]{1,0:T(8,128)(2,1)S(1)}, u32[]{:S(2)}, u32[]{:S(2)}) %collective-permute-start.5) | collective-permute-done | bytes 81952 | tf_op jit(solution)/shard_map/ppermute | solution.py:18
  16.4 3.5 %collective-permute-done.1 = bf16[2,80,512]{2,1,0:T(8,128)(2,1)S(1)} collective-permute-done((bf16[2,80,512]{2,1,0:T(8,128)(2,1)}, bf16[2,80,512]{2,1,0:T(8,128)(2,1)S(1)}, u32[]{:S(2)}, u32[]{:S(2)}) %collective-permute-start.1) | collective-permute-done | bytes 163872 | tf_op jit(solution)/shard_map/ppermute | solution.py:30
  23.8 7.6 %collective-permute-done.7.far_own_ref = bf16[2,80,512]{2,1,0:T(8,128)(2,1)S(1)} collective-permute-done((bf16[2,80,512]{2,1,0:T(8,128)(2,1)S(1)}, bf16[2,80,512]{2,1,0:T(8,128)(2,1)S(1)}, u32[]{:S(2)}, u32[]{:S(2)}) %collective-permute-start.7) | collective-permute-done | bytes 163872 | tf_op jit(solution)/shard_map/ppermute | solution.py:18
  31.4 1.6 %collective-permute-start.8 = (bf16[2,240,512]{2,1,0:T(8,128)(2,1)S(1)}, bf16[2,240,512]{2,1,0:T(8,128)(2,1)S(1)}, u32[]{:S(2)}, u32[]{:S(2)}) collective-permute-start(bf16[2,240,512]{2,1,0:T(8,128)(2,1)S(1)} %pad_maximum_fusion.pair_ref), channel_id=1, source_target_pairs={{0,4},{4,0},{1,5},{5,1},{2,6},{6,2},{3,7},{7,3},{8,12},{12,8},{9,1... | collective-permute-start | bytes 1474568 | tf_op jit(solution)/shard_map/ppermute | solution.py:18
  36.3 7.4 %collective-permute-done.8.rows_y_ref = bf16[2,240,512]{2,1,0:T(8,128)(2,1)S(1)} collective-permute-done((bf16[2,240,512]{2,1,0:T(8,128)(2,1)S(1)}, bf16[2,240,512]{2,1,0:T(8,128)(2,1)S(1)}, u32[]{:S(2)}, u32[]{:S(2)}) %collective-permute-start.8) | collective-permute-done | bytes 491552 | tf_op jit(solution)/shard_map/ppermute | solution.py:18
  47.1 2.6 %collective-permute-done.14.own_y_ref = bf16[224,512]{1,0:T(8,128)(2,1)S(1)} collective-permute-done((bf16[224,512]{1,0:T(8,128)(2,1)S(1)}, bf16[224,512]{1,0:T(8,128)(2,1)S(1)}, u32[]{:S(2)}, u32[]{:S(2)}) %collective-permute-start.14) | collective-permute-done | bytes 229408 | tf_op jit(solution)/shard_map/ppermute | solution.py:18
  51.2 2.8 %shard_map.181 = (bf16[400,2048]{1,0:T(8,128)(2,1)S(1)}, f32[400,512]{1,0:T(8,128)S(1)}, f32[400,512]{1,0:T(8,128)S(1)}, bf16[400,512]{1,0:T(8,128)(2,1)S(1)}, b...) custom-call(bf16[224,512]{1,0:T(8,128)(2,1)S(1)} %maximum_maximum_fusion.own_ref, ...), custom_call_target="tpu_custom_call" | custom-call | flops 2348810240 | tf_op jit(solution)/shard_map/pallas_call | solution.py:298
  54.1 3.6 %shard_map.182 = (bf16[240,2048]{1,0:T(8,128)(2,1)S(1)}, bf16[640,1024]{1,0:T(8,128)(2,1)S(1)}, bf16[240,512]{1,0:T(8,128)(2,1)S(1)}, bf16[640,512]{1,0:T(8,128)...) custom-call(bf16[2,240,512]{2,1,0:T(8,128)(2,1)S(1)} %collective-permute-done.8.rows_y_ref, ...), custom_call_target="tpu_custom_call" | custom-call | flops 3019898880 | tf_op jit(solution)/shard_map/pallas_call | solution.py:298
  61.0 2.5 %collective-permute-start.25 = (bf16[240,512]{1,0:T(8,128)(2,1)S(1)}, bf16[240,512]{1,0:T(8,128)(2,1)S(1)}, u32[]{:S(2)}, u32[]{:S(2)}) collective-permute-start(bf16[240,512]{1,0:T(8,128)(2,1)S(1)} %get-tuple-element.94), channel_id=1, source_target_pairs={{0,6},{2,4},{4,2},{6,0},{1,7},{3,5},{5,3},{7,1},{8,14},{10,12},{12... | collective-permute-start | bytes 737288 | tf_op jit(solution)/shard_map/ppermute | solution.py:22
  64.6 4.2 %collective-permute-start.26 = (bf16[2,64,512]{2,1,0:T(8,128)(2,1)S(1)}, bf16[2,64,512]{2,1,0:T(8,128)(2,1)S(1)}, u32[]{:S(2)}, u32[]{:S(2)}) collective-permute-start(bf16[2,64,512]{2,1,0:T(8,128)(2,1)S(1)} %pad_maximum_fusion.5.refs_0_), channel_id=1, source_target_pairs={{0,8},{8,16},{16,24},{24,0},{1,9},{9,17},{17,25},{25,1},{2,10},{10... | collective-permute-start | bytes 393224 | tf_op jit(solution)/shard_map/ppermute | solution.py:30
  68.8 3.2 %shard_map.186 = bf16[1,2048,512]{2,1,0:T(8,128)(2,1)} custom-call(bf16[400,2048]{1,0:T(8,128)(2,1)S(1)} %get-tuple-element.104.early_ref, bf16[240,2048]{1,0:T(8,128)(2,1)S(1)} %get-tuple-element.105.late_ref, bf16[640,512]{1,0:T(8,128)(2,1)S(1)} %get-tuple-element.85.d_up_ref), custom_call_target="tpu_custom_call" | custom-call | flops 1342177280 | tf_op jit(solution)/shard_map/pallas_call | solution.py:298
  72.0 2.4 %collective-permute-start.28 = (bf16[2,64,512]{2,1,0:T(8,128)(2,1)S(1)}, bf16[2,64,512]{2,1,0:T(8,128)(2,1)S(1)}, u32[]{:S(2)}, u32[]{:S(2)}) collective-permute-start(bf16[2,64,512]{2,1,0:T(8,128)(2,1)S(1)} %pad_maximum_fusion.5.refs_0_), channel_id=1, source_target_pairs={{0,24},{8,0},{16,8},{24,16},{1,25},{9,1},{17,9},{25,17},{2,26},{10... | collective-permute-start | bytes 393224 | tf_op jit(solution)/shard_map/ppermute | solution.py:30
  79.9 2.8 %collective-permute-start.29 = (bf16[80,512]{1,0:T(8,128)(2,1)S(1)}, bf16[80,512]{1,0:T(8,128)(2,1)S(1)}, u32[]{:S(2)}, u32[]{:S(2)}) collective-permute-start(bf16[80,512]{1,0:T(8,128)(2,1)S(1)} %get-tuple-element.125), channel_id=1, source_target_pairs={{0,24},{8,0},{16,8},{24,16},{1,25},{9,1},{17,9},{25,17},{2,26},{10... | collective-permute-start | bytes 245768 | tf_op jit(solution)/shard_map/ppermute | solution.py:30
  82.6 2.0 %collective-permute-start.30 = (bf16[80,512]{1,0:T(8,128)(2,1)S(1)}, bf16[80,512]{1,0:T(8,128)(2,1)S(1)}, u32[]{:S(2)}, u32[]{:S(2)}) collective-permute-start(bf16[80,512]{1,0:T(8,128)(2,1)S(1)} %get-tuple-element.124), channel_id=1, source_target_pairs={{0,16},{8,24},{16,0},{24,8},{1,17},{9,25},{17,1},{25,9},{2,18},{10... | collective-permute-start | bytes 245768 | tf_op jit(solution)/shard_map/ppermute | solution.py:30
  84.7 3.2 %shard_map.187 = bf16[1,512,2048]{2,1,0:T(8,128)(2,1)} custom-call(bf16[640,1024]{1,0:T(8,128)(2,1)S(1)} %get-tuple-element.106.near_ref, bf16[640,1024]{1,0:T(8,128)(2,1)S(1)} %get-tuple-element.107.far_ref, bf16[400,512]{1,0:T(8,128)(2,1)S(1)} %get-tuple-element.108.early_ref, bf16[240,512]{1,0:T(8,128)(2,1)S(1)} %get-tuple-element.109.late_ref), custom_call_target="tpu_custom_call" | custom-call | flops 1342177280 | tf_op jit(solution)/shard_map/pallas_call | solution.py:298
  87.9 3.5 %collective-permute-done.30 = bf16[80,512]{1,0:T(8,128)(2,1)S(1)} collective-permute-done((bf16[80,512]{1,0:T(8,128)(2,1)S(1)}, bf16[80,512]{1,0:T(8,128)(2,1)S(1)}, u32[]{:S(2)}, u32[]{:S(2)}) %collective-permute-start.30) | collective-permute-done | bytes 81952 | tf_op jit(solution)/shard_map/ppermute | solution.py:30
  91.7 7.3 %all_gather.3.d_normed_ref = bf16[128,2048]{1,0:T(8,128)(2,1)S(1)} all-gather(bf16[128,512]{1,0:T(8,128)(2,1)S(1)} %convolution_convert_fusion), channel_id=1, replica_groups=mesh['e'=4,'j'=2,'x'=2,'c'=2] {'x','c'}, dimensions={1}, use_global_device_ids=true | all-gather | bytes 655360 | tf_op jit(solution)/shard_map/all_gather | solution.py:479
  99.1 1.6 %shard_map.185 = (bf16[128,2048]{1,0:T(8,128)(2,1)}, bf16[8,64,256]{2,1,0:T(8,128)(2,1)}, bf16[128,256]{1,0:T(8,128)(2,1)}, f32[128,256]{1,0:T(8,128)S(1)}, bf16...) custom-call(bf16[128,2048]{1,0:T(8,128)(2,1)S(1)} %all_gather.3.d_normed_ref, bf16[128,2048]{1,0:T(8,128)(2,1)S(1)} %copy-done.3, ...), custom_call_target="tpu_custom_call" | custom-call | flops 4194304 | tf_op jit(solution)/shard_map/pallas_call | solution.py:298
  100.7 2.7 %collective-permute-start.33 = (bf16[1,256]{1,0:T(2,128)(2,1)S(1)}, bf16[1,256]{1,0:T(2,128)(2,1)S(1)}, u32[]{:S(2)}, u32[]{:S(2)}) collective-permute-start(bf16[1,256]{1,0:T(2,128)(2,1)S(1)} %get-tuple-element.113), channel_id=1, source_target_pairs={{0,4},{4,8},{8,12},{12,16},{16,20},{20,24},{24,28},{1,5},{5,9},{9,... | collective-permute-start | bytes 1544 | tf_op jit(solution)/shard_map/ppermute | solution.py:519
  104.7 4.6 %all-to-all-start = ((bf16[8,64,256]{2,1,0:T(8,128)(2,1)}), bf16[8,64,256]{2,1,0:T(8,128)(2,1)S(1)}, u32[]{:S(2)}, u32[]{:S(2)}) async-start(bf16[8,64,256]{2,1,0:T(8,128)(2,1)} %get-tuple-element.114), calls=%async_computation | async-start | bytes 524288 | tf_op jit(solution)/shard_map/all_to_all | solution.py:513
  110.0 8.1 %all-to-all-done = bf16[8,64,256]{2,1,0:T(8,128)(2,1)S(1)} async-done(((bf16[8,64,256]{2,1,0:T(8,128)(2,1)}), bf16[8,64,256]{2,1,0:T(8,128)(2,1)S(1)}, u32[]{:S(2)}, u32[]{:S(2)}) %all-to-all-start) | async-done | bytes 262176 | tf_op jit(solution)/shard_map/all_to_all | solution.py:513
  (111 shorter events, 32.6 us)
Async XLA Ops:
  3.3 13.1 %collective-permute-start = (bf16[2,80,512]{2,1,0:T(8,128)(2,1)}, bf16[2,80,512]{2,1,0:T(8,128)(2,1)S(1)}, u32[]{:S(2)}, u32[]{:S(2)}) collective-permute-start(bf16[2,80,512]{2,1,0:T(8,128)(2,1)} %get-tuple-element.65), channel_id=1, source_target_pairs={{0,8},{8,16},{16,24},{24,0},{1,9},{9,17},{17,25},{25,1},{2,10},{10... | collective-permute-start | bytes 491528 | tf_op jit(solution)/shard_map/ppermute | solution.py:30
  6.3 13.5 %collective-permute-start.1 = (bf16[2,80,512]{2,1,0:T(8,128)(2,1)}, bf16[2,80,512]{2,1,0:T(8,128)(2,1)S(1)}, u32[]{:S(2)}, u32[]{:S(2)}) collective-permute-start(bf16[2,80,512]{2,1,0:T(8,128)(2,1)} %get-tuple-element.66), channel_id=1, source_target_pairs={{0,16},{8,24},{16,0},{24,8},{1,17},{9,25},{17,1},{25,9},{2,18},{10... | collective-permute-start | bytes 491528 | tf_op jit(solution)/shard_map/ppermute | solution.py:30
  8.9 11.0 %collective-permute-start.2 = (bf16[2,80,512]{2,1,0:T(8,128)(2,1)}, bf16[2,80,512]{2,1,0:T(8,128)(2,1)S(1)}, u32[]{:S(2)}, u32[]{:S(2)}) collective-permute-start(bf16[2,80,512]{2,1,0:T(8,128)(2,1)} %get-tuple-element.67), channel_id=1, source_target_pairs={{0,24},{8,0},{16,8},{24,16},{1,25},{9,1},{17,9},{25,17},{2,26},{10... | collective-permute-start | bytes 491528 | tf_op jit(solution)/shard_map/ppermute | solution.py:30
  20.0 11.4 %collective-permute-start.3 = (bf16[240,512]{1,0:T(8,128)(2,1)S(1)}, bf16[240,512]{1,0:T(8,128)(2,1)S(1)}, u32[]{:S(2)}, u32[]{:S(2)}) collective-permute-start(bf16[240,512]{1,0:T(8,128)(2,1)S(1)} %get-tuple-element.129), channel_id=1, source_target_pairs={{0,2},{2,0},{1,3},{3,1},{4,6},{6,4},{5,7},{7,5},{8,10},{10,8},{9,1... | collective-permute-start | bytes 737288 | tf_op jit(solution)/shard_map/ppermute | solution.py:18
  21.6 9.8 %collective-permute-start.4 = (bf16[240,512]{1,0:T(8,128)(2,1)S(1)}, bf16[240,512]{1,0:T(8,128)(2,1)S(1)}, u32[]{:S(2)}, u32[]{:S(2)}) collective-permute-start(bf16[240,512]{1,0:T(8,128)(2,1)S(1)} %get-tuple-element.127), channel_id=1, source_target_pairs={{0,4},{4,0},{1,5},{5,1},{2,6},{6,2},{3,7},{7,3},{8,12},{12,8},{9,1... | collective-permute-start | bytes 737288 | tf_op jit(solution)/shard_map/ppermute | solution.py:18
  23.2 8.2 %collective-permute-start.7 = (bf16[2,80,512]{2,1,0:T(8,128)(2,1)S(1)}, bf16[2,80,512]{2,1,0:T(8,128)(2,1)S(1)}, u32[]{:S(2)}, u32[]{:S(2)}) collective-permute-start(bf16[2,80,512]{2,1,0:T(8,128)(2,1)S(1)} %pad_maximum_fusion.4.near_own_ref), channel_id=1, source_target_pairs={{0,2},{2,0},{1,3},{3,1},{4,6},{6,4},{5,7},{7,5},{8,10},{10,8},{9,1... | collective-permute-start | bytes 491528 | tf_op jit(solution)/shard_map/ppermute | solution.py:18
  31.4 12.3 %collective-permute-start.8 = (bf16[2,240,512]{2,1,0:T(8,128)(2,1)S(1)}, bf16[2,240,512]{2,1,0:T(8,128)(2,1)S(1)}, u32[]{:S(2)}, u32[]{:S(2)}) collective-permute-start(bf16[2,240,512]{2,1,0:T(8,128)(2,1)S(1)} %pad_maximum_fusion.pair_ref), channel_id=1, source_target_pairs={{0,4},{4,0},{1,5},{5,1},{2,6},{6,2},{3,7},{7,3},{8,12},{12,8},{9,1... | collective-permute-start | bytes 1474568 | tf_op jit(solution)/shard_map/ppermute | solution.py:18
  33.1 12.1 %collective-permute-start.9 = (bf16[2,240,512]{2,1,0:T(8,128)(2,1)S(1)}, bf16[2,240,512]{2,1,0:T(8,128)(2,1)S(1)}, u32[]{:S(2)}, u32[]{:S(2)}) collective-permute-start(bf16[2,240,512]{2,1,0:T(8,128)(2,1)S(1)} %pad_maximum_fusion.1.near_ref), channel_id=1, source_target_pairs={{0,2},{2,0},{1,3},{3,1},{4,6},{6,4},{5,7},{7,5},{8,10},{10,8},{9,1... | collective-permute-start | bytes 1474568 | tf_op jit(solution)/shard_map/ppermute | solution.py:18
  34.8 12.0 %collective-permute-start.13 = (bf16[224,512]{1,0:T(8,128)(2,1)S(1)}, bf16[224,512]{1,0:T(8,128)(2,1)S(1)}, u32[]{:S(2)}, u32[]{:S(2)}) collective-permute-start(bf16[224,512]{1,0:T(8,128)(2,1)S(1)} %maximum_maximum_fusion.own_ref), channel_id=1, source_target_pairs={{0,1},{1,0},{2,3},{3,2},{4,5},{5,4},{6,7},{7,6},{8,9},{9,8},{10,11... | collective-permute-start | bytes 688136 | tf_op jit(solution)/shard_map/ppermute | solution.py:18
  35.3 15.9 %collective-permute-start.16 = (bf16[2,240,512]{2,1,0:T(8,128)(2,1)S(1)}, bf16[2,240,512]{2,1,0:T(8,128)(2,1)S(1)}, u32[]{:S(2)}, u32[]{:S(2)}) collective-permute-start(bf16[2,240,512]{2,1,0:T(8,128)(2,1)S(1)} %pad_maximum_fusion.pair_ref), channel_id=1, source_target_pairs={{0,1},{1,0},{2,3},{3,2},{4,5},{5,4},{6,7},{7,6},{8,9},{9,8},{10,11... | collective-permute-start | bytes 1474568 | tf_op jit(solution)/shard_map/ppermute | solution.py:18
  36.1 15.1 %collective-permute-start.18 = (bf16[2,240,512]{2,1,0:T(8,128)(2,1)S(1)}, bf16[2,240,512]{2,1,0:T(8,128)(2,1)S(1)}, u32[]{:S(2)}, u32[]{:S(2)}) collective-permute-start(bf16[2,240,512]{2,1,0:T(8,128)(2,1)S(1)} %pad_maximum_fusion.1.near_ref), channel_id=1, source_target_pairs={{0,1},{1,0},{2,3},{3,2},{4,5},{5,4},{6,7},{7,6},{8,9},{9,8},{10,11... | collective-permute-start | bytes 1474568 | tf_op jit(solution)/shard_map/ppermute | solution.py:18
  61.0 11.0 %collective-permute-start.25 = (bf16[240,512]{1,0:T(8,128)(2,1)S(1)}, bf16[240,512]{1,0:T(8,128)(2,1)S(1)}, u32[]{:S(2)}, u32[]{:S(2)}) collective-permute-start(bf16[240,512]{1,0:T(8,128)(2,1)S(1)} %get-tuple-element.94), channel_id=1, source_target_pairs={{0,6},{2,4},{4,2},{6,0},{1,7},{3,5},{5,3},{7,1},{8,14},{10,12},{12... | collective-permute-start | bytes 737288 | tf_op jit(solution)/shard_map/ppermute | solution.py:22
  63.5 11.7 %collective-permute-start.24 = (bf16[240,512]{1,0:T(8,128)(2,1)S(1)}, bf16[240,512]{1,0:T(8,128)(2,1)S(1)}, u32[]{:S(2)}, u32[]{:S(2)}) collective-permute-start(bf16[240,512]{1,0:T(8,128)(2,1)S(1)} %get-tuple-element.93), channel_id=1, source_target_pairs={{0,4},{4,0},{1,5},{5,1},{2,6},{6,2},{3,7},{7,3},{8,12},{12,8},{9,1... | collective-permute-start | bytes 737288 | tf_op jit(solution)/shard_map/ppermute | solution.py:18
  64.0 12.7 %collective-permute-start.23 = (bf16[240,512]{1,0:T(8,128)(2,1)S(1)}, bf16[240,512]{1,0:T(8,128)(2,1)S(1)}, u32[]{:S(2)}, u32[]{:S(2)}) collective-permute-start(bf16[240,512]{1,0:T(8,128)(2,1)S(1)} %get-tuple-element.92), channel_id=1, source_target_pairs={{0,2},{2,0},{1,3},{3,1},{4,6},{6,4},{5,7},{7,5},{8,10},{10,8},{9,1... | collective-permute-start | bytes 737288 | tf_op jit(solution)/shard_map/ppermute | solution.py:18
  64.6 13.1 %collective-permute-start.26 = (bf16[2,64,512]{2,1,0:T(8,128)(2,1)S(1)}, bf16[2,64,512]{2,1,0:T(8,128)(2,1)S(1)}, u32[]{:S(2)}, u32[]{:S(2)}) collective-permute-start(bf16[2,64,512]{2,1,0:T(8,128)(2,1)S(1)} %pad_maximum_fusion.5.refs_0_), channel_id=1, source_target_pairs={{0,8},{8,16},{16,24},{24,0},{1,9},{9,17},{17,25},{25,1},{2,10},{10... | collective-permute-start | bytes 393224 | tf_op jit(solution)/shard_map/ppermute | solution.py:30
  68.8 10.1 %collective-permute-start.27 = (bf16[2,64,512]{2,1,0:T(8,128)(2,1)S(1)}, bf16[2,64,512]{2,1,0:T(8,128)(2,1)S(1)}, u32[]{:S(2)}, u32[]{:S(2)}) collective-permute-start(bf16[2,64,512]{2,1,0:T(8,128)(2,1)S(1)} %pad_maximum_fusion.5.refs_0_), channel_id=1, source_target_pairs={{0,16},{8,24},{16,0},{24,8},{1,17},{9,25},{17,1},{25,9},{2,18},{10... | collective-permute-start | bytes 393224 | tf_op jit(solution)/shard_map/ppermute | solution.py:30
  72.0 7.8 %collective-permute-start.28 = (bf16[2,64,512]{2,1,0:T(8,128)(2,1)S(1)}, bf16[2,64,512]{2,1,0:T(8,128)(2,1)S(1)}, u32[]{:S(2)}, u32[]{:S(2)}) collective-permute-start(bf16[2,64,512]{2,1,0:T(8,128)(2,1)S(1)} %pad_maximum_fusion.5.refs_0_), channel_id=1, source_target_pairs={{0,24},{8,0},{16,8},{24,16},{1,25},{9,1},{17,9},{25,17},{2,26},{10... | collective-permute-start | bytes 393224 | tf_op jit(solution)/shard_map/ppermute | solution.py:30
  75.2 9.4 %collective-permute-start.20 = (bf16[80,512]{1,0:T(8,128)(2,1)S(1)}, bf16[80,512]{1,0:T(8,128)(2,1)S(1)}, u32[]{:S(2)}, u32[]{:S(2)}) collective-permute-start(bf16[80,512]{1,0:T(8,128)(2,1)S(1)} %get-tuple-element.88), channel_id=1, source_target_pairs={{0,2},{2,0},{1,3},{3,1},{4,6},{6,4},{5,7},{7,5},{8,10},{10,8},{9,1... | collective-permute-start | bytes 245768 | tf_op jit(solution)/shard_map/ppermute | solution.py:18
  76.7 11.2 %collective-permute-start.21 = (bf16[80,512]{1,0:T(8,128)(2,1)S(1)}, bf16[80,512]{1,0:T(8,128)(2,1)S(1)}, u32[]{:S(2)}, u32[]{:S(2)}) collective-permute-start(bf16[80,512]{1,0:T(8,128)(2,1)S(1)} %get-tuple-element.89), channel_id=1, source_target_pairs={{0,4},{4,0},{1,5},{5,1},{2,6},{6,2},{3,7},{7,3},{8,12},{12,8},{9,1... | collective-permute-start | bytes 245768 | tf_op jit(solution)/shard_map/ppermute | solution.py:18
  77.7 10.2 %collective-permute-start.22 = (bf16[80,512]{1,0:T(8,128)(2,1)S(1)}, bf16[80,512]{1,0:T(8,128)(2,1)S(1)}, u32[]{:S(2)}, u32[]{:S(2)}) collective-permute-start(bf16[80,512]{1,0:T(8,128)(2,1)S(1)} %get-tuple-element.90), channel_id=1, source_target_pairs={{0,6},{2,4},{4,2},{6,0},{1,7},{3,5},{5,3},{7,1},{8,14},{10,12},{12... | collective-permute-start | bytes 245768 | tf_op jit(solution)/shard_map/ppermute | solution.py:22
  79.9 8.1 %collective-permute-start.29 = (bf16[80,512]{1,0:T(8,128)(2,1)S(1)}, bf16[80,512]{1,0:T(8,128)(2,1)S(1)}, u32[]{:S(2)}, u32[]{:S(2)}) collective-permute-start(bf16[80,512]{1,0:T(8,128)(2,1)S(1)} %get-tuple-element.125), channel_id=1, source_target_pairs={{0,24},{8,0},{16,8},{24,16},{1,25},{9,1},{17,9},{25,17},{2,26},{10... | collective-permute-start | bytes 245768 | tf_op jit(solution)/shard_map/ppermute | solution.py:30
  82.6 8.8 %collective-permute-start.30 = (bf16[80,512]{1,0:T(8,128)(2,1)S(1)}, bf16[80,512]{1,0:T(8,128)(2,1)S(1)}, u32[]{:S(2)}, u32[]{:S(2)}) collective-permute-start(bf16[80,512]{1,0:T(8,128)(2,1)S(1)} %get-tuple-element.124), channel_id=1, source_target_pairs={{0,16},{8,24},{16,0},{24,8},{1,17},{9,25},{17,1},{25,9},{2,18},{10... | collective-permute-start | bytes 245768 | tf_op jit(solution)/shard_map/ppermute | solution.py:30
  100.7 8.6 %collective-permute-start.33 = (bf16[1,256]{1,0:T(2,128)(2,1)S(1)}, bf16[1,256]{1,0:T(2,128)(2,1)S(1)}, u32[]{:S(2)}, u32[]{:S(2)}) collective-permute-start(bf16[1,256]{1,0:T(2,128)(2,1)S(1)} %get-tuple-element.113), channel_id=1, source_target_pairs={{0,4},{4,8},{8,12},{12,16},{16,20},{20,24},{24,28},{1,5},{5,9},{9,... | collective-permute-start | bytes 1544 | tf_op jit(solution)/shard_map/ppermute | solution.py:519
  104.7 13.4 %all-to-all-start = ((bf16[8,64,256]{2,1,0:T(8,128)(2,1)}), bf16[8,64,256]{2,1,0:T(8,128)(2,1)S(1)}, u32[]{:S(2)}, u32[]{:S(2)}) async-start(bf16[8,64,256]{2,1,0:T(8,128)(2,1)} %get-tuple-element.114), calls=%async_computation | async-start | bytes 524288 | tf_op jit(solution)/shard_map/all_to_all | solution.py:513
  (26 other events, 310.0 us)

commit v8 on v7

--- a/solution.py
+++ b/solution.py
@@ -333,11 +333,11 @@
         + [((experts, cap, tokens), BF16)],
         [],
         4 * experts * cap * tokens * quarter,
-        60 * 2**20,
-        routes.T,
-        route_weights.T,
-        residual,
-        out_grad,
+        16 * 2**20,
+        *[
+            pltpu.with_memory_space_constraint(v, pltpu.HBM)
+            for v in (routes.T, route_weights.T, residual, out_grad)
+        ],
     )
     own_rows, own_grads, sends, sel = outs[0], outs[1], outs[2:-1], outs[-1]
     conv_f32 = conv_out.astype(F32)

time: 121 us -> 120 us (level)
  no operation moved by 1% of the time
where the time goes in v8:
time: 120 us
  starting transfers between devices  47.1 us (39%)
  waiting for transfers between devices  42.9 us (36%)
  Pallas kernels  18.1 us (15%)
  blocking collectives  7.29 us (6%)
  other arithmetic  1.74 us (1%)
  matrix products  1.49 us (1%)
    ppermute x22, waiting for transfers between devices, swap(): return lax.ppermute(value, axis, [(0, 1), (1, 0)])  26.9 us
    ppermute x9, starting transfers between devices, exchange(): lax.ppermute(b, 'e', [(i, (i + sign * s) % count) for i in range(count)])  18.5 us
    pallas_call x9, Pallas kernels, in_vmem(): pl.pallas_call(kernel, out_shape=[jax.ShapeDtypeStruct(shape, kind) for s...  18.1 us
    ppermute x22, starting transfers between devices, swap(): return lax.ppermute(value, axis, [(0, 1), (1, 0)])  16.3 us
    all_to_all x1, waiting for transfers between devices, per_device(): lax.all_to_all(blocks, ('e', 'j'), 0, 0, tiled=True)  8.12 us
    ppermute x9, waiting for transfers between devices, exchange(): lax.ppermute(b, 'e', [(i, (i + sign * s) % count) for i in range(count)])  7.88 us
    all_gather x1, blocking collectives, per_device(): d_normed = lax.all_gather(d_part, ('x', 'c'), axis=1, tiled=True)  7.29 us
    all_to_all x1, starting transfers between devices, per_device(): lax.all_to_all(blocks, ('e', 'j'), 0, 0, tiled=True)  4.56 us
  transfers between devices with their start and end apart: 36, of which 15 were waited for; matrix products, arithmetic and copies ran while one was open for 2% of the time, Pallas kernels for 9%

profile of v8, /device:TPU:0, one launch (start us, length us, event | category | flops | bytes accessed | tf_op | source)
XLA Modules:
  0.0 119.8 jit_solution(17436575337802655124)
XLA Ops:
  0.6 1.9 %shard_map.180 = (bf16[80,512]{1,0:T(8,128)(2,1)S(1)}, bf16[80,512]{1,0:T(8,128)(2,1)S(1)}, bf16[2,80,512]{2,1,0:T(8,128)(2,1)S(1)}, bf16[2,80,512]{2,1,0:T(8,12...) custom-call(s32[2,128]{1,0:T(2,128)} %bitcast.57, f32[2,128]{1,0:T(2,128)} %bitcast.58, ...), custom_call_target="tpu_custom_call" | custom-call | flops 83886080 | tf_op jit(solution)/shard_map/pallas_call | solution.py:298
  2.6 3.1 %collective-permute-start = (bf16[2,80,512]{2,1,0:T(8,128)(2,1)S(1)}, bf16[2,80,512]{2,1,0:T(8,128)(2,1)S(1)}, u32[]{:S(2)}, u32[]{:S(2)}) collective-permute-start(bf16[2,80,512]{2,1,0:T(8,128)(2,1)S(1)} %get-tuple-element.65), channel_id=1, source_target_pairs={{0,8},{8,16},{16,24},{24,0},{1,9},{9,17},{17,25},{25,1},{2,10},{10... | collective-permute-start | bytes 491528 | tf_op jit(solution)/shard_map/ppermute | solution.py:30
  5.7 2.6 %collective-permute-start.1 = (bf16[2,80,512]{2,1,0:T(8,128)(2,1)S(1)}, bf16[2,80,512]{2,1,0:T(8,128)(2,1)S(1)}, u32[]{:S(2)}, u32[]{:S(2)}) collective-permute-start(bf16[2,80,512]{2,1,0:T(8,128)(2,1)S(1)} %get-tuple-element.66), channel_id=1, source_target_pairs={{0,16},{8,24},{16,0},{24,8},{1,17},{9,25},{17,1},{25,9},{2,18},{10... | collective-permute-start | bytes 491528 | tf_op jit(solution)/shard_map/ppermute | solution.py:30
  15.5 3.5 %collective-permute-done.1 = bf16[2,80,512]{2,1,0:T(8,128)(2,1)S(1)} collective-permute-done((bf16[2,80,512]{2,1,0:T(8,128)(2,1)S(1)}, bf16[2,80,512]{2,1,0:T(8,128)(2,1)S(1)}, u32[]{:S(2)}, u32[]{:S(2)}) %collective-permute-start.1) | collective-permute-done | bytes 163872 | tf_op jit(solution)/shard_map/ppermute | solution.py:30
  20.7 1.6 %collective-permute-start.4 = (bf16[240,512]{1,0:T(8,128)(2,1)S(1)}, bf16[240,512]{1,0:T(8,128)(2,1)S(1)}, u32[]{:S(2)}, u32[]{:S(2)}) collective-permute-start(bf16[240,512]{1,0:T(8,128)(2,1)S(1)} %get-tuple-element.127), channel_id=1, source_target_pairs={{0,4},{4,0},{1,5},{5,1},{2,6},{6,2},{3,7},{7,3},{8,12},{12,8},{9,1... | collective-permute-start | bytes 737288 | tf_op jit(solution)/shard_map/ppermute | solution.py:18
  23.0 7.6 %collective-permute-done.7.far_own_ref = bf16[2,80,512]{2,1,0:T(8,128)(2,1)S(1)} collective-permute-done((bf16[2,80,512]{2,1,0:T(8,128)(2,1)S(1)}, bf16[2,80,512]{2,1,0:T(8,128)(2,1)S(1)}, u32[]{:S(2)}, u32[]{:S(2)}) %collective-permute-start.7) | collective-permute-done | bytes 163872 | tf_op jit(solution)/shard_map/ppermute | solution.py:18
  30.6 1.6 %collective-permute-start.8 = (bf16[2,240,512]{2,1,0:T(8,128)(2,1)S(1)}, bf16[2,240,512]{2,1,0:T(8,128)(2,1)S(1)}, u32[]{:S(2)}, u32[]{:S(2)}) collective-permute-start(bf16[2,240,512]{2,1,0:T(8,128)(2,1)S(1)} %pad_maximum_fusion.pair_ref), channel_id=1, source_target_pairs={{0,4},{4,0},{1,5},{5,1},{2,6},{6,2},{3,7},{7,3},{8,12},{12,8},{9,1... | collective-permute-start | bytes 1474568 | tf_op jit(solution)/shard_map/ppermute | solution.py:18
  35.4 7.4 %collective-permute-done.8.rows_y_ref = bf16[2,240,512]{2,1,0:T(8,128)(2,1)S(1)} collective-permute-done((bf16[2,240,512]{2,1,0:T(8,128)(2,1)S(1)}, bf16[2,240,512]{2,1,0:T(8,128)(2,1)S(1)}, u32[]{:S(2)}, u32[]{:S(2)}) %collective-permute-start.8) | collective-permute-done | bytes 491552 | tf_op jit(solution)/shard_map/ppermute | solution.py:18
  46.3 2.6 %collective-permute-done.14.own_y_ref = bf16[224,512]{1,0:T(8,128)(2,1)S(1)} collective-permute-done((bf16[224,512]{1,0:T(8,128)(2,1)S(1)}, bf16[224,512]{1,0:T(8,128)(2,1)S(1)}, u32[]{:S(2)}, u32[]{:S(2)}) %collective-permute-start.14) | collective-permute-done | bytes 229408 | tf_op jit(solution)/shard_map/ppermute | solution.py:18
  50.4 2.8 %shard_map.181 = (bf16[400,2048]{1,0:T(8,128)(2,1)S(1)}, f32[400,512]{1,0:T(8,128)S(1)}, f32[400,512]{1,0:T(8,128)S(1)}, bf16[400,512]{1,0:T(8,128)(2,1)S(1)}, b...) custom-call(bf16[224,512]{1,0:T(8,128)(2,1)S(1)} %maximum_maximum_fusion.own_ref, ...), custom_call_target="tpu_custom_call" | custom-call | flops 2348810240 | tf_op jit(solution)/shard_map/pallas_call | solution.py:298
  53.3 3.6 %shard_map.182 = (bf16[240,2048]{1,0:T(8,128)(2,1)S(1)}, bf16[640,1024]{1,0:T(8,128)(2,1)S(1)}, bf16[240,512]{1,0:T(8,128)(2,1)S(1)}, bf16[640,512]{1,0:T(8,128)...) custom-call(bf16[2,240,512]{2,1,0:T(8,128)(2,1)S(1)} %collective-permute-done.8.rows_y_ref, ...), custom_call_target="tpu_custom_call" | custom-call | flops 3019898880 | tf_op jit(solution)/shard_map/pallas_call | solution.py:298
  60.2 2.5 %collective-permute-start.25 = (bf16[240,512]{1,0:T(8,128)(2,1)S(1)}, bf16[240,512]{1,0:T(8,128)(2,1)S(1)}, u32[]{:S(2)}, u32[]{:S(2)}) collective-permute-start(bf16[240,512]{1,0:T(8,128)(2,1)S(1)} %get-tuple-element.94), channel_id=1, source_target_pairs={{0,6},{2,4},{4,2},{6,0},{1,7},{3,5},{5,3},{7,1},{8,14},{10,12},{12... | collective-permute-start | bytes 737288 | tf_op jit(solution)/shard_map/ppermute | solution.py:22
  63.7 4.2 %collective-permute-start.26 = (bf16[2,64,512]{2,1,0:T(8,128)(2,1)S(1)}, bf16[2,64,512]{2,1,0:T(8,128)(2,1)S(1)}, u32[]{:S(2)}, u32[]{:S(2)}) collective-permute-start(bf16[2,64,512]{2,1,0:T(8,128)(2,1)S(1)} %pad_maximum_fusion.5.refs_0_), channel_id=1, source_target_pairs={{0,8},{8,16},{16,24},{24,0},{1,9},{9,17},{17,25},{25,1},{2,10},{10... | collective-permute-start | bytes 393224 | tf_op jit(solution)/shard_map/ppermute | solution.py:30
  68.0 3.2 %shard_map.186 = bf16[1,2048,512]{2,1,0:T(8,128)(2,1)} custom-call(bf16[400,2048]{1,0:T(8,128)(2,1)S(1)} %get-tuple-element.104.early_ref, bf16[240,2048]{1,0:T(8,128)(2,1)S(1)} %get-tuple-element.105.late_ref, bf16[640,512]{1,0:T(8,128)(2,1)S(1)} %get-tuple-element.85.d_up_ref), custom_call_target="tpu_custom_call" | custom-call | flops 1342177280 | tf_op jit(solution)/shard_map/pallas_call | solution.py:298
  71.1 2.4 %collective-permute-start.28 = (bf16[2,64,512]{2,1,0:T(8,128)(2,1)S(1)}, bf16[2,64,512]{2,1,0:T(8,128)(2,1)S(1)}, u32[]{:S(2)}, u32[]{:S(2)}) collective-permute-start(bf16[2,64,512]{2,1,0:T(8,128)(2,1)S(1)} %pad_maximum_fusion.5.refs_0_), channel_id=1, source_target_pairs={{0,24},{8,0},{16,8},{24,16},{1,25},{9,1},{17,9},{25,17},{2,26},{10... | collective-permute-start | bytes 393224 | tf_op jit(solution)/shard_map/ppermute | solution.py:30
  79.0 2.8 %collective-permute-start.29 = (bf16[80,512]{1,0:T(8,128)(2,1)S(1)}, bf16[80,512]{1,0:T(8,128)(2,1)S(1)}, u32[]{:S(2)}, u32[]{:S(2)}) collective-permute-start(bf16[80,512]{1,0:T(8,128)(2,1)S(1)} %get-tuple-element.125), channel_id=1, source_target_pairs={{0,24},{8,0},{16,8},{24,16},{1,25},{9,1},{17,9},{25,17},{2,26},{10... | collective-permute-start | bytes 245768 | tf_op jit(solution)/shard_map/ppermute | solution.py:30
  81.8 2.0 %collective-permute-start.30 = (bf16[80,512]{1,0:T(8,128)(2,1)S(1)}, bf16[80,512]{1,0:T(8,128)(2,1)S(1)}, u32[]{:S(2)}, u32[]{:S(2)}) collective-permute-start(bf16[80,512]{1,0:T(8,128)(2,1)S(1)} %get-tuple-element.124), channel_id=1, source_target_pairs={{0,16},{8,24},{16,0},{24,8},{1,17},{9,25},{17,1},{25,9},{2,18},{10... | collective-permute-start | bytes 245768 | tf_op jit(solution)/shard_map/ppermute | solution.py:30
  83.8 3.2 %shard_map.187 = bf16[1,512,2048]{2,1,0:T(8,128)(2,1)} custom-call(bf16[640,1024]{1,0:T(8,128)(2,1)S(1)} %get-tuple-element.106.near_ref, bf16[640,1024]{1,0:T(8,128)(2,1)S(1)} %get-tuple-element.107.far_ref, bf16[400,512]{1,0:T(8,128)(2,1)S(1)} %get-tuple-element.108.early_ref, bf16[240,512]{1,0:T(8,128)(2,1)S(1)} %get-tuple-element.109.late_ref), custom_call_target="tpu_custom_call" | custom-call | flops 1342177280 | tf_op jit(solution)/shard_map/pallas_call | solution.py:298
  87.1 3.5 %collective-permute-done.30 = bf16[80,512]{1,0:T(8,128)(2,1)S(1)} collective-permute-done((bf16[80,512]{1,0:T(8,128)(2,1)S(1)}, bf16[80,512]{1,0:T(8,128)(2,1)S(1)}, u32[]{:S(2)}, u32[]{:S(2)}) %collective-permute-start.30) | collective-permute-done | bytes 81952 | tf_op jit(solution)/shard_map/ppermute | solution.py:30
  90.9 7.3 %all_gather.3.d_normed_ref = bf16[128,2048]{1,0:T(8,128)(2,1)S(1)} all-gather(bf16[128,512]{1,0:T(8,128)(2,1)S(1)} %convolution_convert_fusion), channel_id=1, replica_groups=mesh['e'=4,'j'=2,'x'=2,'c'=2] {'x','c'}, dimensions={1}, use_global_device_ids=true | all-gather | bytes 655360 | tf_op jit(solution)/shard_map/all_gather | solution.py:479
  98.2 1.6 %shard_map.185 = (bf16[128,2048]{1,0:T(8,128)(2,1)}, bf16[8,64,256]{2,1,0:T(8,128)(2,1)}, bf16[128,256]{1,0:T(8,128)(2,1)}, f32[128,256]{1,0:T(8,128)S(1)}, bf16...) custom-call(bf16[128,2048]{1,0:T(8,128)(2,1)S(1)} %all_gather.3.d_normed_ref, bf16[128,2048]{1,0:T(8,128)(2,1)S(1)} %copy-done.3, ...), custom_call_target="tpu_custom_call" | custom-call | flops 4194304 | tf_op jit(solution)/shard_map/pallas_call | solution.py:298
  99.8 2.7 %collective-permute-start.33 = (bf16[1,256]{1,0:T(2,128)(2,1)S(1)}, bf16[1,256]{1,0:T(2,128)(2,1)S(1)}, u32[]{:S(2)}, u32[]{:S(2)}) collective-permute-start(bf16[1,256]{1,0:T(2,128)(2,1)S(1)} %get-tuple-element.113), channel_id=1, source_target_pairs={{0,4},{4,8},{8,12},{12,16},{16,20},{20,24},{24,28},{1,5},{5,9},{9,... | collective-permute-start | bytes 1544 | tf_op jit(solution)/shard_map/ppermute | solution.py:519
  103.8 4.6 %all-to-all-start = ((bf16[8,64,256]{2,1,0:T(8,128)(2,1)}), bf16[8,64,256]{2,1,0:T(8,128)(2,1)S(1)}, u32[]{:S(2)}, u32[]{:S(2)}) async-start(bf16[8,64,256]{2,1,0:T(8,128)(2,1)} %get-tuple-element.114), calls=%async_computation | async-start | bytes 524288 | tf_op jit(solution)/shard_map/all_to_all | solution.py:513
  109.1 8.1 %all-to-all-done = bf16[8,64,256]{2,1,0:T(8,128)(2,1)S(1)} async-done(((bf16[8,64,256]{2,1,0:T(8,128)(2,1)}), bf16[8,64,256]{2,1,0:T(8,128)(2,1)S(1)}, u32[]{:S(2)}, u32[]{:S(2)}) %all-to-all-start) | async-done | bytes 262176 | tf_op jit(solution)/shard_map/all_to_all | solution.py:513
  (105 shorter events, 32.4 us)
Async XLA Ops:
  2.6 13.0 %collective-permute-start = (bf16[2,80,512]{2,1,0:T(8,128)(2,1)S(1)}, bf16[2,80,512]{2,1,0:T(8,128)(2,1)S(1)}, u32[]{:S(2)}, u32[]{:S(2)}) collective-permute-start(bf16[2,80,512]{2,1,0:T(8,128)(2,1)S(1)} %get-tuple-element.65), channel_id=1, source_target_pairs={{0,8},{8,16},{16,24},{24,0},{1,9},{9,17},{17,25},{25,1},{2,10},{10... | collective-permute-start | bytes 491528 | tf_op jit(solution)/shard_map/ppermute | solution.py:30
  5.7 13.3 %collective-permute-start.1 = (bf16[2,80,512]{2,1,0:T(8,128)(2,1)S(1)}, bf16[2,80,512]{2,1,0:T(8,128)(2,1)S(1)}, u32[]{:S(2)}, u32[]{:S(2)}) collective-permute-start(bf16[2,80,512]{2,1,0:T(8,128)(2,1)S(1)} %get-tuple-element.66), channel_id=1, source_target_pairs={{0,16},{8,24},{16,0},{24,8},{1,17},{9,25},{17,1},{25,9},{2,18},{10... | collective-permute-start | bytes 491528 | tf_op jit(solution)/shard_map/ppermute | solution.py:30
  8.3 10.8 %collective-permute-start.2 = (bf16[2,80,512]{2,1,0:T(8,128)(2,1)S(1)}, bf16[2,80,512]{2,1,0:T(8,128)(2,1)S(1)}, u32[]{:S(2)}, u32[]{:S(2)}) collective-permute-start(bf16[2,80,512]{2,1,0:T(8,128)(2,1)S(1)} %get-tuple-element.67), channel_id=1, source_target_pairs={{0,24},{8,0},{16,8},{24,16},{1,25},{9,1},{17,9},{25,17},{2,26},{10... | collective-permute-start | bytes 491528 | tf_op jit(solution)/shard_map/ppermute | solution.py:30
  19.2 11.4 %collective-permute-start.3 = (bf16[240,512]{1,0:T(8,128)(2,1)S(1)}, bf16[240,512]{1,0:T(8,128)(2,1)S(1)}, u32[]{:S(2)}, u32[]{:S(2)}) collective-permute-start(bf16[240,512]{1,0:T(8,128)(2,1)S(1)} %get-tuple-element.129), channel_id=1, source_target_pairs={{0,2},{2,0},{1,3},{3,1},{4,6},{6,4},{5,7},{7,5},{8,10},{10,8},{9,1... | collective-permute-start | bytes 737288 | tf_op jit(solution)/shard_map/ppermute | solution.py:18
  20.7 9.8 %collective-permute-start.4 = (bf16[240,512]{1,0:T(8,128)(2,1)S(1)}, bf16[240,512]{1,0:T(8,128)(2,1)S(1)}, u32[]{:S(2)}, u32[]{:S(2)}) collective-permute-start(bf16[240,512]{1,0:T(8,128)(2,1)S(1)} %get-tuple-element.127), channel_id=1, source_target_pairs={{0,4},{4,0},{1,5},{5,1},{2,6},{6,2},{3,7},{7,3},{8,12},{12,8},{9,1... | collective-permute-start | bytes 737288 | tf_op jit(solution)/shard_map/ppermute | solution.py:18
  22.3 8.2 %collective-permute-start.7 = (bf16[2,80,512]{2,1,0:T(8,128)(2,1)S(1)}, bf16[2,80,512]{2,1,0:T(8,128)(2,1)S(1)}, u32[]{:S(2)}, u32[]{:S(2)}) collective-permute-start(bf16[2,80,512]{2,1,0:T(8,128)(2,1)S(1)} %pad_maximum_fusion.4.near_own_ref), channel_id=1, source_target_pairs={{0,2},{2,0},{1,3},{3,1},{4,6},{6,4},{5,7},{7,5},{8,10},{10,8},{9,1... | collective-permute-start | bytes 491528 | tf_op jit(solution)/shard_map/ppermute | solution.py:18
  30.6 12.3 %collective-permute-start.8 = (bf16[2,240,512]{2,1,0:T(8,128)(2,1)S(1)}, bf16[2,240,512]{2,1,0:T(8,128)(2,1)S(1)}, u32[]{:S(2)}, u32[]{:S(2)}) collective-permute-start(bf16[2,240,512]{2,1,0:T(8,128)(2,1)S(1)} %pad_maximum_fusion.pair_ref), channel_id=1, source_target_pairs={{0,4},{4,0},{1,5},{5,1},{2,6},{6,2},{3,7},{7,3},{8,12},{12,8},{9,1... | collective-permute-start | bytes 1474568 | tf_op jit(solution)/shard_map/ppermute | solution.py:18
  32.2 12.1 %collective-permute-start.9 = (bf16[2,240,512]{2,1,0:T(8,128)(2,1)S(1)}, bf16[2,240,512]{2,1,0:T(8,128)(2,1)S(1)}, u32[]{:S(2)}, u32[]{:S(2)}) collective-permute-start(bf16[2,240,512]{2,1,0:T(8,128)(2,1)S(1)} %pad_maximum_fusion.1.near_ref), channel_id=1, source_target_pairs={{0,2},{2,0},{1,3},{3,1},{4,6},{6,4},{5,7},{7,5},{8,10},{10,8},{9,1... | collective-permute-start | bytes 1474568 | tf_op jit(solution)/shard_map/ppermute | solution.py:18
  33.9 12.0 %collective-permute-start.13 = (bf16[224,512]{1,0:T(8,128)(2,1)S(1)}, bf16[224,512]{1,0:T(8,128)(2,1)S(1)}, u32[]{:S(2)}, u32[]{:S(2)}) collective-permute-start(bf16[224,512]{1,0:T(8,128)(2,1)S(1)} %maximum_maximum_fusion.own_ref), channel_id=1, source_target_pairs={{0,1},{1,0},{2,3},{3,2},{4,5},{5,4},{6,7},{7,6},{8,9},{9,8},{10,11... | collective-permute-start | bytes 688136 | tf_op jit(solution)/shard_map/ppermute | solution.py:18
  34.5 15.9 %collective-permute-start.16 = (bf16[2,240,512]{2,1,0:T(8,128)(2,1)S(1)}, bf16[2,240,512]{2,1,0:T(8,128)(2,1)S(1)}, u32[]{:S(2)}, u32[]{:S(2)}) collective-permute-start(bf16[2,240,512]{2,1,0:T(8,128)(2,1)S(1)} %pad_maximum_fusion.pair_ref), channel_id=1, source_target_pairs={{0,1},{1,0},{2,3},{3,2},{4,5},{5,4},{6,7},{7,6},{8,9},{9,8},{10,11... | collective-permute-start | bytes 1474568 | tf_op jit(solution)/shard_map/ppermute | solution.py:18
  35.3 15.1 %collective-permute-start.18 = (bf16[2,240,512]{2,1,0:T(8,128)(2,1)S(1)}, bf16[2,240,512]{2,1,0:T(8,128)(2,1)S(1)}, u32[]{:S(2)}, u32[]{:S(2)}) collective-permute-start(bf16[2,240,512]{2,1,0:T(8,128)(2,1)S(1)} %pad_maximum_fusion.1.near_ref), channel_id=1, source_target_pairs={{0,1},{1,0},{2,3},{3,2},{4,5},{5,4},{6,7},{7,6},{8,9},{9,8},{10,11... | collective-permute-start | bytes 1474568 | tf_op jit(solution)/shard_map/ppermute | solution.py:18
  60.2 11.0 %collective-permute-start.25 = (bf16[240,512]{1,0:T(8,128)(2,1)S(1)}, bf16[240,512]{1,0:T(8,128)(2,1)S(1)}, u32[]{:S(2)}, u32[]{:S(2)}) collective-permute-start(bf16[240,512]{1,0:T(8,128)(2,1)S(1)} %get-tuple-element.94), channel_id=1, source_target_pairs={{0,6},{2,4},{4,2},{6,0},{1,7},{3,5},{5,3},{7,1},{8,14},{10,12},{12... | collective-permute-start | bytes 737288 | tf_op jit(solution)/shard_map/ppermute | solution.py:22
  62.7 11.7 %collective-permute-start.24 = (bf16[240,512]{1,0:T(8,128)(2,1)S(1)}, bf16[240,512]{1,0:T(8,128)(2,1)S(1)}, u32[]{:S(2)}, u32[]{:S(2)}) collective-permute-start(bf16[240,512]{1,0:T(8,128)(2,1)S(1)} %get-tuple-element.93), channel_id=1, source_target_pairs={{0,4},{4,0},{1,5},{5,1},{2,6},{6,2},{3,7},{7,3},{8,12},{12,8},{9,1... | collective-permute-start | bytes 737288 | tf_op jit(solution)/shard_map/ppermute | solution.py:18
  63.2 12.7 %collective-permute-start.23 = (bf16[240,512]{1,0:T(8,128)(2,1)S(1)}, bf16[240,512]{1,0:T(8,128)(2,1)S(1)}, u32[]{:S(2)}, u32[]{:S(2)}) collective-permute-start(bf16[240,512]{1,0:T(8,128)(2,1)S(1)} %get-tuple-element.92), channel_id=1, source_target_pairs={{0,2},{2,0},{1,3},{3,1},{4,6},{6,4},{5,7},{7,5},{8,10},{10,8},{9,1... | collective-permute-start | bytes 737288 | tf_op jit(solution)/shard_map/ppermute | solution.py:18
  63.7 13.1 %collective-permute-start.26 = (bf16[2,64,512]{2,1,0:T(8,128)(2,1)S(1)}, bf16[2,64,512]{2,1,0:T(8,128)(2,1)S(1)}, u32[]{:S(2)}, u32[]{:S(2)}) collective-permute-start(bf16[2,64,512]{2,1,0:T(8,128)(2,1)S(1)} %pad_maximum_fusion.5.refs_0_), channel_id=1, source_target_pairs={{0,8},{8,16},{16,24},{24,0},{1,9},{9,17},{17,25},{25,1},{2,10},{10... | collective-permute-start | bytes 393224 | tf_op jit(solution)/shard_map/ppermute | solution.py:30
  67.9 10.1 %collective-permute-start.27 = (bf16[2,64,512]{2,1,0:T(8,128)(2,1)S(1)}, bf16[2,64,512]{2,1,0:T(8,128)(2,1)S(1)}, u32[]{:S(2)}, u32[]{:S(2)}) collective-permute-start(bf16[2,64,512]{2,1,0:T(8,128)(2,1)S(1)} %pad_maximum_fusion.5.refs_0_), channel_id=1, source_target_pairs={{0,16},{8,24},{16,0},{24,8},{1,17},{9,25},{17,1},{25,9},{2,18},{10... | collective-permute-start | bytes 393224 | tf_op jit(solution)/shard_map/ppermute | solution.py:30
  71.1 7.8 %collective-permute-start.28 = (bf16[2,64,512]{2,1,0:T(8,128)(2,1)S(1)}, bf16[2,64,512]{2,1,0:T(8,128)(2,1)S(1)}, u32[]{:S(2)}, u32[]{:S(2)}) collective-permute-start(bf16[2,64,512]{2,1,0:T(8,128)(2,1)S(1)} %pad_maximum_fusion.5.refs_0_), channel_id=1, source_target_pairs={{0,24},{8,0},{16,8},{24,16},{1,25},{9,1},{17,9},{25,17},{2,26},{10... | collective-permute-start | bytes 393224 | tf_op jit(solution)/shard_map/ppermute | solution.py:30
  74.4 9.4 %collective-permute-start.20 = (bf16[80,512]{1,0:T(8,128)(2,1)S(1)}, bf16[80,512]{1,0:T(8,128)(2,1)S(1)}, u32[]{:S(2)}, u32[]{:S(2)}) collective-permute-start(bf16[80,512]{1,0:T(8,128)(2,1)S(1)} %get-tuple-element.88), channel_id=1, source_target_pairs={{0,2},{2,0},{1,3},{3,1},{4,6},{6,4},{5,7},{7,5},{8,10},{10,8},{9,1... | collective-permute-start | bytes 245768 | tf_op jit(solution)/shard_map/ppermute | solution.py:18
  75.9 11.2 %collective-permute-start.21 = (bf16[80,512]{1,0:T(8,128)(2,1)S(1)}, bf16[80,512]{1,0:T(8,128)(2,1)S(1)}, u32[]{:S(2)}, u32[]{:S(2)}) collective-permute-start(bf16[80,512]{1,0:T(8,128)(2,1)S(1)} %get-tuple-element.89), channel_id=1, source_target_pairs={{0,4},{4,0},{1,5},{5,1},{2,6},{6,2},{3,7},{7,3},{8,12},{12,8},{9,1... | collective-permute-start | bytes 245768 | tf_op jit(solution)/shard_map/ppermute | solution.py:18
  76.8 10.2 %collective-permute-start.22 = (bf16[80,512]{1,0:T(8,128)(2,1)S(1)}, bf16[80,512]{1,0:T(8,128)(2,1)S(1)}, u32[]{:S(2)}, u32[]{:S(2)}) collective-permute-start(bf16[80,512]{1,0:T(8,128)(2,1)S(1)} %get-tuple-element.90), channel_id=1, source_target_pairs={{0,6},{2,4},{4,2},{6,0},{1,7},{3,5},{5,3},{7,1},{8,14},{10,12},{12... | collective-permute-start | bytes 245768 | tf_op jit(solution)/shard_map/ppermute | solution.py:22
  79.0 8.1 %collective-permute-start.29 = (bf16[80,512]{1,0:T(8,128)(2,1)S(1)}, bf16[80,512]{1,0:T(8,128)(2,1)S(1)}, u32[]{:S(2)}, u32[]{:S(2)}) collective-permute-start(bf16[80,512]{1,0:T(8,128)(2,1)S(1)} %get-tuple-element.125), channel_id=1, source_target_pairs={{0,24},{8,0},{16,8},{24,16},{1,25},{9,1},{17,9},{25,17},{2,26},{10... | collective-permute-start | bytes 245768 | tf_op jit(solution)/shard_map/ppermute | solution.py:30
  81.8 8.8 %collective-permute-start.30 = (bf16[80,512]{1,0:T(8,128)(2,1)S(1)}, bf16[80,512]{1,0:T(8,128)(2,1)S(1)}, u32[]{:S(2)}, u32[]{:S(2)}) collective-permute-start(bf16[80,512]{1,0:T(8,128)(2,1)S(1)} %get-tuple-element.124), channel_id=1, source_target_pairs={{0,16},{8,24},{16,0},{24,8},{1,17},{9,25},{17,1},{25,9},{2,18},{10... | collective-permute-start | bytes 245768 | tf_op jit(solution)/shard_map/ppermute | solution.py:30
  99.8 8.6 %collective-permute-start.33 = (bf16[1,256]{1,0:T(2,128)(2,1)S(1)}, bf16[1,256]{1,0:T(2,128)(2,1)S(1)}, u32[]{:S(2)}, u32[]{:S(2)}) collective-permute-start(bf16[1,256]{1,0:T(2,128)(2,1)S(1)} %get-tuple-element.113), channel_id=1, source_target_pairs={{0,4},{4,8},{8,12},{12,16},{16,20},{20,24},{24,28},{1,5},{5,9},{9,... | collective-permute-start | bytes 1544 | tf_op jit(solution)/shard_map/ppermute | solution.py:519
  103.8 13.4 %all-to-all-start = ((bf16[8,64,256]{2,1,0:T(8,128)(2,1)}), bf16[8,64,256]{2,1,0:T(8,128)(2,1)S(1)}, u32[]{:S(2)}, u32[]{:S(2)}) async-start(bf16[8,64,256]{2,1,0:T(8,128)(2,1)} %get-tuple-element.114), calls=%async_computation | async-start | bytes 524288 | tf_op jit(solution)/shard_map/all_to_all | solution.py:513
  (23 other events, 267.1 us)
